TPU v7x, 256 devices: a 4x2x16 block of a 4x16x16 slice. The times are simulated.
256 devices in a mesh: grp: 2 (over y), fs: 32 (over z, core), tp: 4 (over x).
Axes of the slice: x: 4, y: 2, z: 16, core: 2. Of those that a mesh axis runs over, the one named last changes fastest.
The devices are a block of a 4x16x16 slice.
Arguments:
- tokens: bfloat16 [4096, 2048], P(('grp', 'fs')), parts along dimension 0, may hold values from -6 to 6
- routes: int32 [4096, 2], P(('grp', 'fs')), parts along dimension 0, may hold values from 0 to 3, as said below
- route_logits: float32 [4096, 2], P(('grp', 'fs')), parts along dimension 0, may hold values from -8 to 8
- gain: float32 [2048], P('fs'), may hold values from 0.1 to 1.9
- w_gate: float32 [4, 2048, 7168], P(None, 'fs', 'tp'), may hold values from -0.125 to 0.125
- w_up: float32 [4, 2048, 7168], P(None, 'fs', 'tp'), may hold values from -0.125 to 0.125
- w_down: float32 [4, 7168, 2048], P(None, 'fs', 'tp'), may hold values from -0.0625 to 0.0625
Outputs:
- gate_served: bfloat16 [8, 2048, 7168], P(('grp', 'tp'), None, 'fs'), parts along dimension 0
- up_served: bfloat16 [8, 2048, 7168], P(('grp', 'tp'), None, 'fs'), parts along dimension 0
- down_served: bfloat16 [8, 7168, 2048], P(('grp', 'tp'), 'fs'), parts along dimension 0
- mixed: bfloat16 [4096, 2048], P(('grp', 'fs'), 'tp'), parts along dimension 0
There are 2 independent parts, one for each index of `grp`. A program takes and returns all parts, laid end to end along the dimension named above; an argument that names none is the same for every part. Nothing has to cross between parts.
Inputs may be any that keep to these rules, and one draw needn't show every extreme that they name: `routes`: each row names 2 different experts; every expert is named by some row.
All inputs are finite; a program needn't handle non-finite values.
Results may differ from a plain program's by a relative error of at most 0.0085.
Values may be sent and summed in bfloat16 or wider, within the bound.
No kernel may reach another device: no remote copies, remote signals or barrier semaphores. Data moves between devices by JAX's collectives and lax.ppermute only.
A program may use at most 128 MiB of HBM per device.

v0:
```python
import functools

import jax
import jax.numpy as jnp
from jax import lax
from jax.experimental import pallas as pl
from jax.experimental.pallas import tpu as pltpu
from jax.sharding import PartitionSpec as P

BF16, F32 = jnp.bfloat16, jnp.float32
LANES = 128
VMEM = 56 * 1024 * 1024


def params(*semantics):
    return pltpu.CompilerParams(dimension_semantics=semantics, vmem_limit_bytes=VMEM)


def pack_kernel(parts, width, place_ref, scale_ref, gate_ref, up_ref, first_ref, *late_refs):
    del place_ref
    both = jnp.concatenate([gate_ref[0], up_ref[0]], axis=0)
    columns = (both.T * scale_ref[...]).astype(BF16)
    blocks = columns.shape[0] // width
    for k in range(blocks):
        low, size = parts[0]
        first_ref[0, k] = columns[k * width + low : k * width + low + size]
    for shift, late_ref in enumerate(late_refs):

        @pl.when(pl.program_id(0) == shift)
        def _():
            low, size = parts[1]
            for k in range(blocks):
                late_ref[k] = columns[k * width + low : k * width + low + size]


def pack(place, gain, w_gate, w_up, parts, width):
    experts, rows, columns = w_gate.shape
    scale = jnp.concatenate([gain, gain])[None, :]
    blocks = columns // width
    chosen = lambda s, place_ref: (lax.rem(s + place_ref[0], experts), 0, 0)
    out = pl.pallas_call(
        functools.partial(pack_kernel, parts, width),
        grid_spec=pltpu.PrefetchScalarGridSpec(
            num_scalar_prefetch=1,
            grid=(experts,),
            in_specs=[
                pl.BlockSpec((1, 2 * rows), lambda s, place_ref: (0, 0)),
                pl.BlockSpec((1, rows, columns), chosen),
                pl.BlockSpec((1, rows, columns), chosen),
            ],
            out_specs=[
                pl.BlockSpec(
                    (1, blocks, parts[0][1], 2 * rows),
                    lambda s, place_ref: (lax.rem(s + place_ref[0], experts), 0, 0, 0),
                ),
                *[pl.BlockSpec((blocks, parts[1][1], 2 * rows), lambda s, place_ref: (0, 0, 0))] * experts,
            ],
        ),
        out_shape=[
            jax.ShapeDtypeStruct((experts, blocks, parts[0][1], 2 * rows), BF16),
            *[jax.ShapeDtypeStruct((blocks, parts[1][1], 2 * rows), BF16)] * experts,
        ],
        compiler_params=params("arbitrary"),
        cost_estimate=pl.CostEstimate(
            flops=experts * rows * columns * 1000, bytes_accessed=experts * rows * columns * 12, transcendentals=0
        ),
        name="pack",
    )(place, scale, w_gate, w_up)
    return out[0], out[1:]


def cast_kernel(place_ref, down_ref, padded_ref, *piece_refs):
    del place_ref
    rows = down_ref.shape[1]
    cast = down_ref[0].astype(BF16)
    padded_ref[0, :rows] = cast
    padded_ref[0, rows:] = jnp.zeros((padded_ref.shape[1] - rows, cast.shape[1]), BF16)
    for shift, piece_ref in enumerate(piece_refs):

        @pl.when(pl.program_id(0) == shift)
        def _():
            piece_ref[...] = cast


def cast_down(place, w_down, padded):
    experts, rows, features = w_down.shape
    out = pl.pallas_call(
        cast_kernel,
        grid_spec=pltpu.PrefetchScalarGridSpec(
            num_scalar_prefetch=1,
            grid=(experts,),
            in_specs=[pl.BlockSpec((1, rows, features), lambda s, p: (lax.rem(s + p[0], experts), 0, 0))],
            out_specs=[
                pl.BlockSpec((1, padded, features), lambda s, p: (lax.rem(s + p[0], experts), 0, 0)),
                *[pl.BlockSpec((rows, features), lambda s, p: (0, 0))] * experts,
            ],
        ),
        out_shape=[
            jax.ShapeDtypeStruct((experts, padded, features), BF16),
            *[jax.ShapeDtypeStruct((rows, features), BF16)] * experts,
        ],
        compiler_params=params("arbitrary"),
        cost_estimate=pl.CostEstimate(flops=w_down.size * 500, bytes_accessed=w_down.size * 8, transcendentals=0),
        name="cast_down",
    )(place, w_down)
    return out[0], out[1:]


def join_kernel(place_ref, *refs):
    del place_ref
    out_ref = refs[-1]
    for shift, ref in enumerate(refs[:-1]):

        @pl.when(pl.program_id(0) == shift)
        def _():
            out_ref[...] = ref[...]


def join(place, pieces, dim):
    n, dims = len(pieces), pieces[0].shape
    spot = lambda s, p: tuple(lax.rem(p[0] + n - s, n) if d == dim else 0 for d in range(len(dims)))
    whole = tuple(size * n if d == dim else size for d, size in enumerate(dims))
    return pl.pallas_call(
        join_kernel,
        grid_spec=pltpu.PrefetchScalarGridSpec(
            num_scalar_prefetch=1,
            grid=(n,),
            in_specs=[pl.BlockSpec(dims, lambda s, p: (0,) * len(dims))] * n,
            out_specs=pl.BlockSpec(dims, spot),
        ),
        out_shape=jax.ShapeDtypeStruct(whole, BF16),
        compiler_params=params("arbitrary"),
        cost_estimate=pl.CostEstimate(flops=pieces[0].size * n * 500, bytes_accessed=pieces[0].size * n * 4, transcendentals=0),
        name="join",
    )(place, *pieces)


def unpack_kernel(size, recv_ref, gate_ref, up_ref, both_ref):
    half = recv_ref.shape[2] // 2
    pad = both_ref.shape[0] // 2 - size
    if pad:
        zeros = jnp.zeros((pad, both_ref.shape[1]), BF16)
        both_ref[size : size + pad] = zeros
        both_ref[size + pad + size :] = zeros
    for k in range(recv_ref.shape[0] // 2):
        one, two = recv_ref[2 * k], recv_ref[2 * k + 1]
        at = slice(k * 2 * half, (k + 1) * 2 * half)
        gate = jnp.concatenate([one[:, :half], two[:, :half]], axis=1)
        up = jnp.concatenate([one[:, half:], two[:, half:]], axis=1)
        gate_ref[:, at] = gate
        up_ref[:, at] = up
        both_ref[0:size, at] = gate
        both_ref[size + pad : size + pad + size, at] = up


def unpack(recv, padded):
    count, size, lanes = recv.shape
    width = count * lanes // 2
    return pl.pallas_call(
        functools.partial(unpack_kernel, size),
        in_specs=[pl.BlockSpec(memory_space=pltpu.VMEM)],
        out_specs=[pl.BlockSpec(memory_space=pltpu.VMEM)] * 3,
        out_shape=[
            jax.ShapeDtypeStruct((size, width), BF16),
            jax.ShapeDtypeStruct((size, width), BF16),
            jax.ShapeDtypeStruct((2 * padded, width), BF16),
        ],
        compiler_params=params(),
        cost_estimate=pl.CostEstimate(flops=count * size * lanes * 40, bytes_accessed=count * size * lanes * 6, transcendentals=0),
        name="unpack",
    )(recv)


def hidden_kernel(depth, n_tp, first, place_ref, early_ref, late_ref, *refs):
    token_refs, (out_ref, block_ref) = refs[:-2], refs[-2:]
    quarter, core = pl.program_id(0) + first, pl.program_id(1)
    shift = lax.rem(place_ref[0] + n_tp - quarter, n_tp)
    other = jnp.where(core == place_ref[1], 0, 1)
    for k, token_ref in enumerate(token_refs):

        @pl.when(2 * shift + other == k)
        def _():
            block_ref[...] = token_ref[...]

    tokens = block_ref[:, :depth]
    shares = block_ref[:, depth:].astype(F32)
    lane = lax.broadcasted_iota(jnp.int32, shares.shape, 1)
    share = jnp.sum(jnp.where(lane == place_ref[0], shares, 0.0), axis=1, keepdims=True)
    at = 0
    for both_ref in (early_ref, late_ref):
        acts = lax.dot_general(tokens, both_ref[...], (((1,), (1,)), ((), ())), preferred_element_type=F32)
        half = acts.shape[1] // 2
        gate, up = acts[:, :half], acts[:, half:]
        hidden = gate / (1.0 + jnp.exp(-gate)) * up * share
        out_ref[0, 0, :, at : at + half] = hidden.astype(BF16)
        at += half


def hidden_of(place, tokens, boths, depth, first, count):
    n_tp = len(tokens) // 2
    rows, wide = tokens[0].shape
    half = sum(both.shape[0] for both in boths) // 2
    work = count * 2 * rows
    vmem = pl.BlockSpec(memory_space=pltpu.VMEM)
    return pl.pallas_call(
        functools.partial(hidden_kernel, depth, n_tp, first),
        grid=(count, 2),
        in_specs=[pl.BlockSpec(memory_space=pltpu.SMEM), vmem, vmem, *[vmem] * len(tokens)],
        out_specs=pl.BlockSpec((1, 1, rows, half), lambda q, c: (q, c, 0, 0)),
        out_shape=jax.ShapeDtypeStruct((count, 2, rows, half), BF16),
        scratch_shapes=[pltpu.VMEM((rows, wide), BF16)],
        compiler_params=params("arbitrary", "arbitrary"),
        cost_estimate=pl.CostEstimate(
            flops=2 * work * depth * 2 * half, bytes_accessed=work * wide * 2, transcendentals=work * half
        ),
        name="hidden",
    )(place, *boths, *tokens)


def down_kernel(place_ref, down_ref, *refs):
    parts, (keep_ref, send_ref) = refs[:-2], refs[-2:]
    experts = len(parts)
    total = None
    for shift, part_ref in enumerate(parts):
        left = part_ref[0].reshape(-1, part_ref.shape[3])
        source = lax.rem(place_ref[0] + experts - shift, experts)
        term = jnp.dot(left, down_ref[source], preferred_element_type=F32)
        total = term if total is None else total + term
    rows = total.shape[0] // 2
    mine = place_ref[1] == 0
    even, odd = total[:rows], total[rows:]
    keep = jnp.where(mine, even, odd)
    send = jnp.where(mine, odd, even).astype(BF16)
    keep_ref[...] = keep.reshape(keep_ref.shape)
    send_ref[...] = send.reshape(send_ref.shape)


def down_of(place, down, pieces, n_z):
    features = down.shape[2]
    count, _, rows, width = pieces[0].shape
    out = pl.BlockSpec((n_z, 1, rows // n_z, features), lambda q: (0, q, 0, 0))
    shape = (n_z, count, rows // n_z, features)
    return pl.pallas_call(
        down_kernel,
        grid=(count,),
        in_specs=[
            pl.BlockSpec(memory_space=pltpu.SMEM),
            pl.BlockSpec(down.shape, lambda q: (0, 0, 0)),
            *[pl.BlockSpec((1, 2, rows, width), lambda q: (q, 0, 0, 0))] * len(pieces),
        ],
        out_specs=[out, out],
        out_shape=[jax.ShapeDtypeStruct(shape, F32), jax.ShapeDtypeStruct(shape, BF16)],
        compiler_params=params("arbitrary"),
        cost_estimate=pl.CostEstimate(
            flops=4 * count * rows * down.size, bytes_accessed=count * rows * 2 * (features * 3 + 2048), transcendentals=0
        ),
        name="down",
    )(place, down, *pieces)


def held_kernel(in_ref, out_ref):
    out_ref[...] = in_ref[...]


def held(array):
    vmem = pl.BlockSpec(memory_space=pltpu.VMEM)
    return pl.pallas_call(
        held_kernel,
        in_specs=[vmem],
        out_specs=vmem,
        out_shape=jax.ShapeDtypeStruct(array.shape, array.dtype),
        compiler_params=params(),
        cost_estimate=pl.CostEstimate(flops=array.size * 500, bytes_accessed=array.size * 4, transcendentals=0),
        name="held",
    )(array)


def around(array, axis):
    n = lax.axis_size(axis)
    got = {0: array}
    for shift in [1, n - 1, *range(2, n - 1)]:
        got[shift] = lax.ppermute(array, axis, [(i, (i + shift) % n) for i in range(n)])
    return [got[shift] for shift in range(n)]


def dealt(pieces, axis):
    n = lax.axis_size(axis)
    got = {0: pieces[0]}
    for shift in [1, n - 1, *range(2, n - 1)]:
        got[shift] = lax.ppermute(pieces[shift], axis, [(i, (i + shift) % n) for i in range(n)])
    return [got[shift] for shift in range(n)]


def body(chunks, tokens, routes, route_logits, gain, w_gate, w_up, w_down):
    n_fs, n_tp = lax.axis_size("fs"), lax.axis_size("tp")
    _, hidden_rows, features = w_down.shape
    count, depth = tokens.shape
    me = lax.axis_index("fs")
    expert = lax.axis_index("tp").astype(jnp.int32)
    place = jnp.stack([expert, (me % 2).astype(jnp.int32)])
    parts = ((0, LANES), (LANES, hidden_rows - LANES))
    swap = [(i, i + 1 - 2 * (i % 2)) for i in range(n_fs)]
    columns = [list(range(c, n_fs, 2)) for c in range(2)]
    n_z = n_fs // 2

    some = count // n_tp
    tokens, routes, route_logits = (
        lax.dynamic_slice_in_dim(a, expert * some, some) for a in (tokens, routes, route_logits)
    )
    values = tokens.astype(F32)
    mean_square = jnp.mean(values * values, axis=-1, keepdims=True)
    normed = (values * lax.rsqrt(mean_square + 1e-06)).astype(BF16)
    first = jax.nn.sigmoid(route_logits[:, 0:1] - route_logits[:, 1:2])
    second = jax.nn.sigmoid(route_logits[:, 1:2] - route_logits[:, 0:1])
    names = lax.broadcasted_iota(jnp.int32, (some, LANES), 1)
    share = first * (routes[:, 0:1] == names).astype(F32)
    share = (share + second * (routes[:, 1:2] == names).astype(F32)).astype(BF16)
    rows = jnp.concatenate([normed, share], axis=1)
    rows, place = lax.optimization_barrier((rows, place))
    quarter = lax.all_gather(rows, "fs", axis=0, axis_index_groups=columns, tiled=True)
    first_part, late_parts = pack(place, gain, w_gate, w_up, parts, hidden_rows)
    first_part = first_part.reshape(n_tp, -1, first_part.shape[3])
    across = lax.all_to_all(first_part, "tp", 0, 0, tiled=True).reshape(n_fs, -1, first_part.shape[2])
    received = lax.all_to_all(across, "fs", 0, 0, tiled=True)
    late_across = join(place, dealt(late_parts, "tp"), 0)
    late_across, received = lax.optimization_barrier((late_across, received))
    late_received = lax.all_to_all(late_across, "fs", 0, 0, tiled=True)

    quarter = held(quarter)
    quarters = around(quarter, "tp")
    all_tokens = []
    for piece in quarters:
        all_tokens += [piece, lax.ppermute(piece, "fs", swap)]

    down_padded, down_pieces = cast_down(place, w_down, len(parts) * LANES)
    down_served = join(place, dealt(down_pieces, "tp"), 1)[None]

    gate_a, up_a, both_a = unpack(received, LANES)
    gate_b, up_b, both_b = unpack(late_received, LANES)
    gates, ups = (gate_a, gate_b), (up_a, up_b)
    per = n_tp // chunks
    hiddens = [hidden_of(place, all_tokens, (both_a, both_b), depth, q * per, per) for q in range(chunks)]
    gathered = []
    for hidden in hiddens:
        gathered.append(around(hidden, "tp"))
    *gathered[0], hiddens[1] = lax.optimization_barrier((*gathered[0], hiddens[1]))
    gathered[1][0] = hiddens[1]
    out = []
    for q in range(chunks):
        keep, send = down_of(place, down_padded, gathered[q], n_z)
        summed = (keep + lax.ppermute(send, "fs", swap).astype(F32)).astype(BF16)
        summed = summed.reshape(n_z, per * some, features)
        spread = lax.all_to_all(summed, "fs", 0, 0, axis_index_groups=columns, tiled=True)
        out.append(jnp.sum(spread.astype(F32), axis=0).astype(BF16))
    mixed = jnp.concatenate(out, axis=0)
    gate_served = jnp.concatenate(gates, axis=0).T[None]
    up_served = jnp.concatenate(ups, axis=0).T[None]
    return gate_served, up_served, down_served, mixed


def layer(chunks, *args):
    return body(chunks, *args)


def solution(mesh):
    return jax.shard_map(
        functools.partial(layer, 2),
        mesh=mesh,
        in_specs=(
            P(("grp", "fs"), None),
            P(("grp", "fs"), None),
            P(("grp", "fs"), None),
            P("fs"),
            P(None, "fs", "tp"),
            P(None, "fs", "tp"),
            P(None, "fs", "tp"),
        ),
        out_specs=(
            P(("grp", "tp"), None, "fs"),
            P(("grp", "tp"), None, "fs"),
            P(("grp", "tp"), "fs", None),
            P(("grp", "fs"), "tp"),
        ),
        check_vma=False,
    )
```

profile of v0, /device:TPU:40, one launch (start us, length us, event | category | flops | bytes accessed | tf_op | source)
XLA Modules:
  0.0 344.9 jit_solution(7454964174455903135)
XLA Ops:
  7.2 0.7 copy-done
  7.9 0.7 constant_dynamic-slice_fusion
  8.7 1.0 fusion
  9.7 0.9 fusion.1
  10.6 0.6 pad_add_fusion.place_ref
  11.3 0.6 pad_maximum_fusion
  12.0 1.3 maximum_bitcast_fusion.2.scale_ref
  13.3 5.4 %pack.1 = (bf16[4,8,128,128]{3,2,1,0:T(8,128)(2,1)}, bf16[8,96,128]{2,1,0:T(8,128)(2,1)}, bf16[8,96,128]{2,1,0:T(8,128)(2,1)}, bf16[8,96,128]{2,1,0:T(8,128)(2,1)}, bf16[8,96,128]{2,1,0:T(8,128)(2,1)}) custom-call(s32[2]{0:T(128)} %pad_add_fusion.place_ref, f32[1,128]{1,0:T(1,128)} %maximum_bitcast_fusion.2.scale_ref, f32[4,64,1792]{2,1,0:T(8,128)} %gate_ref.1, ...), custom_call_target="tpu_custom_call" | custom-call | flops 458752000 | bytes 5505024 | tf_op jit(solution)/shard_map/pack/pallas_call | solution.py:41
  18.7 20.0 %all_to_all.25 = bf16[4,1024,128]{2,1,0:T(8,128)(2,1)} all-to-all(bf16[4,1024,128]{2,1,0:T(8,128)(2,1)} %bitcast.25), channel_id=1, replica_groups=mesh['grp'=2,'fs'=32,'tp'=4] {'tp'}, dimensions={0} | all-to-all | bytes 2097152 | tf_op jit(solution)/shard_map/all_to_all | solution.py:323
  38.7 24.7 %all-to-all-start.1 = ((bf16[32,128,128]{2,1,0:T(8,128)(2,1)}), bf16[32,128,128]{2,1,0:T(8,128)(2,1)S(1)}, u32[]{:S(2)}, u32[]{:S(2)}) async-start(bf16[32,128,128]{2,1,0:T(8,128)(2,1)} %bitcast.8), calls=%async_computation.1 | async-start | bytes 2097152 | tf_op jit(solution)/shard_map/all_to_all | solution.py:324
  63.6 0.7 all-gather.2.cloned.1.call-update
  64.3 0.9 collective-permute-start
  65.2 1.9 collective-permute-start.1
  67.0 1.0 collective-permute-start.2
  68.0 8.4 %collective-permute-done.refs_1_ = bf16[8,96,128]{2,1,0:T(8,128)(2,1)S(1)} collective-permute-done((bf16[8,96,128]{2,1,0:T(8,128)(2,1)S(1)}, bf16[8,96,128]{2,1,0:T(8,128)(2,1)S(1)}, u32[]{:S(2)}, u32[]{:S(2)}) %collective-permute-start) | collective-permute-done | bytes 196640 | tf_op jit(solution)/shard_map/ppermute | solution.py:290
  76.5 0.6 collective-permute-done.2.refs_3_
  77.2 0.5 copy-done.15
  77.7 3.4 join.2
  81.1 41.1 %all-to-all-done.1.recv_ref = bf16[32,128,128]{2,1,0:T(8,128)(2,1)S(1)} async-done(((bf16[32,128,128]{2,1,0:T(8,128)(2,1)}), bf16[32,128,128]{2,1,0:T(8,128)(2,1)S(1)}, u32[]{:S(2)}, u32[]{:S(2)}) %all-to-all-start.1) | async-done | bytes 1048608 | tf_op jit(solution)/shard_map/all_to_all | solution.py:324
  122.2 5.7 %all-to-all-start.2 = ((bf16[32,96,128]{2,1,0:T(8,128)(2,1)}), bf16[32,96,128]{2,1,0:T(8,128)(2,1)}, u32[]{:S(2)}, u32[]{:S(2)}) async-start(bf16[32,96,128]{2,1,0:T(8,128)(2,1)} %join.2), calls=%async_computation.2 | async-start | bytes 1572864 | tf_op jit(solution)/shard_map/all_to_all | solution.py:327
  128.0 24.1 %all-gather.2.cloned.1.call-done.in_ref = bf16[256,2176]{1,0:T(8,128)(2,1)} async-done(((bf16[16,2176]{1,0:T(8,128)(2,1)}), bf16[256,2176]{1,0:T(8,128)(2,1)}) %all-gather.2.cloned.1.call-update) | async-done | bytes 1114128 | tf_op jit(solution)/shard_map/all_gather | solution.py:320
  152.1 2.3 held.1.refs_0_
  154.4 3.7 %collective-permute-start.9 = (bf16[256,2176]{1,0:T(8,128)(2,1)}, bf16[256,2176]{1,0:T(8,128)(2,1)S(1)}, u32[]{:S(2)}, u32[]{:S(2)}) collective-permute-start(bf16[256,2176]{1,0:T(8,128)(2,1)} %held.1.refs_0_), channel_id=1, source_target_pairs={{0,2},{1,3},{2,0},{3,1},{4,6},{5,7},{6,4},{7,5},{8,10},{9,11},{10,... | collective-permute-start | bytes 3342344 | tf_op jit(solution)/shard_map/ppermute | solution.py:282
  158.2 0.6 collective-permute-start.11
  158.7 1.5 collective-permute-start.7
  160.2 23.6 %collective-permute-done.9.refs_4_ = bf16[256,2176]{1,0:T(8,128)(2,1)S(1)} collective-permute-done((bf16[256,2176]{1,0:T(8,128)(2,1)}, bf16[256,2176]{1,0:T(8,128)(2,1)S(1)}, u32[]{:S(2)}, u32[]{:S(2)}) %collective-permute-start.9) | collective-permute-done | bytes 1114144 | tf_op jit(solution)/shard_map/ppermute | solution.py:282
  183.8 15.9 %collective-permute-done.11.refs_6_ = bf16[256,2176]{1,0:T(8,128)(2,1)S(1)} collective-permute-done((bf16[256,2176]{1,0:T(8,128)(2,1)}, bf16[256,2176]{1,0:T(8,128)(2,1)S(1)}, u32[]{:S(2)}, u32[]{:S(2)}) %collective-permute-start.11) | collective-permute-done | bytes 1114144 | tf_op jit(solution)/shard_map/ppermute | solution.py:282
  199.7 0.7 collective-permute-done.7.refs_2_
  200.5 3.5 %unpack.2 = (bf16[128,2048]{1,0:T(8,128)(2,1)}, bf16[128,2048]{1,0:T(8,128)(2,1)}, bf16[256,2048]{1,0:T(8,128)(2,1)}) custom-call(bf16[32,128,128]{2,1,0:T(8,128)(2,1)} %copy-done.4), custom_call_target="tpu_custom_call" | custom-call | flops 20971520 | bytes 3145728 | tf_op jit(solution)/shard_map/unpack/pallas_call | solution.py:159
  204.0 2.8 unpack.3
  206.8 8.6 %hidden.2.refs_0_ = bf16[2,2,256,256]{3,2,1,0:T(8,128)(2,1)} custom-call(s32[2]{0:T(128)} %pad_add_fusion.place_ref, bf16[256,2048]{1,0:T(8,128)(2,1)} %get-tuple-element.50.early_ref, bf16[256,2048]{1,0:T(8,128)(2,1)} %get-tuple-element.51.late_ref, bf16[256,2176]{1,0:T(8,128)(2,1)} %held.1.refs_0_, bf16[256,2176]{1,0:T(8,128)(2,1)} %collective-permute-done.6.refs_1_, ...), custom_call_target="tpu_custom_call" | custom-call | flops 2147483648 | bytes 4456448 | tf_op jit(solution)/shard_map/hidden/pallas_call | solution.py:205
  215.4 1.3 collective-permute-start.13
  216.8 2.4 collective-permute-start.14
  219.1 1.1 collective-permute-start.15
  220.3 4.6 %cast_down.1 = (bf16[4,256,512]{2,1,0:T(8,128)(2,1)}, bf16[224,512]{1,0:T(8,128)(2,1)}, bf16[224,512]{1,0:T(8,128)(2,1)}, bf16[224,512]{1,0:T(8,128)(2,1)}, bf16[224,512]{1,0:T(8,128)(2,1)}) custom-call(s32[2]{0:T(128)} %pad_add_fusion.place_ref, f32[4,224,512]{2,1,0:T(8,128)} %down_ref.1), custom_call_target="tpu_custom_call" | custom-call | flops 229376000 | bytes 3670016 | tf_op jit(solution)/shard_map/cast_down/pallas_call | solution.py:87
  224.8 8.6 %hidden.3.refs_0_ = bf16[2,2,256,256]{3,2,1,0:T(8,128)(2,1)} custom-call(s32[2]{0:T(128)} %pad_add_fusion.place_ref, bf16[256,2048]{1,0:T(8,128)(2,1)} %get-tuple-element.50.early_ref, bf16[256,2048]{1,0:T(8,128)(2,1)} %get-tuple-element.51.late_ref, bf16[256,2176]{1,0:T(8,128)(2,1)} %held.1.refs_0_, bf16[256,2176]{1,0:T(8,128)(2,1)} %collective-permute-done.6.refs_1_, ...), custom_call_target="tpu_custom_call" | custom-call | flops 2147483648 | bytes 4456448 | tf_op jit(solution)/shard_map/hidden/pallas_call | solution.py:205
  233.4 9.1 %collective-permute-done.14.refs_2_ = bf16[2,2,256,256]{3,2,1,0:T(8,128)(2,1)S(1)} collective-permute-done((bf16[2,2,256,256]{3,2,1,0:T(8,128)(2,1)}, bf16[2,2,256,256]{3,2,1,0:T(8,128)(2,1)S(1)}, u32[]{:S(2)}, u32[]{:S(2)}) %collective-permute-start.14) | collective-permute-done | bytes 524320 | tf_op jit(solution)/shard_map/ppermute | solution.py:282
  242.6 0.8 copy-done.17
  243.4 0.1 copy-done.18
  243.5 4.1 %down.2 = (f32[16,2,16,512]{3,2,1,0:T(8,128)}, bf16[16,2,16,512]{3,2,1,0:T(8,128)(2,1)}) custom-call(s32[2]{0:T(128)} %pad_add_fusion.place_ref, bf16[4,256,512]{2,1,0:T(8,128)(2,1)} %get-tuple-element.49.down_ref, bf16[2,2,256,256]{3,2,1,0:T(8,128)(2,1)} %hidden.2.refs_0_, bf16[2,2,256,256]{3,2,1,0:T(8,128)(2,1)} %copy-done.16, ...), custom_call_target="tpu_custom_call" | custom-call | flops 1073741824 | bytes 3670016 | tf_op jit(solution)/shard_map/down/pallas_call | solution.py:243
  247.7 2.1 collective-permute-done.16
  249.8 2.2 add_convert_fusion.1
  252.0 7.1 %all-to-all-start.3 = ((bf16[16,32,512]{2,1,0:T(8,128)(2,1)}), bf16[16,32,512]{2,1,0:T(8,128)(2,1)S(1)}, u32[]{:S(2)}, u32[]{:S(2)}) async-start(bf16[16,32,512]{2,1,0:T(8,128)(2,1)} %bitcast.14), calls=%async_computation.3 | async-start | bytes 1048576 | tf_op jit(solution)/shard_map/all_to_all | solution.py:353
  259.2 0.4 collective-permute-start.17
  259.6 3.8 %collective-permute-start.18 = (bf16[2,2,256,256]{3,2,1,0:T(8,128)(2,1)S(1)}, bf16[2,2,256,256]{3,2,1,0:T(8,128)(2,1)S(1)}, u32[]{:S(2)}, u32[]{:S(2)}) collective-permute-start(bf16[2,2,256,256]{3,2,1,0:T(8,128)(2,1)S(1)} %copy-done.7), channel_id=1, source_target_pairs={{0,2},{1,3},{2,0},{3,1},{4,6},{5,7},{6,4},{7,5},{8,10},{9,11},{10,... | collective-permute-start | bytes 1572872 | tf_op jit(solution)/shard_map/ppermute | solution.py:282
  263.4 11.1 %collective-permute-done.17.refs_1_ = bf16[2,2,256,256]{3,2,1,0:T(8,128)(2,1)S(1)} collective-permute-done((bf16[2,2,256,256]{3,2,1,0:T(8,128)(2,1)S(1)}, bf16[2,2,256,256]{3,2,1,0:T(8,128)(2,1)S(1)}, u32[]{:S(2)}, u32[]{:S(2)}) %collective-permute-start.17) | collective-permute-done | bytes 524320 | tf_op jit(solution)/shard_map/ppermute | solution.py:282
  274.5 11.8 %collective-permute-done.18.refs_2_ = bf16[2,2,256,256]{3,2,1,0:T(8,128)(2,1)S(1)} collective-permute-done((bf16[2,2,256,256]{3,2,1,0:T(8,128)(2,1)S(1)}, bf16[2,2,256,256]{3,2,1,0:T(8,128)(2,1)S(1)}, u32[]{:S(2)}, u32[]{:S(2)}) %collective-permute-start.18) | collective-permute-done | bytes 524320 | tf_op jit(solution)/shard_map/ppermute | solution.py:282
  286.3 0.8 copy-done.20
  287.1 0.8 copy-done.21
  287.9 4.1 %down.3 = (f32[16,2,16,512]{3,2,1,0:T(8,128)}, bf16[16,2,16,512]{3,2,1,0:T(8,128)(2,1)}) custom-call(s32[2]{0:T(128)} %pad_add_fusion.place_ref, bf16[4,256,512]{2,1,0:T(8,128)(2,1)} %get-tuple-element.49.down_ref, bf16[2,2,256,256]{3,2,1,0:T(8,128)(2,1)} %hidden.3.refs_0_, bf16[2,2,256,256]{3,2,1,0:T(8,128)(2,1)} %copy-done.19, ...), custom_call_target="tpu_custom_call" | custom-call | flops 1073741824 | bytes 3670016 | tf_op jit(solution)/shard_map/down/pallas_call | solution.py:243
  292.0 0.1 collective-permute-start.20
  292.1 2.1 collective-permute-done.20
  294.2 2.2 add_convert_fusion
  296.5 11.9 %all-to-all-start.4 = ((bf16[16,32,512]{2,1,0:T(8,128)(2,1)}), bf16[16,32,512]{2,1,0:T(8,128)(2,1)S(1)}, u32[]{:S(2)}, u32[]{:S(2)}) async-start(bf16[16,32,512]{2,1,0:T(8,128)(2,1)} %bitcast.15), calls=%async_computation.4 | async-start | bytes 1048576 | tf_op jit(solution)/shard_map/all_to_all | solution.py:353
  308.5 3.1 collective-permute-start.4
  311.6 0.3 collective-permute-start.5
  311.8 10.3 %collective-permute-done.3.refs_1_ = bf16[224,512]{1,0:T(8,128)(2,1)S(1)} collective-permute-done((bf16[224,512]{1,0:T(8,128)(2,1)}, bf16[224,512]{1,0:T(8,128)(2,1)S(1)}, u32[]{:S(2)}, u32[]{:S(2)}) %collective-permute-start.3) | collective-permute-done | bytes 229408 | tf_op jit(solution)/shard_map/ppermute | solution.py:290
  322.2 0.4 collective-permute-done.5.refs_3_
  322.6 0.3 copy-done.10
  323.0 0.3 copy-done.12
  323.3 3.5 %join.3 = bf16[224,2048]{1,0:T(8,128)(2,1)} custom-call(s32[2]{0:T(128)} %pad_add_fusion.place_ref, bf16[224,512]{1,0:T(8,128)(2,1)} %get-tuple-element.45.refs_0_, bf16[224,512]{1,0:T(8,128)(2,1)} %copy-done.10, bf16[224,512]{1,0:T(8,128)(2,1)} %copy-done.11, bf16[224,512]{1,0:T(8,128)(2,1)} %copy-done.12), custom_call_target="tpu_custom_call" | custom-call | flops 229376000 | bytes 1835008 | tf_op jit(solution)/shard_map/join/pallas_call | solution.py:123
  326.8 1.3 maximum_bitcast_fusion
  328.2 9.2 %all-to-all-done.4 = bf16[16,32,512]{2,1,0:T(8,128)(2,1)S(1)} async-done(((bf16[16,32,512]{2,1,0:T(8,128)(2,1)}), bf16[16,32,512]{2,1,0:T(8,128)(2,1)S(1)}, u32[]{:S(2)}, u32[]{:S(2)}) %all-to-all-start.4) | async-done | bytes 524320 | tf_op jit(solution)/shard_map/all_to_all | solution.py:353
  337.5 0.6 pad_maximum_fusion.1
  (72 shorter events, 1.1 us)
Async XLA Ops:
  7.2 0.7 copy-start
  18.7 45.6 %copy-start.26 = (bf16[8,96,128]{2,1,0:T(8,128)(2,1)S(1)}, bf16[8,96,128]{2,1,0:T(8,128)(2,1)}, u32[]{:S(2)}) copy-start(bf16[8,96,128]{2,1,0:T(8,128)(2,1)} %get-tuple-element.35) | copy-start | bytes 589828
  18.7 46.5 %copy-start.25 = (bf16[8,96,128]{2,1,0:T(8,128)(2,1)S(1)}, bf16[8,96,128]{2,1,0:T(8,128)(2,1)}, u32[]{:S(2)}) copy-start(bf16[8,96,128]{2,1,0:T(8,128)(2,1)} %get-tuple-element.36) | copy-start | bytes 589828
  18.7 48.3 %copy-start.24 = (bf16[8,96,128]{2,1,0:T(8,128)(2,1)S(1)}, bf16[8,96,128]{2,1,0:T(8,128)(2,1)}, u32[]{:S(2)}) copy-start(bf16[8,96,128]{2,1,0:T(8,128)(2,1)} %get-tuple-element.37) | copy-start | bytes 589828
  38.7 83.5 %all-to-all-start.1 = ((bf16[32,128,128]{2,1,0:T(8,128)(2,1)}), bf16[32,128,128]{2,1,0:T(8,128)(2,1)S(1)}, u32[]{:S(2)}, u32[]{:S(2)}) async-start(bf16[32,128,128]{2,1,0:T(8,128)(2,1)} %bitcast.8), calls=%async_computation.1 | async-start | bytes 2097152 | tf_op jit(solution)/shard_map/all_to_all | solution.py:324
  63.5 88.6 %all-gather.2.cloned.1.call-start = ((), (), s32[]{:S(2)}) async-start(), calls=%async_computation.5 | async-start | bytes 1183744 | tf_op jit(solution)/shard_map/all_gather | solution.py:320
  64.3 12.2 %collective-permute-start = (bf16[8,96,128]{2,1,0:T(8,128)(2,1)S(1)}, bf16[8,96,128]{2,1,0:T(8,128)(2,1)S(1)}, u32[]{:S(2)}, u32[]{:S(2)}) collective-permute-start(bf16[8,96,128]{2,1,0:T(8,128)(2,1)S(1)} %copy-done.26), channel_id=1, source_target_pairs={{0,1},{1,2},{2,3},{3,0},{4,5},{5,6},{6,7},{7,4},{8,9},{9,10},{10,1... | collective-permute-start | bytes 589832 | tf_op jit(solution)/shard_map/ppermute | solution.py:290
  65.2 11.3 %collective-permute-start.1 = (bf16[8,96,128]{2,1,0:T(8,128)(2,1)S(1)}, bf16[8,96,128]{2,1,0:T(8,128)(2,1)S(1)}, u32[]{:S(2)}, u32[]{:S(2)}) collective-permute-start(bf16[8,96,128]{2,1,0:T(8,128)(2,1)S(1)} %copy-done.25), channel_id=1, source_target_pairs={{0,2},{1,3},{2,0},{3,1},{4,6},{5,7},{6,4},{7,5},{8,10},{9,11},{10,... | collective-permute-start | bytes 589832 | tf_op jit(solution)/shard_map/ppermute | solution.py:290
  67.0 10.0 %collective-permute-start.2 = (bf16[8,96,128]{2,1,0:T(8,128)(2,1)S(1)}, bf16[8,96,128]{2,1,0:T(8,128)(2,1)S(1)}, u32[]{:S(2)}, u32[]{:S(2)}) collective-permute-start(bf16[8,96,128]{2,1,0:T(8,128)(2,1)S(1)} %copy-done.24), channel_id=1, source_target_pairs={{0,3},{1,0},{2,1},{3,2},{4,7},{5,4},{6,5},{7,6},{8,11},{9,8},{10,9... | collective-permute-start | bytes 589832 | tf_op jit(solution)/shard_map/ppermute | solution.py:290
  76.4 0.7 copy-start.13
  76.4 0.8 copy-start.14
  77.1 0.7 copy-start.15
  122.2 29.8 %copy-start.4 = (bf16[32,128,128]{2,1,0:T(8,128)(2,1)}, bf16[32,128,128]{2,1,0:T(8,128)(2,1)S(1)}, u32[]{:S(2)}) copy-start(bf16[32,128,128]{2,1,0:T(8,128)(2,1)S(1)} %all-to-all-done.1.recv_ref) | copy-start | bytes 3145732
  122.2 81.8 %all-to-all-start.2 = ((bf16[32,96,128]{2,1,0:T(8,128)(2,1)}), bf16[32,96,128]{2,1,0:T(8,128)(2,1)}, u32[]{:S(2)}, u32[]{:S(2)}) async-start(bf16[32,96,128]{2,1,0:T(8,128)(2,1)} %join.2), calls=%async_computation.2 | async-start | bytes 1572864 | tf_op jit(solution)/shard_map/all_to_all | solution.py:327
  154.4 29.4 %collective-permute-start.9 = (bf16[256,2176]{1,0:T(8,128)(2,1)}, bf16[256,2176]{1,0:T(8,128)(2,1)S(1)}, u32[]{:S(2)}, u32[]{:S(2)}) collective-permute-start(bf16[256,2176]{1,0:T(8,128)(2,1)} %held.1.refs_0_), channel_id=1, source_target_pairs={{0,2},{1,3},{2,0},{3,1},{4,6},{5,7},{6,4},{7,5},{8,10},{9,11},{10,... | collective-permute-start | bytes 3342344 | tf_op jit(solution)/shard_map/ppermute | solution.py:282
  158.2 41.6 %collective-permute-start.11 = (bf16[256,2176]{1,0:T(8,128)(2,1)}, bf16[256,2176]{1,0:T(8,128)(2,1)S(1)}, u32[]{:S(2)}, u32[]{:S(2)}) collective-permute-start(bf16[256,2176]{1,0:T(8,128)(2,1)} %held.1.refs_0_), channel_id=1, source_target_pairs={{0,3},{1,0},{2,1},{3,2},{4,7},{5,4},{6,5},{7,6},{8,11},{9,8},{10,9... | collective-permute-start | bytes 3342344 | tf_op jit(solution)/shard_map/ppermute | solution.py:282
  158.7 41.7 %collective-permute-start.7 = (bf16[256,2176]{1,0:T(8,128)(2,1)}, bf16[256,2176]{1,0:T(8,128)(2,1)S(1)}, u32[]{:S(2)}, u32[]{:S(2)}) collective-permute-start(bf16[256,2176]{1,0:T(8,128)(2,1)} %held.1.refs_0_), channel_id=1, source_target_pairs={{0,1},{1,2},{2,3},{3,0},{4,5},{5,6},{6,7},{7,4},{8,9},{9,10},{10,1... | collective-permute-start | bytes 3342344 | tf_op jit(solution)/shard_map/ppermute | solution.py:282
  160.2 46.6 %collective-permute-start.6 = (bf16[256,2176]{1,0:T(8,128)(2,1)}, bf16[256,2176]{1,0:T(8,128)(2,1)}, u32[]{:S(2)}, u32[]{:S(2)}) collective-permute-start(bf16[256,2176]{1,0:T(8,128)(2,1)} %held.1.refs_0_), channel_id=1, source_target_pairs={{0,4},{4,0},{8,12},{12,8},{16,20},{20,16},{24,28},{28,24},{32,36},... | collective-permute-start | bytes 3342344 | tf_op jit(solution)/shard_map/ppermute | solution.py:333
  183.8 23.0 %copy-start.1 = (bf16[256,2176]{1,0:T(8,128)(2,1)}, bf16[256,2176]{1,0:T(8,128)(2,1)S(1)}, u32[]{:S(2)}) copy-start(bf16[256,2176]{1,0:T(8,128)(2,1)S(1)} %collective-permute-done.9.refs_4_) | copy-start | bytes 3342340
  183.8 23.0 %collective-permute-start.10 = (bf16[256,2176]{1,0:T(8,128)(2,1)S(1)}, bf16[256,2176]{1,0:T(8,128)(2,1)}, u32[]{:S(2)}, u32[]{:S(2)}) collective-permute-start(bf16[256,2176]{1,0:T(8,128)(2,1)S(1)} %collective-permute-done.9.refs_4_), channel_id=1, source_target_pairs={{0,4},{4,0},{8,12},{12,8},{16,20},{20,16},{24,28},{28,24},{32,36},... | collective-permute-start | bytes 3342344 | tf_op jit(solution)/shard_map/ppermute | solution.py:333
  199.7 7.1 %copy-start.2 = (bf16[256,2176]{1,0:T(8,128)(2,1)}, bf16[256,2176]{1,0:T(8,128)(2,1)S(1)}, u32[]{:S(2)}) copy-start(bf16[256,2176]{1,0:T(8,128)(2,1)S(1)} %collective-permute-done.11.refs_6_) | copy-start | bytes 3342340
  199.7 7.1 %collective-permute-start.12 = (bf16[256,2176]{1,0:T(8,128)(2,1)S(1)}, bf16[256,2176]{1,0:T(8,128)(2,1)}, u32[]{:S(2)}, u32[]{:S(2)}) collective-permute-start(bf16[256,2176]{1,0:T(8,128)(2,1)S(1)} %collective-permute-done.11.refs_6_), channel_id=1, source_target_pairs={{0,4},{4,0},{8,12},{12,8},{16,20},{20,16},{24,28},{28,24},{32,36},... | collective-permute-start | bytes 3342344 | tf_op jit(solution)/shard_map/ppermute | solution.py:333
  200.4 6.4 %copy-start.3 = (bf16[256,2176]{1,0:T(8,128)(2,1)}, bf16[256,2176]{1,0:T(8,128)(2,1)S(1)}, u32[]{:S(2)}) copy-start(bf16[256,2176]{1,0:T(8,128)(2,1)S(1)} %collective-permute-done.7.refs_2_) | copy-start | bytes 3342340
  200.4 6.4 %collective-permute-start.8 = (bf16[256,2176]{1,0:T(8,128)(2,1)S(1)}, bf16[256,2176]{1,0:T(8,128)(2,1)}, u32[]{:S(2)}, u32[]{:S(2)}) collective-permute-start(bf16[256,2176]{1,0:T(8,128)(2,1)S(1)} %collective-permute-done.7.refs_2_), channel_id=1, source_target_pairs={{0,4},{4,0},{8,12},{12,8},{16,20},{20,16},{24,28},{28,24},{32,36},... | collective-permute-start | bytes 3342344 | tf_op jit(solution)/shard_map/ppermute | solution.py:333
  215.4 18.0 %collective-permute-start.13 = (bf16[2,2,256,256]{3,2,1,0:T(8,128)(2,1)}, bf16[2,2,256,256]{3,2,1,0:T(8,128)(2,1)S(1)}, u32[]{:S(2)}, u32[]{:S(2)}) collective-permute-start(bf16[2,2,256,256]{3,2,1,0:T(8,128)(2,1)} %hidden.2.refs_0_), channel_id=1, source_target_pairs={{0,1},{1,2},{2,3},{3,0},{4,5},{5,6},{6,7},{7,4},{8,9},{9,10},{10,1... | collective-permute-start | bytes 1572872 | tf_op jit(solution)/shard_map/ppermute | solution.py:282
  216.8 25.8 %collective-permute-start.14 = (bf16[2,2,256,256]{3,2,1,0:T(8,128)(2,1)}, bf16[2,2,256,256]{3,2,1,0:T(8,128)(2,1)S(1)}, u32[]{:S(2)}, u32[]{:S(2)}) collective-permute-start(bf16[2,2,256,256]{3,2,1,0:T(8,128)(2,1)} %hidden.2.refs_0_), channel_id=1, source_target_pairs={{0,2},{1,3},{2,0},{3,1},{4,6},{5,7},{6,4},{7,5},{8,10},{9,11},{10,... | collective-permute-start | bytes 1572872 | tf_op jit(solution)/shard_map/ppermute | solution.py:282
  219.1 23.5 %collective-permute-start.15 = (bf16[2,2,256,256]{3,2,1,0:T(8,128)(2,1)}, bf16[2,2,256,256]{3,2,1,0:T(8,128)(2,1)S(1)}, u32[]{:S(2)}, u32[]{:S(2)}) collective-permute-start(bf16[2,2,256,256]{3,2,1,0:T(8,128)(2,1)} %hidden.2.refs_0_), channel_id=1, source_target_pairs={{0,3},{1,0},{2,1},{3,2},{4,7},{5,4},{6,5},{7,6},{8,11},{9,8},{10,9... | collective-permute-start | bytes 1572872 | tf_op jit(solution)/shard_map/ppermute | solution.py:282
  233.4 9.2 %copy-start.16 = (bf16[2,2,256,256]{3,2,1,0:T(8,128)(2,1)}, bf16[2,2,256,256]{3,2,1,0:T(8,128)(2,1)S(1)}, u32[]{:S(2)}) copy-start(bf16[2,2,256,256]{3,2,1,0:T(8,128)(2,1)S(1)} %collective-permute-done.13.refs_1_) | copy-start | bytes 1572868
  242.5 0.8 copy-start.17
  242.6 0.9 copy-start.18
  247.6 11.6 %copy-start.7 = (bf16[2,2,256,256]{3,2,1,0:T(8,128)(2,1)S(1)}, bf16[2,2,256,256]{3,2,1,0:T(8,128)(2,1)}, u32[]{:S(2)}) copy-start(bf16[2,2,256,256]{3,2,1,0:T(8,128)(2,1)} %hidden.3.refs_0_) | copy-start | bytes 1572868
  247.6 2.2 collective-permute-start.16
  252.0 44.4 %all-to-all-start.3 = ((bf16[16,32,512]{2,1,0:T(8,128)(2,1)}), bf16[16,32,512]{2,1,0:T(8,128)(2,1)S(1)}, u32[]{:S(2)}, u32[]{:S(2)}) async-start(bf16[16,32,512]{2,1,0:T(8,128)(2,1)} %bitcast.14), calls=%async_computation.3 | async-start | bytes 1048576 | tf_op jit(solution)/shard_map/all_to_all | solution.py:353
  259.2 15.3 %collective-permute-start.17 = (bf16[2,2,256,256]{3,2,1,0:T(8,128)(2,1)S(1)}, bf16[2,2,256,256]{3,2,1,0:T(8,128)(2,1)S(1)}, u32[]{:S(2)}, u32[]{:S(2)}) collective-permute-start(bf16[2,2,256,256]{3,2,1,0:T(8,128)(2,1)S(1)} %copy-done.7), channel_id=1, source_target_pairs={{0,1},{1,2},{2,3},{3,0},{4,5},{5,6},{6,7},{7,4},{8,9},{9,10},{10,1... | collective-permute-start | bytes 1572872 | tf_op jit(solution)/shard_map/ppermute | solution.py:282
  259.6 26.7 %collective-permute-start.18 = (bf16[2,2,256,256]{3,2,1,0:T(8,128)(2,1)S(1)}, bf16[2,2,256,256]{3,2,1,0:T(8,128)(2,1)S(1)}, u32[]{:S(2)}, u32[]{:S(2)}) collective-permute-start(bf16[2,2,256,256]{3,2,1,0:T(8,128)(2,1)S(1)} %copy-done.7), channel_id=1, source_target_pairs={{0,2},{1,3},{2,0},{3,1},{4,6},{5,7},{6,4},{7,5},{8,10},{9,11},{10,... | collective-permute-start | bytes 1572872 | tf_op jit(solution)/shard_map/ppermute | solution.py:282
  263.4 22.9 %collective-permute-start.19 = (bf16[2,2,256,256]{3,2,1,0:T(8,128)(2,1)S(1)}, bf16[2,2,256,256]{3,2,1,0:T(8,128)(2,1)S(1)}, u32[]{:S(2)}, u32[]{:S(2)}) collective-permute-start(bf16[2,2,256,256]{3,2,1,0:T(8,128)(2,1)S(1)} %copy-done.7), channel_id=1, source_target_pairs={{0,3},{1,0},{2,1},{3,2},{4,7},{5,4},{6,5},{7,6},{8,11},{9,8},{10,9... | collective-permute-start | bytes 1572872 | tf_op jit(solution)/shard_map/ppermute | solution.py:282
  274.5 11.8 %copy-start.19 = (bf16[2,2,256,256]{3,2,1,0:T(8,128)(2,1)}, bf16[2,2,256,256]{3,2,1,0:T(8,128)(2,1)S(1)}, u32[]{:S(2)}) copy-start(bf16[2,2,256,256]{3,2,1,0:T(8,128)(2,1)S(1)} %collective-permute-done.17.refs_1_) | copy-start | bytes 1572868
  286.3 0.8 copy-start.20
  287.1 0.8 copy-start.21
  291.9 16.6 %copy-start.23 = (bf16[224,512]{1,0:T(8,128)(2,1)S(1)}, bf16[224,512]{1,0:T(8,128)(2,1)}, u32[]{:S(2)}) copy-start(bf16[224,512]{1,0:T(8,128)(2,1)} %get-tuple-element.47) | copy-start | bytes 688132
  291.9 19.6 %copy-start.22 = (bf16[224,512]{1,0:T(8,128)(2,1)S(1)}, bf16[224,512]{1,0:T(8,128)(2,1)}, u32[]{:S(2)}) copy-start(bf16[224,512]{1,0:T(8,128)(2,1)} %get-tuple-element.48) | copy-start | bytes 688132
  292.0 2.2 collective-permute-start.20
  296.4 30.3 %copy-start.5 = (bf16[128,2048]{1,0:T(8,128)(2,1)S(1)}, bf16[128,2048]{1,0:T(8,128)(2,1)}, u32[]{:S(2)}) copy-start(bf16[128,2048]{1,0:T(8,128)(2,1)} %get-tuple-element.40) | copy-start | bytes 1572868
  296.4 30.3 %copy-start.6 = (bf16[128,2048]{1,0:T(8,128)(2,1)S(1)}, bf16[128,2048]{1,0:T(8,128)(2,1)}, u32[]{:S(2)}) copy-start(bf16[128,2048]{1,0:T(8,128)(2,1)} %get-tuple-element.43) | copy-start | bytes 1572868
  296.4 30.3 %copy-start.8 = (bf16[96,2048]{1,0:T(8,128)(2,1)S(1)}, bf16[96,2048]{1,0:T(8,128)(2,1)}, u32[]{:S(2)}) copy-start(bf16[96,2048]{1,0:T(8,128)(2,1)} %get-tuple-element.42) | copy-start | bytes 1179652
  296.4 30.3 %copy-start.9 = (bf16[96,2048]{1,0:T(8,128)(2,1)S(1)}, bf16[96,2048]{1,0:T(8,128)(2,1)}, u32[]{:S(2)}) copy-start(bf16[96,2048]{1,0:T(8,128)(2,1)} %get-tuple-element.44) | copy-start | bytes 1179652
  296.5 40.9 %all-to-all-start.4 = ((bf16[16,32,512]{2,1,0:T(8,128)(2,1)}), bf16[16,32,512]{2,1,0:T(8,128)(2,1)S(1)}, u32[]{:S(2)}, u32[]{:S(2)}) async-start(bf16[16,32,512]{2,1,0:T(8,128)(2,1)} %bitcast.15), calls=%async_computation.4 | async-start | bytes 1048576 | tf_op jit(solution)/shard_map/all_to_all | solution.py:353
  308.4 13.8 %collective-permute-start.3 = (bf16[224,512]{1,0:T(8,128)(2,1)}, bf16[224,512]{1,0:T(8,128)(2,1)S(1)}, u32[]{:S(2)}, u32[]{:S(2)}) collective-permute-start(bf16[224,512]{1,0:T(8,128)(2,1)} %get-tuple-element.46), channel_id=1, source_target_pairs={{0,1},{1,2},{2,3},{3,0},{4,5},{5,6},{6,7},{7,4},{8,9},{9,10},{10,1... | collective-permute-start | bytes 688136 | tf_op jit(solution)/shard_map/ppermute | solution.py:290
  308.5 13.7 %collective-permute-start.4 = (bf16[224,512]{1,0:T(8,128)(2,1)S(1)}, bf16[224,512]{1,0:T(8,128)(2,1)S(1)}, u32[]{:S(2)}, u32[]{:S(2)}) collective-permute-start(bf16[224,512]{1,0:T(8,128)(2,1)S(1)} %copy-done.23), channel_id=1, source_target_pairs={{0,2},{1,3},{2,0},{3,1},{4,6},{5,7},{6,4},{7,5},{8,10},{9,11},{10,... | collective-permute-start | bytes 688136 | tf_op jit(solution)/shard_map/ppermute | solution.py:290
  311.6 11.0 %collective-permute-start.5 = (bf16[224,512]{1,0:T(8,128)(2,1)S(1)}, bf16[224,512]{1,0:T(8,128)(2,1)S(1)}, u32[]{:S(2)}, u32[]{:S(2)}) collective-permute-start(bf16[224,512]{1,0:T(8,128)(2,1)S(1)} %copy-done.22), channel_id=1, source_target_pairs={{0,3},{1,0},{2,1},{3,2},{4,7},{5,4},{6,5},{7,6},{8,11},{9,8},{10,9... | collective-permute-start | bytes 688136 | tf_op jit(solution)/shard_map/ppermute | solution.py:290
  322.2 0.7 copy-start.10
  322.2 0.8 copy-start.11
  322.6 0.7 copy-start.12
Sparse Core Ops, SparseCore 0:
  66.1 85.8 all-gather.1
where the time goes:
time: 346 us; the launch traced here: 345 us
  waiting for transfers between devices  171 us (49%)
  starting transfers between devices  71.8 us (21%)
  Pallas kernels  50.8 us (15%)
  blocking collectives  20 us (6%)
  between operations  14.3 us (4%)
  other arithmetic  11.2 us (3%)
  local copies, waits for them, and re-layouts  5.42 us (2%)
    ppermute x9, waiting for transfers between devices, around(): lax.ppermute(array, axis, [(i, (i + shift) % n) for i in range(n)])  72.3 us
    all_to_all x1, waiting for transfers between devices, body(): received = lax.all_to_all(across, 'fs', 0, 0, tiled=True)  41.1 us
    all_to_all x1, starting transfers between devices, body(): received = lax.all_to_all(across, 'fs', 0, 0, tiled=True)  24.7 us
    all_gather x1, waiting for transfers between devices, body(): lax.all_gather(rows, 'fs', axis=0, axis_index_groups=columns, tiled=True)  24.1 us
    all_to_all x1, blocking collectives, body(): lax.all_to_all(first_part, 'tp', 0, 0, tiled=True)  20 us
    ppermute x6, waiting for transfers between devices, dealt(): lax.ppermute(pieces[shift], axis, [(i, (i + shift) % n) for i in range(n)])  19.8 us
    all_to_all x2, starting transfers between devices, body(): lax.all_to_all(summed, 'fs', 0, 0, axis_index_groups=columns, tiled=True)  19 us
    pallas_call x2, Pallas kernels, hidden_of(): pl.pallas_call(functools.partial(hidden_kernel, depth, n_tp, first), grid...  17.1 us
  transfers between devices with their start and end apart: 26, of which 16 were waited for; matrix products, arithmetic and copies ran while one was open for 1% of the time, Pallas kernels for 9%

commit v1 on v0

--- a/solution.py
+++ b/solution.py
@@ -171,8 +171,8 @@
     )(recv)
 
 
-def hidden_kernel(depth, n_tp, first, place_ref, early_ref, late_ref, *refs):
-    token_refs, (out_ref, block_ref) = refs[:-2], refs[-2:]
+def hidden_kernel(depth, n_tp, first, n_parts, place_ref, *refs):
+    both_refs, token_refs, (out_ref, block_ref) = refs[:n_parts], refs[n_parts:-2], refs[-2:]
     quarter, core = pl.program_id(0) + first, pl.program_id(1)
     shift = lax.rem(place_ref[0] + n_tp - quarter, n_tp)
     other = jnp.where(core == place_ref[1], 0, 1)
@@ -187,7 +187,7 @@
     lane = lax.broadcasted_iota(jnp.int32, shares.shape, 1)
     share = jnp.sum(jnp.where(lane == place_ref[0], shares, 0.0), axis=1, keepdims=True)
     at = 0
-    for both_ref in (early_ref, late_ref):
+    for both_ref in both_refs:
         acts = lax.dot_general(tokens, both_ref[...], (((1,), (1,)), ((), ())), preferred_element_type=F32)
         half = acts.shape[1] // 2
         gate, up = acts[:, :half], acts[:, half:]
@@ -203,9 +203,9 @@
     work = count * 2 * rows
     vmem = pl.BlockSpec(memory_space=pltpu.VMEM)
     return pl.pallas_call(
-        functools.partial(hidden_kernel, depth, n_tp, first),
+        functools.partial(hidden_kernel, depth, n_tp, first, len(boths)),
         grid=(count, 2),
-        in_specs=[pl.BlockSpec(memory_space=pltpu.SMEM), vmem, vmem, *[vmem] * len(tokens)],
+        in_specs=[pl.BlockSpec(memory_space=pltpu.SMEM), *[vmem] * (len(boths) + len(tokens))],
         out_specs=pl.BlockSpec((1, 1, rows, half), lambda q, c: (q, c, 0, 0)),
         out_shape=jax.ShapeDtypeStruct((count, 2, rows, half), BF16),
         scratch_shapes=[pltpu.VMEM((rows, wide), BF16)],
@@ -218,11 +218,12 @@
 
 
 def down_kernel(place_ref, down_ref, *refs):
-    parts, (keep_ref, send_ref) = refs[:-2], refs[-2:]
-    experts = len(parts)
+    pieces, (keep_ref, send_ref) = refs[:-2], refs[-2:]
+    experts = down_ref.shape[0]
     total = None
-    for shift, part_ref in enumerate(parts):
-        left = part_ref[0].reshape(-1, part_ref.shape[3])
+    for shift in range(experts):
+        parts = [ref[0].reshape(-1, ref.shape[3]) for ref in pieces[shift::experts]]
+        left = jnp.concatenate(parts, axis=1) if len(parts) > 1 else parts[0]
         source = lax.rem(place_ref[0] + experts - shift, experts)
         term = jnp.dot(left, down_ref[source], preferred_element_type=F32)
         total = term if total is None else total + term
@@ -237,7 +238,7 @@
 
 def down_of(place, down, pieces, n_z):
     features = down.shape[2]
-    count, _, rows, width = pieces[0].shape
+    count, _, rows, _ = pieces[0].shape
     out = pl.BlockSpec((n_z, 1, rows // n_z, features), lambda q: (0, q, 0, 0))
     shape = (n_z, count, rows // n_z, features)
     return pl.pallas_call(
@@ -246,7 +247,7 @@
         in_specs=[
             pl.BlockSpec(memory_space=pltpu.SMEM),
             pl.BlockSpec(down.shape, lambda q: (0, 0, 0)),
-            *[pl.BlockSpec((1, 2, rows, width), lambda q: (q, 0, 0, 0))] * len(pieces),
+            *[pl.BlockSpec((1, 2, rows, piece.shape[3]), lambda q: (q, 0, 0, 0)) for piece in pieces],
         ],
         out_specs=[out, out],
         out_shape=[jax.ShapeDtypeStruct(shape, F32), jax.ShapeDtypeStruct(shape, BF16)],
@@ -333,18 +334,20 @@
         all_tokens += [piece, lax.ppermute(piece, "fs", swap)]
 
     down_padded, down_pieces = cast_down(place, w_down, len(parts) * LANES)
-    down_served = join(place, dealt(down_pieces, "tp"), 1)[None]
-
+    down_pieces = dealt(down_pieces, "tp")
+    down_served = join(place, down_pieces, 1)[None]
+
+    per = n_tp // chunks
     gate_a, up_a, both_a = unpack(received, LANES)
+    hidden = hidden_of(place, all_tokens, (both_a,), depth, 0, per)
+    gathered = [around(hidden, "tp")]
     gate_b, up_b, both_b = unpack(late_received, LANES)
     gates, ups = (gate_a, gate_b), (up_a, up_b)
-    per = n_tp // chunks
-    hiddens = [hidden_of(place, all_tokens, (both_a, both_b), depth, q * per, per) for q in range(chunks)]
-    gathered = []
-    for hidden in hiddens:
+    hidden = hidden_of(place, all_tokens, (both_b,), depth, 0, per)
+    gathered[0] = gathered[0] + around(hidden, "tp")
+    for q in range(1, chunks):
+        hidden = hidden_of(place, all_tokens, (both_a, both_b), depth, q * per, per)
         gathered.append(around(hidden, "tp"))
-    *gathered[0], hiddens[1] = lax.optimization_barrier((*gathered[0], hiddens[1]))
-    gathered[1][0] = hiddens[1]
     out = []
     for q in range(chunks):
         keep, send = down_of(place, down_padded, gathered[q], n_z)

time: 346 us -> 355 us (1.026)
  Pallas kernels: 50.8 us -> 56.5 us
    pallas_call x2 -> x3, Pallas kernels: 17.1 us -> 22.7 us  [hidden_of(): pl.pallas_call(functools.partial(hidden_kernel, depth, n_tp, first, len(b...]
    ppermute x9 -> x12, starting transfers between devices: 14.8 us -> 16.7 us  [around(): lax.ppermute(array, axis, [(i, (i + shift) % n) for i in range(n)])]
    ppermute x9 -> x12, waiting for transfers between devices: 72.3 us -> 73.6 us  [around(): lax.ppermute(array, axis, [(i, (i + shift) % n) for i in range(n)])]
  transfers between devices with their start and end apart: 26 -> 29, of which waited for: 16 -> 17; matrix products, arithmetic and copies ran while one was open for 1% -> 1% of each run, Pallas kernels for 9% -> 13%
where the time goes in v1:
time: 355 us; the launch traced here: 353 us
  waiting for transfers between devices  171 us (48%)
  starting transfers between devices  74.7 us (21%)
  Pallas kernels  56.5 us (16%)
  blocking collectives  20 us (6%)
  between operations  14.3 us (4%)
  other arithmetic  11.2 us (3%)
  local copies, waits for them, and re-layouts  5.75 us (2%)
    ppermute x12, waiting for transfers between devices, around(): lax.ppermute(array, axis, [(i, (i + shift) % n) for i in range(n)])  73.6 us
    all_to_all x1, waiting for transfers between devices, body(): received = lax.all_to_all(across, 'fs', 0, 0, tiled=True)  41 us
    all_to_all x1, starting transfers between devices, body(): received = lax.all_to_all(across, 'fs', 0, 0, tiled=True)  24.7 us
    all_gather x1, waiting for transfers between devices, body(): lax.all_gather(rows, 'fs', axis=0, axis_index_groups=columns, tiled=True)  23.4 us
    pallas_call x3, Pallas kernels, hidden_of(): pl.pallas_call(functools.partial(hidden_kernel, depth, n_tp, first, len(b...  22.7 us
    all_to_all x1, blocking collectives, body(): lax.all_to_all(first_part, 'tp', 0, 0, tiled=True)  20 us
    all_to_all x2, starting transfers between devices, body(): lax.all_to_all(summed, 'fs', 0, 0, axis_index_groups=columns, tiled=True)  18.9 us
    ppermute x6, waiting for transfers between devices, dealt(): lax.ppermute(pieces[shift], axis, [(i, (i + shift) % n) for i in range(n)])  18.8 us
  transfers between devices with their start and end apart: 29, of which 17 were waited for; matrix products, arithmetic and copies ran while one was open for 1% of the time, Pallas kernels for 13%

profile of v1, /device:TPU:40, one launch (start us, length us, event | category | flops | bytes accessed | tf_op | source)
XLA Modules:
  0.0 353.3 jit_solution(10332347744752792249)
XLA Ops:
  7.2 1.4 maximum_bitcast_fusion.2.scale_ref
  8.6 1.0 fusion
  9.6 0.8 constant_dynamic-slice_fusion
  10.4 0.9 fusion.1
  11.3 0.6 pad_add_fusion.place_ref
  12.0 0.6 pad_maximum_fusion
  12.6 5.4 %pack.1 = (bf16[4,8,128,128]{3,2,1,0:T(8,128)(2,1)}, bf16[8,96,128]{2,1,0:T(8,128)(2,1)}, bf16[8,96,128]{2,1,0:T(8,128)(2,1)}, bf16[8,96,128]{2,1,0:T(8,128)(2,1)}, bf16[8,96,128]{2,1,0:T(8,128)(2,1)}) custom-call(s32[2]{0:T(128)} %pad_add_fusion.place_ref, f32[1,128]{1,0:T(1,128)} %maximum_bitcast_fusion.2.scale_ref, f32[4,64,1792]{2,1,0:T(8,128)} %gate_ref.1, ...), custom_call_target="tpu_custom_call" | custom-call | flops 458752000 | bytes 5505024 | tf_op jit(solution)/shard_map/pack/pallas_call | solution.py:41
  18.1 20.0 %all_to_all.25 = bf16[4,1024,128]{2,1,0:T(8,128)(2,1)} all-to-all(bf16[4,1024,128]{2,1,0:T(8,128)(2,1)} %bitcast.25), channel_id=1, replica_groups=mesh['grp'=2,'fs'=32,'tp'=4] {'tp'}, dimensions={0} | all-to-all | bytes 2097152 | tf_op jit(solution)/shard_map/all_to_all | solution.py:324
  38.0 24.7 %all-to-all-start.1 = ((bf16[32,128,128]{2,1,0:T(8,128)(2,1)}), bf16[32,128,128]{2,1,0:T(8,128)(2,1)S(1)}, u32[]{:S(2)}, u32[]{:S(2)}) async-start(bf16[32,128,128]{2,1,0:T(8,128)(2,1)} %bitcast.8), calls=%async_computation.1 | async-start | bytes 2097152 | tf_op jit(solution)/shard_map/all_to_all | solution.py:325
  62.9 0.7 all-gather.2.cloned.1.call-update
  63.6 0.9 collective-permute-start
  64.5 1.9 collective-permute-start.1
  66.4 1.0 collective-permute-start.2
  67.4 8.4 %collective-permute-done.refs_1_ = bf16[8,96,128]{2,1,0:T(8,128)(2,1)S(1)} collective-permute-done((bf16[8,96,128]{2,1,0:T(8,128)(2,1)S(1)}, bf16[8,96,128]{2,1,0:T(8,128)(2,1)S(1)}, u32[]{:S(2)}, u32[]{:S(2)}) %collective-permute-start) | collective-permute-done | bytes 196640 | tf_op jit(solution)/shard_map/ppermute | solution.py:291
  75.8 0.6 collective-permute-done.2.refs_3_
  76.5 0.5 copy-done.18
  77.1 3.4 join.2
  80.5 41.0 %all-to-all-done.1.recv_ref = bf16[32,128,128]{2,1,0:T(8,128)(2,1)S(1)} async-done(((bf16[32,128,128]{2,1,0:T(8,128)(2,1)}), bf16[32,128,128]{2,1,0:T(8,128)(2,1)S(1)}, u32[]{:S(2)}, u32[]{:S(2)}) %all-to-all-start.1) | async-done | bytes 1048608 | tf_op jit(solution)/shard_map/all_to_all | solution.py:325
  121.5 5.8 %all-to-all-start.2 = ((bf16[32,96,128]{2,1,0:T(8,128)(2,1)}), bf16[32,96,128]{2,1,0:T(8,128)(2,1)}, u32[]{:S(2)}, u32[]{:S(2)}) async-start(bf16[32,96,128]{2,1,0:T(8,128)(2,1)} %join.2), calls=%async_computation.2 | async-start | bytes 1572864 | tf_op jit(solution)/shard_map/all_to_all | solution.py:328
  127.3 23.4 %all-gather.2.cloned.1.call-done.in_ref = bf16[256,2176]{1,0:T(8,128)(2,1)} async-done(((bf16[16,2176]{1,0:T(8,128)(2,1)}), bf16[256,2176]{1,0:T(8,128)(2,1)}) %all-gather.2.cloned.1.call-update) | async-done | bytes 1114128 | tf_op jit(solution)/shard_map/all_gather | solution.py:321
  150.7 2.4 held.1.refs_1_.refs_2_
  153.0 4.7 %collective-permute-start.11 = (bf16[256,2176]{1,0:T(8,128)(2,1)}, bf16[256,2176]{1,0:T(8,128)(2,1)S(1)}, u32[]{:S(2)}, u32[]{:S(2)}) collective-permute-start(bf16[256,2176]{1,0:T(8,128)(2,1)} %held.1.refs_1_.refs_2_), channel_id=1, source_target_pairs={{0,3},{1,0},{2,1},{3,2},{4,7},{5,4},{6,5},{7,6},{8,11},{9,8},{10,9... | collective-permute-start | bytes 3342344 | tf_op jit(solution)/shard_map/ppermute | solution.py:283
  157.8 1.3 collective-permute-start.7
  159.1 21.6 %collective-permute-done.11.refs_7_.refs_8_ = bf16[256,2176]{1,0:T(8,128)(2,1)S(1)} collective-permute-done((bf16[256,2176]{1,0:T(8,128)(2,1)}, bf16[256,2176]{1,0:T(8,128)(2,1)S(1)}, u32[]{:S(2)}, u32[]{:S(2)}) %collective-permute-start.11) | collective-permute-done | bytes 1114144 | tf_op jit(solution)/shard_map/ppermute | solution.py:283
  180.7 6.2 %collective-permute-done.9.refs_5_.refs_6_ = bf16[256,2176]{1,0:T(8,128)(2,1)S(1)} collective-permute-done((bf16[256,2176]{1,0:T(8,128)(2,1)}, bf16[256,2176]{1,0:T(8,128)(2,1)S(1)}, u32[]{:S(2)}, u32[]{:S(2)}) %collective-permute-start.9) | collective-permute-done | bytes 1114144 | tf_op jit(solution)/shard_map/ppermute | solution.py:283
  186.9 14.4 %collective-permute-done.7.refs_3_.refs_4_ = bf16[256,2176]{1,0:T(8,128)(2,1)S(1)} collective-permute-done((bf16[256,2176]{1,0:T(8,128)(2,1)}, bf16[256,2176]{1,0:T(8,128)(2,1)S(1)}, u32[]{:S(2)}, u32[]{:S(2)}) %collective-permute-start.7) | collective-permute-done | bytes 1114144 | tf_op jit(solution)/shard_map/ppermute | solution.py:283
  201.3 3.5 unpack.2
  205.0 0.9 copy-done.4
  206.9 7.0 %hidden.3.refs_0_ = bf16[2,2,256,128]{3,2,1,0:T(8,128)(2,1)} custom-call(s32[2]{0:T(128)} %pad_add_fusion.place_ref, bf16[256,2048]{1,0:T(8,128)(2,1)} %get-tuple-element.45.refs_0_, bf16[256,2176]{1,0:T(8,128)(2,1)} %held.1.refs_1_.refs_2_, bf16[256,2176]{1,0:T(8,128)(2,1)} %copy-done.4, bf16[256,2176]{1,0:T(8,128)(2,1)} %copy-done.3, ...), custom_call_target="tpu_custom_call" | custom-call | flops 1073741824 | bytes 4456448 | tf_op jit(solution)/shard_map/hidden/pallas_call | solution.py:205
  214.0 0.6 collective-permute-start.15
  214.6 1.3 collective-permute-start.14
  215.9 0.8 collective-permute-start.13
  216.7 2.9 unpack.3
  219.6 7.0 %hidden.4.refs_4_ = bf16[2,2,256,128]{3,2,1,0:T(8,128)(2,1)} custom-call(s32[2]{0:T(128)} %pad_add_fusion.place_ref, bf16[256,2048]{1,0:T(8,128)(2,1)} %get-tuple-element.47.refs_0_.refs_1_, bf16[256,2176]{1,0:T(8,128)(2,1)} %held.1.refs_1_.refs_2_, bf16[256,2176]{1,0:T(8,128)(2,1)} %copy-done.4, bf16[256,2176]{1,0:T(8,128)(2,1)} %copy-done.3, ...), custom_call_target="tpu_custom_call" | custom-call | flops 1073741824 | bytes 4456448 | tf_op jit(solution)/shard_map/hidden/pallas_call | solution.py:205
  226.6 2.4 collective-permute-start.18
  229.0 1.0 collective-permute-start.17
  230.0 1.4 collective-permute-start.16
  231.5 4.6 %cast_down.1 = (bf16[4,256,512]{2,1,0:T(8,128)(2,1)}, bf16[224,512]{1,0:T(8,128)(2,1)}, bf16[224,512]{1,0:T(8,128)(2,1)}, bf16[224,512]{1,0:T(8,128)(2,1)}, bf16[224,512]{1,0:T(8,128)(2,1)}) custom-call(s32[2]{0:T(128)} %pad_add_fusion.place_ref, f32[4,224,512]{2,1,0:T(8,128)} %down_ref.1), custom_call_target="tpu_custom_call" | custom-call | flops 229376000 | bytes 3670016 | tf_op jit(solution)/shard_map/cast_down/pallas_call | solution.py:87
  236.1 3.9 %collective-permute-done.18.refs_7_ = bf16[2,2,256,128]{3,2,1,0:T(8,128)(2,1)S(1)} collective-permute-done((bf16[2,2,256,128]{3,2,1,0:T(8,128)(2,1)}, bf16[2,2,256,128]{3,2,1,0:T(8,128)(2,1)S(1)}, u32[]{:S(2)}, u32[]{:S(2)}) %collective-permute-start.18) | collective-permute-done | bytes 262176 | tf_op jit(solution)/shard_map/ppermute | solution.py:283
  240.0 3.6 %collective-permute-done.16.refs_5_ = bf16[2,2,256,128]{3,2,1,0:T(8,128)(2,1)S(1)} collective-permute-done((bf16[2,2,256,128]{3,2,1,0:T(8,128)(2,1)}, bf16[2,2,256,128]{3,2,1,0:T(8,128)(2,1)S(1)}, u32[]{:S(2)}, u32[]{:S(2)}) %collective-permute-start.16) | collective-permute-done | bytes 262176 | tf_op jit(solution)/shard_map/ppermute | solution.py:283
  243.6 0.7 copy-done.27
  244.2 4.2 %down.2 = (f32[16,2,16,512]{3,2,1,0:T(8,128)}, bf16[16,2,16,512]{3,2,1,0:T(8,128)(2,1)}) custom-call(s32[2]{0:T(128)} %pad_add_fusion.place_ref, bf16[4,256,512]{2,1,0:T(8,128)(2,1)} %get-tuple-element.44.down_ref, bf16[2,2,256,128]{3,2,1,0:T(8,128)(2,1)} %hidden.3.refs_0_, bf16[2,2,256,128]{3,2,1,0:T(8,128)(2,1)} %copy-done.24, ...), custom_call_target="tpu_custom_call" | custom-call | flops 1073741824 | bytes 3670016 | tf_op jit(solution)/shard_map/down/pallas_call | solution.py:244
  248.5 2.1 collective-permute-done.19
  250.6 2.2 add_convert_fusion.1
  252.9 7.0 %all-to-all-start.3 = ((bf16[16,32,512]{2,1,0:T(8,128)(2,1)}), bf16[16,32,512]{2,1,0:T(8,128)(2,1)S(1)}, u32[]{:S(2)}, u32[]{:S(2)}) async-start(bf16[16,32,512]{2,1,0:T(8,128)(2,1)} %bitcast.14), calls=%async_computation.3 | async-start | bytes 1048576 | tf_op jit(solution)/shard_map/all_to_all | solution.py:356
  259.9 8.6 %hidden.5.refs_0_ = bf16[2,2,256,256]{3,2,1,0:T(8,128)(2,1)} custom-call(s32[2]{0:T(128)} %pad_add_fusion.place_ref, bf16[256,2048]{1,0:T(8,128)(2,1)} %get-tuple-element.45.refs_0_, bf16[256,2048]{1,0:T(8,128)(2,1)} %get-tuple-element.47.refs_0_.refs_1_, bf16[256,2176]{1,0:T(8,128)(2,1)} %held.1.refs_1_.refs_2_, bf16[256,2176]{1,0:T(8,128)(2,1)} %copy-done.4, ...), custom_call_target="tpu_custom_call" | custom-call | flops 2147483648 | bytes 4456448 | tf_op jit(solution)/shard_map/hidden/pallas_call | solution.py:205
  268.5 0.6 collective-permute-start.22
  269.1 1.6 collective-permute-start.21
  270.7 0.8 collective-permute-start.20
  271.5 11.9 %collective-permute-done.22.refs_3_ = bf16[2,2,256,256]{3,2,1,0:T(8,128)(2,1)S(1)} collective-permute-done((bf16[2,2,256,256]{3,2,1,0:T(8,128)(2,1)}, bf16[2,2,256,256]{3,2,1,0:T(8,128)(2,1)S(1)}, u32[]{:S(2)}, u32[]{:S(2)}) %collective-permute-start.22) | collective-permute-done | bytes 524320 | tf_op jit(solution)/shard_map/ppermute | solution.py:283
  283.5 2.2 collective-permute-done.21.refs_2_
  285.7 9.8 %collective-permute-done.20.refs_1_ = bf16[2,2,256,256]{3,2,1,0:T(8,128)(2,1)S(1)} collective-permute-done((bf16[2,2,256,256]{3,2,1,0:T(8,128)(2,1)}, bf16[2,2,256,256]{3,2,1,0:T(8,128)(2,1)S(1)}, u32[]{:S(2)}, u32[]{:S(2)}) %collective-permute-start.20) | collective-permute-done | bytes 524320 | tf_op jit(solution)/shard_map/ppermute | solution.py:283
  295.5 0.8 copy-done.21
  296.3 4.1 %down.3 = (f32[16,2,16,512]{3,2,1,0:T(8,128)}, bf16[16,2,16,512]{3,2,1,0:T(8,128)(2,1)}) custom-call(s32[2]{0:T(128)} %pad_add_fusion.place_ref, bf16[4,256,512]{2,1,0:T(8,128)(2,1)} %get-tuple-element.44.down_ref, bf16[2,2,256,256]{3,2,1,0:T(8,128)(2,1)} %hidden.5.refs_0_, bf16[2,2,256,256]{3,2,1,0:T(8,128)(2,1)} %copy-done.21, ...), custom_call_target="tpu_custom_call" | custom-call | flops 1073741824 | bytes 3670016 | tf_op jit(solution)/shard_map/down/pallas_call | solution.py:244
  300.5 2.1 collective-permute-done.23
  302.6 2.2 add_convert_fusion
  304.9 11.9 %all-to-all-start.4 = ((bf16[16,32,512]{2,1,0:T(8,128)(2,1)}), bf16[16,32,512]{2,1,0:T(8,128)(2,1)S(1)}, u32[]{:S(2)}, u32[]{:S(2)}) async-start(bf16[16,32,512]{2,1,0:T(8,128)(2,1)} %bitcast.15), calls=%async_computation.4 | async-start | bytes 1048576 | tf_op jit(solution)/shard_map/all_to_all | solution.py:356
  317.1 2.9 collective-permute-start.4
  319.9 1.2 collective-permute-start.5
  321.1 9.4 %collective-permute-done.3.refs_1_ = bf16[224,512]{1,0:T(8,128)(2,1)S(1)} collective-permute-done((bf16[224,512]{1,0:T(8,128)(2,1)}, bf16[224,512]{1,0:T(8,128)(2,1)S(1)}, u32[]{:S(2)}, u32[]{:S(2)}) %collective-permute-start.3) | collective-permute-done | bytes 229408 | tf_op jit(solution)/shard_map/ppermute | solution.py:291
  331.7 3.5 join.3
  335.2 1.3 maximum_bitcast_fusion
  336.6 9.2 %all-to-all-done.4 = bf16[16,32,512]{2,1,0:T(8,128)(2,1)S(1)} async-done(((bf16[16,32,512]{2,1,0:T(8,128)(2,1)}), bf16[16,32,512]{2,1,0:T(8,128)(2,1)S(1)}, u32[]{:S(2)}, u32[]{:S(2)}) %all-to-all-start.4) | async-done | bytes 524320 | tf_op jit(solution)/shard_map/all_to_all | solution.py:356
  345.9 0.6 pad_maximum_fusion.1
  (91 shorter events, 3.4 us)
Async XLA Ops:
  7.2 2.4 copy-start
  18.0 45.6 %copy-start.32 = (bf16[8,96,128]{2,1,0:T(8,128)(2,1)S(1)}, bf16[8,96,128]{2,1,0:T(8,128)(2,1)}, u32[]{:S(2)}) copy-start(bf16[8,96,128]{2,1,0:T(8,128)(2,1)} %get-tuple-element.30) | copy-start | bytes 589828
  18.0 46.4 %copy-start.31 = (bf16[8,96,128]{2,1,0:T(8,128)(2,1)S(1)}, bf16[8,96,128]{2,1,0:T(8,128)(2,1)}, u32[]{:S(2)}) copy-start(bf16[8,96,128]{2,1,0:T(8,128)(2,1)} %get-tuple-element.31) | copy-start | bytes 589828
  18.1 48.3 %copy-start.30 = (bf16[8,96,128]{2,1,0:T(8,128)(2,1)S(1)}, bf16[8,96,128]{2,1,0:T(8,128)(2,1)}, u32[]{:S(2)}) copy-start(bf16[8,96,128]{2,1,0:T(8,128)(2,1)} %get-tuple-element.32) | copy-start | bytes 589828
  38.0 83.4 %all-to-all-start.1 = ((bf16[32,128,128]{2,1,0:T(8,128)(2,1)}), bf16[32,128,128]{2,1,0:T(8,128)(2,1)S(1)}, u32[]{:S(2)}, u32[]{:S(2)}) async-start(bf16[32,128,128]{2,1,0:T(8,128)(2,1)} %bitcast.8), calls=%async_computation.1 | async-start | bytes 2097152 | tf_op jit(solution)/shard_map/all_to_all | solution.py:325
  62.8 87.9 %all-gather.2.cloned.1.call-start = ((), (), s32[]{:S(2)}) async-start(), calls=%async_computation.5 | async-start | bytes 1183744 | tf_op jit(solution)/shard_map/all_gather | solution.py:321
  63.6 12.2 %collective-permute-start = (bf16[8,96,128]{2,1,0:T(8,128)(2,1)S(1)}, bf16[8,96,128]{2,1,0:T(8,128)(2,1)S(1)}, u32[]{:S(2)}, u32[]{:S(2)}) collective-permute-start(bf16[8,96,128]{2,1,0:T(8,128)(2,1)S(1)} %copy-done.32), channel_id=1, source_target_pairs={{0,1},{1,2},{2,3},{3,0},{4,5},{5,6},{6,7},{7,4},{8,9},{9,10},{10,1... | collective-permute-start | bytes 589832 | tf_op jit(solution)/shard_map/ppermute | solution.py:291
  64.5 11.3 %collective-permute-start.1 = (bf16[8,96,128]{2,1,0:T(8,128)(2,1)S(1)}, bf16[8,96,128]{2,1,0:T(8,128)(2,1)S(1)}, u32[]{:S(2)}, u32[]{:S(2)}) collective-permute-start(bf16[8,96,128]{2,1,0:T(8,128)(2,1)S(1)} %copy-done.31), channel_id=1, source_target_pairs={{0,2},{1,3},{2,0},{3,1},{4,6},{5,7},{6,4},{7,5},{8,10},{9,11},{10,... | collective-permute-start | bytes 589832 | tf_op jit(solution)/shard_map/ppermute | solution.py:291
  66.4 10.0 %collective-permute-start.2 = (bf16[8,96,128]{2,1,0:T(8,128)(2,1)S(1)}, bf16[8,96,128]{2,1,0:T(8,128)(2,1)S(1)}, u32[]{:S(2)}, u32[]{:S(2)}) collective-permute-start(bf16[8,96,128]{2,1,0:T(8,128)(2,1)S(1)} %copy-done.30), channel_id=1, source_target_pairs={{0,3},{1,0},{2,1},{3,2},{4,7},{5,4},{6,5},{7,6},{8,11},{9,8},{10,9... | collective-permute-start | bytes 589832 | tf_op jit(solution)/shard_map/ppermute | solution.py:291
  75.8 0.7 copy-start.16
  75.8 0.7 copy-start.17
  76.4 0.7 copy-start.18
  121.5 29.2 %copy-start.8 = (bf16[32,128,128]{2,1,0:T(8,128)(2,1)}, bf16[32,128,128]{2,1,0:T(8,128)(2,1)S(1)}, u32[]{:S(2)}) copy-start(bf16[32,128,128]{2,1,0:T(8,128)(2,1)S(1)} %all-to-all-done.1.recv_ref) | copy-start | bytes 3145732
  121.5 95.2 %all-to-all-start.2 = ((bf16[32,96,128]{2,1,0:T(8,128)(2,1)}), bf16[32,96,128]{2,1,0:T(8,128)(2,1)}, u32[]{:S(2)}, u32[]{:S(2)}) async-start(bf16[32,96,128]{2,1,0:T(8,128)(2,1)} %join.2), calls=%async_computation.2 | async-start | bytes 1572864 | tf_op jit(solution)/shard_map/all_to_all | solution.py:328
  153.0 27.6 %collective-permute-start.11 = (bf16[256,2176]{1,0:T(8,128)(2,1)}, bf16[256,2176]{1,0:T(8,128)(2,1)S(1)}, u32[]{:S(2)}, u32[]{:S(2)}) collective-permute-start(bf16[256,2176]{1,0:T(8,128)(2,1)} %held.1.refs_1_.refs_2_), channel_id=1, source_target_pairs={{0,3},{1,0},{2,1},{3,2},{4,7},{5,4},{6,5},{7,6},{8,11},{9,8},{10,9... | collective-permute-start | bytes 3342344 | tf_op jit(solution)/shard_map/ppermute | solution.py:283
  157.8 29.2 %collective-permute-start.9 = (bf16[256,2176]{1,0:T(8,128)(2,1)}, bf16[256,2176]{1,0:T(8,128)(2,1)S(1)}, u32[]{:S(2)}, u32[]{:S(2)}) collective-permute-start(bf16[256,2176]{1,0:T(8,128)(2,1)} %held.1.refs_1_.refs_2_), channel_id=1, source_target_pairs={{0,2},{1,3},{2,0},{3,1},{4,6},{5,7},{6,4},{7,5},{8,10},{9,11},{10,... | collective-permute-start | bytes 3342344 | tf_op jit(solution)/shard_map/ppermute | solution.py:283
  157.8 43.6 %collective-permute-start.7 = (bf16[256,2176]{1,0:T(8,128)(2,1)}, bf16[256,2176]{1,0:T(8,128)(2,1)S(1)}, u32[]{:S(2)}, u32[]{:S(2)}) collective-permute-start(bf16[256,2176]{1,0:T(8,128)(2,1)} %held.1.refs_1_.refs_2_), channel_id=1, source_target_pairs={{0,1},{1,2},{2,3},{3,0},{4,5},{5,6},{6,7},{7,4},{8,9},{9,10},{10,1... | collective-permute-start | bytes 3342344 | tf_op jit(solution)/shard_map/ppermute | solution.py:283
  159.1 45.8 %collective-permute-start.6 = (bf16[256,2176]{1,0:T(8,128)(2,1)}, bf16[256,2176]{1,0:T(8,128)(2,1)S(1)}, u32[]{:S(2)}, u32[]{:S(2)}) collective-permute-start(bf16[256,2176]{1,0:T(8,128)(2,1)} %held.1.refs_1_.refs_2_), channel_id=1, source_target_pairs={{0,4},{4,0},{8,12},{12,8},{16,20},{20,16},{24,28},{28,24},{32,36},... | collective-permute-start | bytes 3342344 | tf_op jit(solution)/shard_map/ppermute | solution.py:334
  180.7 24.3 %copy-start.1 = (bf16[256,2176]{1,0:T(8,128)(2,1)}, bf16[256,2176]{1,0:T(8,128)(2,1)S(1)}, u32[]{:S(2)}) copy-start(bf16[256,2176]{1,0:T(8,128)(2,1)S(1)} %collective-permute-done.11.refs_7_.refs_8_) | copy-start | bytes 3342340
  180.7 24.2 %collective-permute-start.12 = (bf16[256,2176]{1,0:T(8,128)(2,1)S(1)}, bf16[256,2176]{1,0:T(8,128)(2,1)S(1)}, u32[]{:S(2)}, u32[]{:S(2)}) collective-permute-start(bf16[256,2176]{1,0:T(8,128)(2,1)S(1)} %collective-permute-done.11.refs_7_.refs_8_), channel_id=1, source_target_pairs={{0,4},{4,0},{8,12},{12,8},{16,20},{20,16},{24,28},{28,24},{32,36},... | collective-permute-start | bytes 3342344 | tf_op jit(solution)/shard_map/ppermute | solution.py:334
  186.9 18.0 %copy-start.2 = (bf16[256,2176]{1,0:T(8,128)(2,1)}, bf16[256,2176]{1,0:T(8,128)(2,1)S(1)}, u32[]{:S(2)}) copy-start(bf16[256,2176]{1,0:T(8,128)(2,1)S(1)} %collective-permute-done.9.refs_5_.refs_6_) | copy-start | bytes 3342340
  186.9 18.0 %collective-permute-start.10 = (bf16[256,2176]{1,0:T(8,128)(2,1)S(1)}, bf16[256,2176]{1,0:T(8,128)(2,1)S(1)}, u32[]{:S(2)}, u32[]{:S(2)}) collective-permute-start(bf16[256,2176]{1,0:T(8,128)(2,1)S(1)} %collective-permute-done.9.refs_5_.refs_6_), channel_id=1, source_target_pairs={{0,4},{4,0},{8,12},{12,8},{16,20},{20,16},{24,28},{28,24},{32,36},... | collective-permute-start | bytes 3342344 | tf_op jit(solution)/shard_map/ppermute | solution.py:334
  201.3 3.6 %copy-start.3 = (bf16[256,2176]{1,0:T(8,128)(2,1)}, bf16[256,2176]{1,0:T(8,128)(2,1)S(1)}, u32[]{:S(2)}) copy-start(bf16[256,2176]{1,0:T(8,128)(2,1)S(1)} %collective-permute-done.7.refs_3_.refs_4_) | copy-start | bytes 3342340
  201.3 3.6 %collective-permute-start.8 = (bf16[256,2176]{1,0:T(8,128)(2,1)S(1)}, bf16[256,2176]{1,0:T(8,128)(2,1)S(1)}, u32[]{:S(2)}, u32[]{:S(2)}) collective-permute-start(bf16[256,2176]{1,0:T(8,128)(2,1)S(1)} %collective-permute-done.7.refs_3_.refs_4_), channel_id=1, source_target_pairs={{0,4},{4,0},{8,12},{12,8},{16,20},{20,16},{24,28},{28,24},{32,36},... | collective-permute-start | bytes 3342344 | tf_op jit(solution)/shard_map/ppermute | solution.py:334
  204.9 1.0 copy-start.4
  204.9 1.4 copy-start.5
  204.9 1.7 copy-start.6
  204.9 2.0 copy-start.7
  214.0 16.1 %collective-permute-start.15 = (bf16[2,2,256,128]{3,2,1,0:T(8,128)(2,1)}, bf16[2,2,256,128]{3,2,1,0:T(8,128)(2,1)S(1)}, u32[]{:S(2)}, u32[]{:S(2)}) collective-permute-start(bf16[2,2,256,128]{3,2,1,0:T(8,128)(2,1)} %hidden.3.refs_0_), channel_id=1, source_target_pairs={{0,3},{1,0},{2,1},{3,2},{4,7},{5,4},{6,5},{7,6},{8,11},{9,8},{10,9... | collective-permute-start | bytes 786440 | tf_op jit(solution)/shard_map/ppermute | solution.py:283
  214.6 21.5 %collective-permute-start.14 = (bf16[2,2,256,128]{3,2,1,0:T(8,128)(2,1)}, bf16[2,2,256,128]{3,2,1,0:T(8,128)(2,1)S(1)}, u32[]{:S(2)}, u32[]{:S(2)}) collective-permute-start(bf16[2,2,256,128]{3,2,1,0:T(8,128)(2,1)} %hidden.3.refs_0_), channel_id=1, source_target_pairs={{0,2},{1,3},{2,0},{3,1},{4,6},{5,7},{6,4},{7,5},{8,10},{9,11},{10,... | collective-permute-start | bytes 786440 | tf_op jit(solution)/shard_map/ppermute | solution.py:283
  215.9 20.2 %collective-permute-start.13 = (bf16[2,2,256,128]{3,2,1,0:T(8,128)(2,1)}, bf16[2,2,256,128]{3,2,1,0:T(8,128)(2,1)S(1)}, u32[]{:S(2)}, u32[]{:S(2)}) collective-permute-start(bf16[2,2,256,128]{3,2,1,0:T(8,128)(2,1)} %hidden.3.refs_0_), channel_id=1, source_target_pairs={{0,1},{1,2},{2,3},{3,0},{4,5},{5,6},{6,7},{7,4},{8,9},{9,10},{10,1... | collective-permute-start | bytes 786440 | tf_op jit(solution)/shard_map/ppermute | solution.py:283
  226.6 13.4 %collective-permute-start.18 = (bf16[2,2,256,128]{3,2,1,0:T(8,128)(2,1)}, bf16[2,2,256,128]{3,2,1,0:T(8,128)(2,1)S(1)}, u32[]{:S(2)}, u32[]{:S(2)}) collective-permute-start(bf16[2,2,256,128]{3,2,1,0:T(8,128)(2,1)} %hidden.4.refs_4_), channel_id=1, source_target_pairs={{0,3},{1,0},{2,1},{3,2},{4,7},{5,4},{6,5},{7,6},{8,11},{9,8},{10,9... | collective-permute-start | bytes 786440 | tf_op jit(solution)/shard_map/ppermute | solution.py:283
  229.0 11.0 %collective-permute-start.17 = (bf16[2,2,256,128]{3,2,1,0:T(8,128)(2,1)}, bf16[2,2,256,128]{3,2,1,0:T(8,128)(2,1)S(1)}, u32[]{:S(2)}, u32[]{:S(2)}) collective-permute-start(bf16[2,2,256,128]{3,2,1,0:T(8,128)(2,1)} %hidden.4.refs_4_), channel_id=1, source_target_pairs={{0,2},{1,3},{2,0},{3,1},{4,6},{5,7},{6,4},{7,5},{8,10},{9,11},{10,... | collective-permute-start | bytes 786440 | tf_op jit(solution)/shard_map/ppermute | solution.py:283
  230.0 13.5 %copy-start.22 = (bf16[2,2,256,128]{3,2,1,0:T(8,128)(2,1)}, bf16[2,2,256,128]{3,2,1,0:T(8,128)(2,1)S(1)}, u32[]{:S(2)}) copy-start(bf16[2,2,256,128]{3,2,1,0:T(8,128)(2,1)S(1)} %collective-permute-done.15.refs_3_) | copy-start | bytes 786436
  230.0 13.5 %collective-permute-start.16 = (bf16[2,2,256,128]{3,2,1,0:T(8,128)(2,1)}, bf16[2,2,256,128]{3,2,1,0:T(8,128)(2,1)S(1)}, u32[]{:S(2)}, u32[]{:S(2)}) collective-permute-start(bf16[2,2,256,128]{3,2,1,0:T(8,128)(2,1)} %hidden.4.refs_4_), channel_id=1, source_target_pairs={{0,1},{1,2},{2,3},{3,0},{4,5},{5,6},{6,7},{7,4},{8,9},{9,10},{10,1... | collective-permute-start | bytes 786440 | tf_op jit(solution)/shard_map/ppermute | solution.py:283
  236.0 7.5 %copy-start.23 = (bf16[2,2,256,128]{3,2,1,0:T(8,128)(2,1)}, bf16[2,2,256,128]{3,2,1,0:T(8,128)(2,1)S(1)}, u32[]{:S(2)}) copy-start(bf16[2,2,256,128]{3,2,1,0:T(8,128)(2,1)S(1)} %collective-permute-done.14.refs_2_) | copy-start | bytes 786436
  236.1 7.5 %copy-start.24 = (bf16[2,2,256,128]{3,2,1,0:T(8,128)(2,1)}, bf16[2,2,256,128]{3,2,1,0:T(8,128)(2,1)S(1)}, u32[]{:S(2)}) copy-start(bf16[2,2,256,128]{3,2,1,0:T(8,128)(2,1)S(1)} %collective-permute-done.13.refs_1_) | copy-start | bytes 786436
  240.0 3.6 %copy-start.25 = (bf16[2,2,256,128]{3,2,1,0:T(8,128)(2,1)}, bf16[2,2,256,128]{3,2,1,0:T(8,128)(2,1)S(1)}, u32[]{:S(2)}) copy-start(bf16[2,2,256,128]{3,2,1,0:T(8,128)(2,1)S(1)} %collective-permute-done.18.refs_7_) | copy-start | bytes 786436
  240.0 3.6 %copy-start.26 = (bf16[2,2,256,128]{3,2,1,0:T(8,128)(2,1)}, bf16[2,2,256,128]{3,2,1,0:T(8,128)(2,1)S(1)}, u32[]{:S(2)}) copy-start(bf16[2,2,256,128]{3,2,1,0:T(8,128)(2,1)S(1)} %collective-permute-done.17.refs_6_) | copy-start | bytes 786436
  243.5 0.7 copy-start.27
  248.4 2.2 collective-permute-start.19
  252.9 52.0 %all-to-all-start.3 = ((bf16[16,32,512]{2,1,0:T(8,128)(2,1)}), bf16[16,32,512]{2,1,0:T(8,128)(2,1)S(1)}, u32[]{:S(2)}, u32[]{:S(2)}) async-start(bf16[16,32,512]{2,1,0:T(8,128)(2,1)} %bitcast.14), calls=%async_computation.3 | async-start | bytes 1048576 | tf_op jit(solution)/shard_map/all_to_all | solution.py:356
  268.5 15.0 %collective-permute-start.22 = (bf16[2,2,256,256]{3,2,1,0:T(8,128)(2,1)}, bf16[2,2,256,256]{3,2,1,0:T(8,128)(2,1)S(1)}, u32[]{:S(2)}, u32[]{:S(2)}) collective-permute-start(bf16[2,2,256,256]{3,2,1,0:T(8,128)(2,1)} %hidden.5.refs_0_), channel_id=1, source_target_pairs={{0,3},{1,0},{2,1},{3,2},{4,7},{5,4},{6,5},{7,6},{8,11},{9,8},{10,9... | collective-permute-start | bytes 1572872 | tf_op jit(solution)/shard_map/ppermute | solution.py:283
  269.1 16.6 %collective-permute-start.21 = (bf16[2,2,256,256]{3,2,1,0:T(8,128)(2,1)}, bf16[2,2,256,256]{3,2,1,0:T(8,128)(2,1)S(1)}, u32[]{:S(2)}, u32[]{:S(2)}) collective-permute-start(bf16[2,2,256,256]{3,2,1,0:T(8,128)(2,1)} %hidden.5.refs_0_), channel_id=1, source_target_pairs={{0,2},{1,3},{2,0},{3,1},{4,6},{5,7},{6,4},{7,5},{8,10},{9,11},{10,... | collective-permute-start | bytes 1572872 | tf_op jit(solution)/shard_map/ppermute | solution.py:283
  270.7 24.7 %collective-permute-start.20 = (bf16[2,2,256,256]{3,2,1,0:T(8,128)(2,1)}, bf16[2,2,256,256]{3,2,1,0:T(8,128)(2,1)S(1)}, u32[]{:S(2)}, u32[]{:S(2)}) collective-permute-start(bf16[2,2,256,256]{3,2,1,0:T(8,128)(2,1)} %hidden.5.refs_0_), channel_id=1, source_target_pairs={{0,1},{1,2},{2,3},{3,0},{4,5},{5,6},{6,7},{7,4},{8,9},{9,10},{10,1... | collective-permute-start | bytes 1572872 | tf_op jit(solution)/shard_map/ppermute | solution.py:283
  283.5 12.0 %copy-start.19 = (bf16[2,2,256,256]{3,2,1,0:T(8,128)(2,1)}, bf16[2,2,256,256]{3,2,1,0:T(8,128)(2,1)S(1)}, u32[]{:S(2)}) copy-start(bf16[2,2,256,256]{3,2,1,0:T(8,128)(2,1)S(1)} %collective-permute-done.22.refs_3_) | copy-start | bytes 1572868
  285.7 9.8 %copy-start.20 = (bf16[2,2,256,256]{3,2,1,0:T(8,128)(2,1)}, bf16[2,2,256,256]{3,2,1,0:T(8,128)(2,1)S(1)}, u32[]{:S(2)}) copy-start(bf16[2,2,256,256]{3,2,1,0:T(8,128)(2,1)S(1)} %collective-permute-done.21.refs_2_) | copy-start | bytes 1572868
  295.5 0.8 copy-start.21
  300.4 16.7 %copy-start.29 = (bf16[224,512]{1,0:T(8,128)(2,1)S(1)}, bf16[224,512]{1,0:T(8,128)(2,1)}, u32[]{:S(2)}) copy-start(bf16[224,512]{1,0:T(8,128)(2,1)} %get-tuple-element.42) | copy-start | bytes 688132
  300.4 19.6 %copy-start.28 = (bf16[224,512]{1,0:T(8,128)(2,1)S(1)}, bf16[224,512]{1,0:T(8,128)(2,1)}, u32[]{:S(2)}) copy-start(bf16[224,512]{1,0:T(8,128)(2,1)} %get-tuple-element.43) | copy-start | bytes 688132
  300.4 2.2 collective-permute-start.23
  304.8 30.3 %copy-start.9 = (bf16[128,2048]{1,0:T(8,128)(2,1)S(1)}, bf16[128,2048]{1,0:T(8,128)(2,1)}, u32[]{:S(2)}) copy-start(bf16[128,2048]{1,0:T(8,128)(2,1)} %get-tuple-element.35) | copy-start | bytes 1572868
  304.8 30.3 %copy-start.10 = (bf16[128,2048]{1,0:T(8,128)(2,1)S(1)}, bf16[128,2048]{1,0:T(8,128)(2,1)}, u32[]{:S(2)}) copy-start(bf16[128,2048]{1,0:T(8,128)(2,1)} %get-tuple-element.38) | copy-start | bytes 1572868
  304.8 30.3 %copy-start.11 = (bf16[96,2048]{1,0:T(8,128)(2,1)S(1)}, bf16[96,2048]{1,0:T(8,128)(2,1)}, u32[]{:S(2)}) copy-start(bf16[96,2048]{1,0:T(8,128)(2,1)} %get-tuple-element.37) | copy-start | bytes 1179652
  304.8 30.3 %copy-start.12 = (bf16[96,2048]{1,0:T(8,128)(2,1)S(1)}, bf16[96,2048]{1,0:T(8,128)(2,1)}, u32[]{:S(2)}) copy-start(bf16[96,2048]{1,0:T(8,128)(2,1)} %get-tuple-element.39) | copy-start | bytes 1179652
  304.9 40.9 %all-to-all-start.4 = ((bf16[16,32,512]{2,1,0:T(8,128)(2,1)}), bf16[16,32,512]{2,1,0:T(8,128)(2,1)S(1)}, u32[]{:S(2)}, u32[]{:S(2)}) async-start(bf16[16,32,512]{2,1,0:T(8,128)(2,1)} %bitcast.15), calls=%async_computation.4 | async-start | bytes 1048576 | tf_op jit(solution)/shard_map/all_to_all | solution.py:356
  316.8 13.8 %collective-permute-start.3 = (bf16[224,512]{1,0:T(8,128)(2,1)}, bf16[224,512]{1,0:T(8,128)(2,1)S(1)}, u32[]{:S(2)}, u32[]{:S(2)}) collective-permute-start(bf16[224,512]{1,0:T(8,128)(2,1)} %get-tuple-element.41), channel_id=1, source_target_pairs={{0,1},{1,2},{2,3},{3,0},{4,5},{5,6},{6,7},{7,4},{8,9},{9,10},{10,1... | collective-permute-start | bytes 688136 | tf_op jit(solution)/shard_map/ppermute | solution.py:291
  317.1 13.5 %collective-permute-start.4 = (bf16[224,512]{1,0:T(8,128)(2,1)S(1)}, bf16[224,512]{1,0:T(8,128)(2,1)S(1)}, u32[]{:S(2)}, u32[]{:S(2)}) collective-permute-start(bf16[224,512]{1,0:T(8,128)(2,1)S(1)} %copy-done.29), channel_id=1, source_target_pairs={{0,2},{1,3},{2,0},{3,1},{4,6},{5,7},{6,4},{7,5},{8,10},{9,11},{10,... | collective-permute-start | bytes 688136 | tf_op jit(solution)/shard_map/ppermute | solution.py:291
  319.9 11.0 %collective-permute-start.5 = (bf16[224,512]{1,0:T(8,128)(2,1)S(1)}, bf16[224,512]{1,0:T(8,128)(2,1)S(1)}, u32[]{:S(2)}, u32[]{:S(2)}) collective-permute-start(bf16[224,512]{1,0:T(8,128)(2,1)S(1)} %copy-done.28), channel_id=1, source_target_pairs={{0,3},{1,0},{2,1},{3,2},{4,7},{5,4},{6,5},{7,6},{8,11},{9,8},{10,9... | collective-permute-start | bytes 688136 | tf_op jit(solution)/shard_map/ppermute | solution.py:291
  330.6 0.7 copy-start.13
  330.6 0.8 copy-start.14
  331.0 0.7 copy-start.15
Sparse Core Ops, SparseCore 0:
  65.4 85.1 all-gather.1

commit v2 on v1

--- a/solution.py
+++ b/solution.py
@@ -172,49 +172,61 @@
 
 
 def hidden_kernel(depth, n_tp, first, n_parts, place_ref, *refs):
-    both_refs, token_refs, (out_ref, block_ref) = refs[:n_parts], refs[n_parts:-2], refs[-2:]
-    quarter, core = pl.program_id(0) + first, pl.program_id(1)
-    shift = lax.rem(place_ref[0] + n_tp - quarter, n_tp)
-    other = jnp.where(core == place_ref[1], 0, 1)
-    for k, token_ref in enumerate(token_refs):
-
-        @pl.when(2 * shift + other == k)
-        def _():
-            block_ref[...] = token_ref[...]
-
-    tokens = block_ref[:, :depth]
-    shares = block_ref[:, depth:].astype(F32)
-    lane = lax.broadcasted_iota(jnp.int32, shares.shape, 1)
-    share = jnp.sum(jnp.where(lane == place_ref[0], shares, 0.0), axis=1, keepdims=True)
-    at = 0
-    for both_ref in both_refs:
-        acts = lax.dot_general(tokens, both_ref[...], (((1,), (1,)), ((), ())), preferred_element_type=F32)
-        half = acts.shape[1] // 2
-        gate, up = acts[:, :half], acts[:, half:]
-        hidden = gate / (1.0 + jnp.exp(-gate)) * up * share
-        out_ref[0, 0, :, at : at + half] = hidden.astype(BF16)
-        at += half
+    both_refs, token_refs, (out_ref, held_ref, sems) = refs[:n_parts], refs[n_parts:-3], refs[-3:]
+    blocks = held_ref.shape[0]
+    for i in range(blocks):
+        shift = lax.rem(place_ref[0] + n_tp - (first + i // 2), n_tp)
+        other = jnp.where(place_ref[1] == i % 2, 0, 1)
+        for k, token_ref in enumerate(token_refs):
+
+            @pl.when(2 * shift + other == k)
+            def _():
+                pltpu.make_async_copy(token_ref, held_ref.at[i], sems.at[i]).start()
+
+    def step(i, carry):
+        pltpu.make_async_copy(token_refs[0], held_ref.at[i], sems.at[i]).wait()
+        tokens = held_ref[i, :, :depth]
+        shares = held_ref[i, :, depth:].astype(F32)
+        lane = lax.broadcasted_iota(jnp.int32, shares.shape, 1)
+        share = jnp.sum(jnp.where(lane == place_ref[0], shares, 0.0), axis=1, keepdims=True)
+        at = 0
+        for both_ref in both_refs:
+            acts = lax.dot_general(
+                tokens, both_ref[...], (((1,), (1,)), ((), ())), preferred_element_type=F32
+            )
+            half = acts.shape[1] // 2
+            gate, up = acts[:, :half], acts[:, half:]
+            hidden = gate / (1.0 + jnp.exp(-gate)) * up * share
+            out_ref[i, :, at : at + half] = hidden.astype(BF16)
+            at += half
+        return carry
+
+    lax.fori_loop(0, blocks, step, 0)
 
 
 def hidden_of(place, tokens, boths, depth, first, count):
     n_tp = len(tokens) // 2
     rows, wide = tokens[0].shape
     half = sum(both.shape[0] for both in boths) // 2
-    work = count * 2 * rows
+    blocks = 2 * count
     vmem = pl.BlockSpec(memory_space=pltpu.VMEM)
-    return pl.pallas_call(
+    out = pl.pallas_call(
         functools.partial(hidden_kernel, depth, n_tp, first, len(boths)),
-        grid=(count, 2),
-        in_specs=[pl.BlockSpec(memory_space=pltpu.SMEM), *[vmem] * (len(boths) + len(tokens))],
-        out_specs=pl.BlockSpec((1, 1, rows, half), lambda q, c: (q, c, 0, 0)),
-        out_shape=jax.ShapeDtypeStruct((count, 2, rows, half), BF16),
-        scratch_shapes=[pltpu.VMEM((rows, wide), BF16)],
-        compiler_params=params("arbitrary", "arbitrary"),
+        in_specs=[
+            pl.BlockSpec(memory_space=pltpu.SMEM),
+            *[vmem] * len(boths),
+            *[pl.BlockSpec(memory_space=pl.ANY)] * len(tokens),
+        ],
+        out_specs=vmem,
+        out_shape=jax.ShapeDtypeStruct((blocks, rows, half), BF16),
+        scratch_shapes=[pltpu.VMEM((blocks, rows, wide), BF16), pltpu.SemaphoreType.DMA((blocks,))],
+        compiler_params=params(),
         cost_estimate=pl.CostEstimate(
-            flops=2 * work * depth * 2 * half, bytes_accessed=work * wide * 2, transcendentals=work * half
+            flops=4 * blocks * rows * depth * half, bytes_accessed=blocks * rows * wide * 2, transcendentals=blocks * rows * half
         ),
         name="hidden",
     )(place, *boths, *tokens)
+    return out.reshape(count, 2, rows, half)
 
 
 def down_kernel(place_ref, down_ref, *refs):
@@ -232,7 +244,7 @@
     even, odd = total[:rows], total[rows:]
     keep = jnp.where(mine, even, odd)
     send = jnp.where(mine, odd, even).astype(BF16)
-    keep_ref[...] = keep.reshape(keep_ref.shape)
+    keep_ref[...] = keep.astype(BF16).reshape(keep_ref.shape)
     send_ref[...] = send.reshape(send_ref.shape)
 
 
@@ -250,7 +262,7 @@
             *[pl.BlockSpec((1, 2, rows, piece.shape[3]), lambda q: (q, 0, 0, 0)) for piece in pieces],
         ],
         out_specs=[out, out],
-        out_shape=[jax.ShapeDtypeStruct(shape, F32), jax.ShapeDtypeStruct(shape, BF16)],
+        out_shape=[jax.ShapeDtypeStruct(shape, BF16)] * 2,
         compiler_params=params("arbitrary"),
         cost_estimate=pl.CostEstimate(
             flops=4 * count * rows * down.size, bytes_accessed=count * rows * 2 * (features * 3 + 2048), transcendentals=0
@@ -351,7 +363,7 @@
     out = []
     for q in range(chunks):
         keep, send = down_of(place, down_padded, gathered[q], n_z)
-        summed = (keep + lax.ppermute(send, "fs", swap).astype(F32)).astype(BF16)
+        summed = (keep.astype(F32) + lax.ppermute(send, "fs", swap).astype(F32)).astype(BF16)
         summed = summed.reshape(n_z, per * some, features)
         spread = lax.all_to_all(summed, "fs", 0, 0, axis_index_groups=columns, tiled=True)
         out.append(jnp.sum(spread.astype(F32), axis=0).astype(BF16))

time: 355 us -> 349 us (0.983)
  Pallas kernels: 56.5 us -> 50.8 us
    pallas_call x3, Pallas kernels: 22.7 us -> 17.2 us  [hidden_of(): pl.pallas_call(functools.partial(hidden_kernel, depth, n_tp, first, len(b...]
  transfers between devices with their start and end apart: 29 -> 29, of which waited for: 17 -> 17; matrix products, arithmetic and copies ran while one was open for 1% -> 1% of each run, Pallas kernels for 13% -> 12%
where the time goes in v2:
time: 349 us; the launch traced here: 348 us
  waiting for transfers between devices  171 us (49%)
  starting transfers between devices  74.8 us (21%)
  Pallas kernels  50.8 us (15%)
  blocking collectives  20 us (6%)
  between operations  14.4 us (4%)
  other arithmetic  10.9 us (3%)
  local copies, waits for them, and re-layouts  5.74 us (2%)
    ppermute x12, waiting for transfers between devices, around(): lax.ppermute(array, axis, [(i, (i + shift) % n) for i in range(n)])  73.7 us
    all_to_all x1, waiting for transfers between devices, body(): received = lax.all_to_all(across, 'fs', 0, 0, tiled=True)  41 us
    all_to_all x1, starting transfers between devices, body(): received = lax.all_to_all(across, 'fs', 0, 0, tiled=True)  24.7 us
    all_gather x1, waiting for transfers between devices, body(): lax.all_gather(rows, 'fs', axis=0, axis_index_groups=columns, tiled=True)  23.4 us
    all_to_all x1, blocking collectives, body(): lax.all_to_all(first_part, 'tp', 0, 0, tiled=True)  20 us
    ppermute x6, waiting for transfers between devices, dealt(): lax.ppermute(pieces[shift], axis, [(i, (i + shift) % n) for i in range(n)])  19 us
    all_to_all x2, starting transfers between devices, body(): lax.all_to_all(summed, 'fs', 0, 0, axis_index_groups=columns, tiled=True)  19 us
    pallas_call x3, Pallas kernels, hidden_of(): pl.pallas_call(functools.partial(hidden_kernel, depth, n_tp, first, len(b...  17.2 us
  transfers between devices with their start and end apart: 29, of which 17 were waited for; matrix products, arithmetic and copies ran while one was open for 1% of the time, Pallas kernels for 12%

profile of v2, /device:TPU:40, one launch (start us, length us, event | category | flops | bytes accessed | tf_op | source)
XLA Modules:
  0.0 347.9 jit_solution(14419140711394904246)
XLA Ops:
  7.2 1.4 maximum_bitcast_fusion.2.scale_ref
  8.6 1.0 fusion
  9.6 0.8 constant_dynamic-slice_fusion
  10.4 0.9 fusion.1
  11.3 0.6 pad_add_fusion.place_ref
  12.0 0.6 pad_maximum_fusion
  12.7 5.4 %pack.1 = (bf16[4,8,128,128]{3,2,1,0:T(8,128)(2,1)}, bf16[8,96,128]{2,1,0:T(8,128)(2,1)}, bf16[8,96,128]{2,1,0:T(8,128)(2,1)}, bf16[8,96,128]{2,1,0:T(8,128)(2,1)}, bf16[8,96,128]{2,1,0:T(8,128)(2,1)}) custom-call(s32[2]{0:T(128)} %pad_add_fusion.place_ref, f32[1,128]{1,0:T(1,128)} %maximum_bitcast_fusion.2.scale_ref, f32[4,64,1792]{2,1,0:T(8,128)} %gate_ref.1, ...), custom_call_target="tpu_custom_call" | custom-call | flops 458752000 | bytes 5505024 | tf_op jit(solution)/shard_map/pack/pallas_call | solution.py:41
  18.1 20.0 %all_to_all.25 = bf16[4,1024,128]{2,1,0:T(8,128)(2,1)} all-to-all(bf16[4,1024,128]{2,1,0:T(8,128)(2,1)} %bitcast.28), channel_id=1, replica_groups=mesh['grp'=2,'fs'=32,'tp'=4] {'tp'}, dimensions={0} | all-to-all | bytes 2097152 | tf_op jit(solution)/shard_map/all_to_all | solution.py:336
  38.1 24.7 %all-to-all-start.1 = ((bf16[32,128,128]{2,1,0:T(8,128)(2,1)}), bf16[32,128,128]{2,1,0:T(8,128)(2,1)S(1)}, u32[]{:S(2)}, u32[]{:S(2)}) async-start(bf16[32,128,128]{2,1,0:T(8,128)(2,1)} %bitcast.8), calls=%async_computation.1 | async-start | bytes 2097152 | tf_op jit(solution)/shard_map/all_to_all | solution.py:337
  62.9 0.7 all-gather.2.cloned.1.call-update
  63.6 0.9 collective-permute-start
  64.5 1.9 collective-permute-start.1
  66.4 1.0 collective-permute-start.2
  67.4 8.4 %collective-permute-done.refs_1_ = bf16[8,96,128]{2,1,0:T(8,128)(2,1)S(1)} collective-permute-done((bf16[8,96,128]{2,1,0:T(8,128)(2,1)S(1)}, bf16[8,96,128]{2,1,0:T(8,128)(2,1)S(1)}, u32[]{:S(2)}, u32[]{:S(2)}) %collective-permute-start) | collective-permute-done | bytes 196640 | tf_op jit(solution)/shard_map/ppermute | solution.py:303
  75.8 0.6 collective-permute-done.2.refs_3_
  76.5 0.5 copy-done.18
  77.1 3.4 join.2
  80.5 41.0 %all-to-all-done.1.recv_ref = bf16[32,128,128]{2,1,0:T(8,128)(2,1)S(1)} async-done(((bf16[32,128,128]{2,1,0:T(8,128)(2,1)}), bf16[32,128,128]{2,1,0:T(8,128)(2,1)S(1)}, u32[]{:S(2)}, u32[]{:S(2)}) %all-to-all-start.1) | async-done | bytes 1048608 | tf_op jit(solution)/shard_map/all_to_all | solution.py:337
  121.5 5.8 %all-to-all-start.2 = ((bf16[32,96,128]{2,1,0:T(8,128)(2,1)}), bf16[32,96,128]{2,1,0:T(8,128)(2,1)}, u32[]{:S(2)}, u32[]{:S(2)}) async-start(bf16[32,96,128]{2,1,0:T(8,128)(2,1)} %join.2), calls=%async_computation.2 | async-start | bytes 1572864 | tf_op jit(solution)/shard_map/all_to_all | solution.py:340
  127.3 23.4 %all-gather.2.cloned.1.call-done.in_ref = bf16[256,2176]{1,0:T(8,128)(2,1)} async-done(((bf16[16,2176]{1,0:T(8,128)(2,1)}), bf16[256,2176]{1,0:T(8,128)(2,1)}) %all-gather.2.cloned.1.call-update) | async-done | bytes 1114128 | tf_op jit(solution)/shard_map/all_gather | solution.py:333
  150.7 2.4 held.1.refs_1_.refs_2_
  153.0 4.7 %collective-permute-start.11 = (bf16[256,2176]{1,0:T(8,128)(2,1)}, bf16[256,2176]{1,0:T(8,128)(2,1)S(1)}, u32[]{:S(2)}, u32[]{:S(2)}) collective-permute-start(bf16[256,2176]{1,0:T(8,128)(2,1)} %held.1.refs_1_.refs_2_), channel_id=1, source_target_pairs={{0,3},{1,0},{2,1},{3,2},{4,7},{5,4},{6,5},{7,6},{8,11},{9,8},{10,9... | collective-permute-start | bytes 3342344 | tf_op jit(solution)/shard_map/ppermute | solution.py:295
  157.8 1.3 collective-permute-start.7
  159.1 21.6 %collective-permute-done.11.refs_7_.refs_8_ = bf16[256,2176]{1,0:T(8,128)(2,1)S(1)} collective-permute-done((bf16[256,2176]{1,0:T(8,128)(2,1)}, bf16[256,2176]{1,0:T(8,128)(2,1)S(1)}, u32[]{:S(2)}, u32[]{:S(2)}) %collective-permute-start.11) | collective-permute-done | bytes 1114144 | tf_op jit(solution)/shard_map/ppermute | solution.py:295
  180.7 6.2 %collective-permute-done.9.refs_5_.refs_6_ = bf16[256,2176]{1,0:T(8,128)(2,1)S(1)} collective-permute-done((bf16[256,2176]{1,0:T(8,128)(2,1)}, bf16[256,2176]{1,0:T(8,128)(2,1)S(1)}, u32[]{:S(2)}, u32[]{:S(2)}) %collective-permute-start.9) | collective-permute-done | bytes 1114144 | tf_op jit(solution)/shard_map/ppermute | solution.py:295
  186.9 14.4 %collective-permute-done.7.refs_3_.refs_4_ = bf16[256,2176]{1,0:T(8,128)(2,1)S(1)} collective-permute-done((bf16[256,2176]{1,0:T(8,128)(2,1)}, bf16[256,2176]{1,0:T(8,128)(2,1)S(1)}, u32[]{:S(2)}, u32[]{:S(2)}) %collective-permute-start.7) | collective-permute-done | bytes 1114144 | tf_op jit(solution)/shard_map/ppermute | solution.py:295
  201.4 3.5 %unpack.2 = (bf16[128,2048]{1,0:T(8,128)(2,1)}, bf16[128,2048]{1,0:T(8,128)(2,1)}, bf16[256,2048]{1,0:T(8,128)(2,1)}) custom-call(bf16[32,128,128]{2,1,0:T(8,128)(2,1)} %copy-done.8), custom_call_target="tpu_custom_call" | custom-call | flops 20971520 | bytes 3145728 | tf_op jit(solution)/shard_map/unpack/pallas_call | solution.py:159
  205.0 0.9 copy-done.4
  206.9 5.2 %hidden.3 = bf16[4,256,128]{2,1,0:T(8,128)(2,1)} custom-call(s32[2]{0:T(128)} %pad_add_fusion.place_ref, bf16[256,2048]{1,0:T(8,128)(2,1)} %get-tuple-element.45.refs_0_, bf16[256,2176]{1,0:T(8,128)(2,1)} %held.1.refs_1_.refs_2_, bf16[256,2176]{1,0:T(8,128)(2,1)} %copy-done.4, bf16[256,2176]{1,0:T(8,128)(2,1)} %copy-done.3, bf16[256,2176]{1,0:T(8,128)(2,1)} %copy-done.7, ...), custom_call_target="tpu_custom_call" | custom-call | flops 1073741824 | bytes 4456448 | tf_op jit(solution)/shard_map/hidden/pallas_call | solution.py:213
  212.2 0.7 collective-permute-start.15
  212.9 1.3 collective-permute-start.14
  214.2 0.8 collective-permute-start.13
  215.0 2.8 unpack.3
  217.9 5.2 %hidden.4 = bf16[4,256,128]{2,1,0:T(8,128)(2,1)} custom-call(s32[2]{0:T(128)} %pad_add_fusion.place_ref, bf16[256,2048]{1,0:T(8,128)(2,1)} %get-tuple-element.47.refs_0_.refs_1_, bf16[256,2176]{1,0:T(8,128)(2,1)} %held.1.refs_1_.refs_2_, bf16[256,2176]{1,0:T(8,128)(2,1)} %copy-done.4, bf16[256,2176]{1,0:T(8,128)(2,1)} %copy-done.3, ...), custom_call_target="tpu_custom_call" | custom-call | flops 1073741824 | bytes 4456448 | tf_op jit(solution)/shard_map/hidden/pallas_call | solution.py:213
  223.1 2.5 collective-permute-start.18
  225.6 1.2 collective-permute-start.17
  226.8 1.3 collective-permute-start.16
  228.1 4.6 %cast_down.1 = (bf16[4,256,512]{2,1,0:T(8,128)(2,1)}, bf16[224,512]{1,0:T(8,128)(2,1)}, bf16[224,512]{1,0:T(8,128)(2,1)}, bf16[224,512]{1,0:T(8,128)(2,1)}, bf16[224,512]{1,0:T(8,128)(2,1)}) custom-call(s32[2]{0:T(128)} %pad_add_fusion.place_ref, f32[4,224,512]{2,1,0:T(8,128)} %down_ref.1), custom_call_target="tpu_custom_call" | custom-call | flops 229376000 | bytes 3670016 | tf_op jit(solution)/shard_map/cast_down/pallas_call | solution.py:87
  232.7 4.4 %collective-permute-done.18.refs_7_ = bf16[2,2,256,128]{3,2,1,0:T(8,128)(2,1)S(1)} collective-permute-done((bf16[2,2,256,128]{3,2,1,0:T(8,128)(2,1)}, bf16[2,2,256,128]{3,2,1,0:T(8,128)(2,1)S(1)}, u32[]{:S(2)}, u32[]{:S(2)}) %collective-permute-start.18) | collective-permute-done | bytes 262176 | tf_op jit(solution)/shard_map/ppermute | solution.py:295
  237.1 3.0 collective-permute-done.16.refs_5_
  240.2 0.7 copy-done.27
  240.8 4.1 %down.2 = (bf16[16,2,16,512]{3,2,1,0:T(8,128)(2,1)}, bf16[16,2,16,512]{3,2,1,0:T(8,128)(2,1)}) custom-call(s32[2]{0:T(128)} %pad_add_fusion.place_ref, bf16[4,256,512]{2,1,0:T(8,128)(2,1)} %get-tuple-element.44.down_ref, bf16[2,2,256,128]{3,2,1,0:T(8,128)(2,1)} %bitcast.37, bf16[2,2,256,128]{3,2,1,0:T(8,128)(2,1)} %copy-done.24, ...), custom_call_target="tpu_custom_call" | custom-call | flops 1073741824 | bytes 3670016 | tf_op jit(solution)/shard_map/down/pallas_call | solution.py:256
  245.1 2.1 collective-permute-done.19
  247.2 2.1 add_convert_fusion.1
  249.3 7.1 %all-to-all-start.3 = ((bf16[16,32,512]{2,1,0:T(8,128)(2,1)}), bf16[16,32,512]{2,1,0:T(8,128)(2,1)S(1)}, u32[]{:S(2)}, u32[]{:S(2)}) async-start(bf16[16,32,512]{2,1,0:T(8,128)(2,1)} %bitcast.16), calls=%async_computation.3 | async-start | bytes 1048576 | tf_op jit(solution)/shard_map/all_to_all | solution.py:368
  256.3 6.7 %hidden.5 = bf16[4,256,256]{2,1,0:T(8,128)(2,1)} custom-call(s32[2]{0:T(128)} %pad_add_fusion.place_ref, bf16[256,2048]{1,0:T(8,128)(2,1)} %get-tuple-element.45.refs_0_, bf16[256,2048]{1,0:T(8,128)(2,1)} %get-tuple-element.47.refs_0_.refs_1_, bf16[256,2176]{1,0:T(8,128)(2,1)} %held.1.refs_1_.refs_2_, bf16[256,2176]{1,0:T(8,128)(2,1)} %copy-done.4, ...), custom_call_target="tpu_custom_call" | custom-call | flops 2147483648 | bytes 4456448 | tf_op jit(solution)/shard_map/hidden/pallas_call | solution.py:213
  263.1 0.9 collective-permute-start.22
  263.9 1.5 collective-permute-start.21
  265.4 0.8 collective-permute-start.20
  266.2 12.0 %collective-permute-done.22.refs_3_ = bf16[2,2,256,256]{3,2,1,0:T(8,128)(2,1)S(1)} collective-permute-done((bf16[2,2,256,256]{3,2,1,0:T(8,128)(2,1)}, bf16[2,2,256,256]{3,2,1,0:T(8,128)(2,1)S(1)}, u32[]{:S(2)}, u32[]{:S(2)}) %collective-permute-start.22) | collective-permute-done | bytes 524320 | tf_op jit(solution)/shard_map/ppermute | solution.py:295
  278.2 2.3 collective-permute-done.21.refs_2_
  280.5 9.8 %collective-permute-done.20.refs_1_ = bf16[2,2,256,256]{3,2,1,0:T(8,128)(2,1)S(1)} collective-permute-done((bf16[2,2,256,256]{3,2,1,0:T(8,128)(2,1)}, bf16[2,2,256,256]{3,2,1,0:T(8,128)(2,1)S(1)}, u32[]{:S(2)}, u32[]{:S(2)}) %collective-permute-start.20) | collective-permute-done | bytes 524320 | tf_op jit(solution)/shard_map/ppermute | solution.py:295
  290.3 0.8 copy-done.21
  291.1 3.9 %down.3 = (bf16[16,2,16,512]{3,2,1,0:T(8,128)(2,1)}, bf16[16,2,16,512]{3,2,1,0:T(8,128)(2,1)}) custom-call(s32[2]{0:T(128)} %pad_add_fusion.place_ref, bf16[4,256,512]{2,1,0:T(8,128)(2,1)} %get-tuple-element.44.down_ref, bf16[2,2,256,256]{3,2,1,0:T(8,128)(2,1)} %bitcast.33, bf16[2,2,256,256]{3,2,1,0:T(8,128)(2,1)} %copy-done.21, ...), custom_call_target="tpu_custom_call" | custom-call | flops 1073741824 | bytes 3670016 | tf_op jit(solution)/shard_map/down/pallas_call | solution.py:256
  295.2 2.1 collective-permute-done.23
  297.3 2.1 add_convert_fusion
  299.4 11.9 %all-to-all-start.4 = ((bf16[16,32,512]{2,1,0:T(8,128)(2,1)}), bf16[16,32,512]{2,1,0:T(8,128)(2,1)S(1)}, u32[]{:S(2)}, u32[]{:S(2)}) async-start(bf16[16,32,512]{2,1,0:T(8,128)(2,1)} %bitcast.18), calls=%async_computation.4 | async-start | bytes 1048576 | tf_op jit(solution)/shard_map/all_to_all | solution.py:368
  311.4 2.9 collective-permute-start.4
  314.3 1.2 collective-permute-start.5
  315.5 9.6 %collective-permute-done.3.refs_1_ = bf16[224,512]{1,0:T(8,128)(2,1)S(1)} collective-permute-done((bf16[224,512]{1,0:T(8,128)(2,1)}, bf16[224,512]{1,0:T(8,128)(2,1)S(1)}, u32[]{:S(2)}, u32[]{:S(2)}) %collective-permute-start.3) | collective-permute-done | bytes 229408 | tf_op jit(solution)/shard_map/ppermute | solution.py:303
  326.2 3.5 %join.3 = bf16[224,2048]{1,0:T(8,128)(2,1)} custom-call(s32[2]{0:T(128)} %pad_add_fusion.place_ref, bf16[224,512]{1,0:T(8,128)(2,1)} %get-tuple-element.40.refs_0_, bf16[224,512]{1,0:T(8,128)(2,1)} %copy-done.13, bf16[224,512]{1,0:T(8,128)(2,1)} %copy-done.14, bf16[224,512]{1,0:T(8,128)(2,1)} %copy-done.15), custom_call_target="tpu_custom_call" | custom-call | flops 229376000 | bytes 1835008 | tf_op jit(solution)/shard_map/join/pallas_call | solution.py:123
  329.7 1.3 maximum_bitcast_fusion
  331.1 9.2 %all-to-all-done.4 = bf16[16,32,512]{2,1,0:T(8,128)(2,1)S(1)} async-done(((bf16[16,32,512]{2,1,0:T(8,128)(2,1)}), bf16[16,32,512]{2,1,0:T(8,128)(2,1)S(1)}, u32[]{:S(2)}, u32[]{:S(2)}) %all-to-all-start.4) | async-done | bytes 524320 | tf_op jit(solution)/shard_map/all_to_all | solution.py:368
  340.4 0.6 pad_maximum_fusion.1
  (91 shorter events, 3.2 us)
Async XLA Ops:
  7.2 2.4 copy-start
  18.1 45.6 %copy-start.32 = (bf16[8,96,128]{2,1,0:T(8,128)(2,1)S(1)}, bf16[8,96,128]{2,1,0:T(8,128)(2,1)}, u32[]{:S(2)}) copy-start(bf16[8,96,128]{2,1,0:T(8,128)(2,1)} %get-tuple-element.30) | copy-start | bytes 589828
  18.1 46.4 %copy-start.31 = (bf16[8,96,128]{2,1,0:T(8,128)(2,1)S(1)}, bf16[8,96,128]{2,1,0:T(8,128)(2,1)}, u32[]{:S(2)}) copy-start(bf16[8,96,128]{2,1,0:T(8,128)(2,1)} %get-tuple-element.31) | copy-start | bytes 589828
  18.1 48.3 %copy-start.30 = (bf16[8,96,128]{2,1,0:T(8,128)(2,1)S(1)}, bf16[8,96,128]{2,1,0:T(8,128)(2,1)}, u32[]{:S(2)}) copy-start(bf16[8,96,128]{2,1,0:T(8,128)(2,1)} %get-tuple-element.32) | copy-start | bytes 589828
  38.1 83.4 %all-to-all-start.1 = ((bf16[32,128,128]{2,1,0:T(8,128)(2,1)}), bf16[32,128,128]{2,1,0:T(8,128)(2,1)S(1)}, u32[]{:S(2)}, u32[]{:S(2)}) async-start(bf16[32,128,128]{2,1,0:T(8,128)(2,1)} %bitcast.8), calls=%async_computation.1 | async-start | bytes 2097152 | tf_op jit(solution)/shard_map/all_to_all | solution.py:337
  62.8 87.9 %all-gather.2.cloned.1.call-start = ((), (), s32[]{:S(2)}) async-start(), calls=%async_computation.5 | async-start | bytes 1183744 | tf_op jit(solution)/shard_map/all_gather | solution.py:333
  63.6 12.2 %collective-permute-start = (bf16[8,96,128]{2,1,0:T(8,128)(2,1)S(1)}, bf16[8,96,128]{2,1,0:T(8,128)(2,1)S(1)}, u32[]{:S(2)}, u32[]{:S(2)}) collective-permute-start(bf16[8,96,128]{2,1,0:T(8,128)(2,1)S(1)} %copy-done.32), channel_id=1, source_target_pairs={{0,1},{1,2},{2,3},{3,0},{4,5},{5,6},{6,7},{7,4},{8,9},{9,10},{10,1... | collective-permute-start | bytes 589832 | tf_op jit(solution)/shard_map/ppermute | solution.py:303
  64.5 11.3 %collective-permute-start.1 = (bf16[8,96,128]{2,1,0:T(8,128)(2,1)S(1)}, bf16[8,96,128]{2,1,0:T(8,128)(2,1)S(1)}, u32[]{:S(2)}, u32[]{:S(2)}) collective-permute-start(bf16[8,96,128]{2,1,0:T(8,128)(2,1)S(1)} %copy-done.31), channel_id=1, source_target_pairs={{0,2},{1,3},{2,0},{3,1},{4,6},{5,7},{6,4},{7,5},{8,10},{9,11},{10,... | collective-permute-start | bytes 589832 | tf_op jit(solution)/shard_map/ppermute | solution.py:303
  66.4 10.0 %collective-permute-start.2 = (bf16[8,96,128]{2,1,0:T(8,128)(2,1)S(1)}, bf16[8,96,128]{2,1,0:T(8,128)(2,1)S(1)}, u32[]{:S(2)}, u32[]{:S(2)}) collective-permute-start(bf16[8,96,128]{2,1,0:T(8,128)(2,1)S(1)} %copy-done.30), channel_id=1, source_target_pairs={{0,3},{1,0},{2,1},{3,2},{4,7},{5,4},{6,5},{7,6},{8,11},{9,8},{10,9... | collective-permute-start | bytes 589832 | tf_op jit(solution)/shard_map/ppermute | solution.py:303
  75.8 0.7 copy-start.16
  75.8 0.7 copy-start.17
  76.4 0.7 copy-start.18
  121.5 29.2 %copy-start.8 = (bf16[32,128,128]{2,1,0:T(8,128)(2,1)}, bf16[32,128,128]{2,1,0:T(8,128)(2,1)S(1)}, u32[]{:S(2)}) copy-start(bf16[32,128,128]{2,1,0:T(8,128)(2,1)S(1)} %all-to-all-done.1.recv_ref) | copy-start | bytes 3145732
  121.5 93.5 %all-to-all-start.2 = ((bf16[32,96,128]{2,1,0:T(8,128)(2,1)}), bf16[32,96,128]{2,1,0:T(8,128)(2,1)}, u32[]{:S(2)}, u32[]{:S(2)}) async-start(bf16[32,96,128]{2,1,0:T(8,128)(2,1)} %join.2), calls=%async_computation.2 | async-start | bytes 1572864 | tf_op jit(solution)/shard_map/all_to_all | solution.py:340
  153.0 27.6 %collective-permute-start.11 = (bf16[256,2176]{1,0:T(8,128)(2,1)}, bf16[256,2176]{1,0:T(8,128)(2,1)S(1)}, u32[]{:S(2)}, u32[]{:S(2)}) collective-permute-start(bf16[256,2176]{1,0:T(8,128)(2,1)} %held.1.refs_1_.refs_2_), channel_id=1, source_target_pairs={{0,3},{1,0},{2,1},{3,2},{4,7},{5,4},{6,5},{7,6},{8,11},{9,8},{10,9... | collective-permute-start | bytes 3342344 | tf_op jit(solution)/shard_map/ppermute | solution.py:295
  157.8 29.2 %collective-permute-start.9 = (bf16[256,2176]{1,0:T(8,128)(2,1)}, bf16[256,2176]{1,0:T(8,128)(2,1)S(1)}, u32[]{:S(2)}, u32[]{:S(2)}) collective-permute-start(bf16[256,2176]{1,0:T(8,128)(2,1)} %held.1.refs_1_.refs_2_), channel_id=1, source_target_pairs={{0,2},{1,3},{2,0},{3,1},{4,6},{5,7},{6,4},{7,5},{8,10},{9,11},{10,... | collective-permute-start | bytes 3342344 | tf_op jit(solution)/shard_map/ppermute | solution.py:295
  157.8 43.6 %collective-permute-start.7 = (bf16[256,2176]{1,0:T(8,128)(2,1)}, bf16[256,2176]{1,0:T(8,128)(2,1)S(1)}, u32[]{:S(2)}, u32[]{:S(2)}) collective-permute-start(bf16[256,2176]{1,0:T(8,128)(2,1)} %held.1.refs_1_.refs_2_), channel_id=1, source_target_pairs={{0,1},{1,2},{2,3},{3,0},{4,5},{5,6},{6,7},{7,4},{8,9},{9,10},{10,1... | collective-permute-start | bytes 3342344 | tf_op jit(solution)/shard_map/ppermute | solution.py:295
  159.1 45.8 %collective-permute-start.6 = (bf16[256,2176]{1,0:T(8,128)(2,1)}, bf16[256,2176]{1,0:T(8,128)(2,1)S(1)}, u32[]{:S(2)}, u32[]{:S(2)}) collective-permute-start(bf16[256,2176]{1,0:T(8,128)(2,1)} %held.1.refs_1_.refs_2_), channel_id=1, source_target_pairs={{0,4},{4,0},{8,12},{12,8},{16,20},{20,16},{24,28},{28,24},{32,36},... | collective-permute-start | bytes 3342344 | tf_op jit(solution)/shard_map/ppermute | solution.py:346
  180.7 24.3 %copy-start.1 = (bf16[256,2176]{1,0:T(8,128)(2,1)}, bf16[256,2176]{1,0:T(8,128)(2,1)S(1)}, u32[]{:S(2)}) copy-start(bf16[256,2176]{1,0:T(8,128)(2,1)S(1)} %collective-permute-done.11.refs_7_.refs_8_) | copy-start | bytes 3342340
  180.7 24.2 %collective-permute-start.12 = (bf16[256,2176]{1,0:T(8,128)(2,1)S(1)}, bf16[256,2176]{1,0:T(8,128)(2,1)S(1)}, u32[]{:S(2)}, u32[]{:S(2)}) collective-permute-start(bf16[256,2176]{1,0:T(8,128)(2,1)S(1)} %collective-permute-done.11.refs_7_.refs_8_), channel_id=1, source_target_pairs={{0,4},{4,0},{8,12},{12,8},{16,20},{20,16},{24,28},{28,24},{32,36},... | collective-permute-start | bytes 3342344 | tf_op jit(solution)/shard_map/ppermute | solution.py:346
  186.9 18.0 %copy-start.2 = (bf16[256,2176]{1,0:T(8,128)(2,1)}, bf16[256,2176]{1,0:T(8,128)(2,1)S(1)}, u32[]{:S(2)}) copy-start(bf16[256,2176]{1,0:T(8,128)(2,1)S(1)} %collective-permute-done.9.refs_5_.refs_6_) | copy-start | bytes 3342340
  186.9 18.0 %collective-permute-start.10 = (bf16[256,2176]{1,0:T(8,128)(2,1)S(1)}, bf16[256,2176]{1,0:T(8,128)(2,1)S(1)}, u32[]{:S(2)}, u32[]{:S(2)}) collective-permute-start(bf16[256,2176]{1,0:T(8,128)(2,1)S(1)} %collective-permute-done.9.refs_5_.refs_6_), channel_id=1, source_target_pairs={{0,4},{4,0},{8,12},{12,8},{16,20},{20,16},{24,28},{28,24},{32,36},... | collective-permute-start | bytes 3342344 | tf_op jit(solution)/shard_map/ppermute | solution.py:346
  201.4 3.6 %copy-start.3 = (bf16[256,2176]{1,0:T(8,128)(2,1)}, bf16[256,2176]{1,0:T(8,128)(2,1)S(1)}, u32[]{:S(2)}) copy-start(bf16[256,2176]{1,0:T(8,128)(2,1)S(1)} %collective-permute-done.7.refs_3_.refs_4_) | copy-start | bytes 3342340
  201.4 3.6 %collective-permute-start.8 = (bf16[256,2176]{1,0:T(8,128)(2,1)S(1)}, bf16[256,2176]{1,0:T(8,128)(2,1)S(1)}, u32[]{:S(2)}, u32[]{:S(2)}) collective-permute-start(bf16[256,2176]{1,0:T(8,128)(2,1)S(1)} %collective-permute-done.7.refs_3_.refs_4_), channel_id=1, source_target_pairs={{0,4},{4,0},{8,12},{12,8},{16,20},{20,16},{24,28},{28,24},{32,36},... | collective-permute-start | bytes 3342344 | tf_op jit(solution)/shard_map/ppermute | solution.py:346
  204.9 1.0 copy-start.4
  204.9 1.4 copy-start.5
  204.9 1.7 copy-start.6
  205.0 2.0 copy-start.7
  212.2 14.6 %collective-permute-start.15 = (bf16[2,2,256,128]{3,2,1,0:T(8,128)(2,1)}, bf16[2,2,256,128]{3,2,1,0:T(8,128)(2,1)S(1)}, u32[]{:S(2)}, u32[]{:S(2)}) collective-permute-start(bf16[2,2,256,128]{3,2,1,0:T(8,128)(2,1)} %bitcast.34), channel_id=1, source_target_pairs={{0,3},{1,0},{2,1},{3,2},{4,7},{5,4},{6,5},{7,6},{8,11},{9,8},{10,9... | collective-permute-start | bytes 786440 | tf_op jit(solution)/shard_map/ppermute | solution.py:295
  212.9 19.8 %collective-permute-start.14 = (bf16[2,2,256,128]{3,2,1,0:T(8,128)(2,1)}, bf16[2,2,256,128]{3,2,1,0:T(8,128)(2,1)S(1)}, u32[]{:S(2)}, u32[]{:S(2)}) collective-permute-start(bf16[2,2,256,128]{3,2,1,0:T(8,128)(2,1)} %bitcast.35), channel_id=1, source_target_pairs={{0,2},{1,3},{2,0},{3,1},{4,6},{5,7},{6,4},{7,5},{8,10},{9,11},{10,... | collective-permute-start | bytes 786440 | tf_op jit(solution)/shard_map/ppermute | solution.py:295
  214.2 18.5 %collective-permute-start.13 = (bf16[2,2,256,128]{3,2,1,0:T(8,128)(2,1)}, bf16[2,2,256,128]{3,2,1,0:T(8,128)(2,1)S(1)}, u32[]{:S(2)}, u32[]{:S(2)}) collective-permute-start(bf16[2,2,256,128]{3,2,1,0:T(8,128)(2,1)} %bitcast.36), channel_id=1, source_target_pairs={{0,1},{1,2},{2,3},{3,0},{4,5},{5,6},{6,7},{7,4},{8,9},{9,10},{10,1... | collective-permute-start | bytes 786440 | tf_op jit(solution)/shard_map/ppermute | solution.py:295
  223.1 14.0 %collective-permute-start.18 = (bf16[2,2,256,128]{3,2,1,0:T(8,128)(2,1)}, bf16[2,2,256,128]{3,2,1,0:T(8,128)(2,1)S(1)}, u32[]{:S(2)}, u32[]{:S(2)}) collective-permute-start(bf16[2,2,256,128]{3,2,1,0:T(8,128)(2,1)} %bitcast.38), channel_id=1, source_target_pairs={{0,3},{1,0},{2,1},{3,2},{4,7},{5,4},{6,5},{7,6},{8,11},{9,8},{10,9... | collective-permute-start | bytes 786440 | tf_op jit(solution)/shard_map/ppermute | solution.py:295
  225.6 11.5 %collective-permute-start.17 = (bf16[2,2,256,128]{3,2,1,0:T(8,128)(2,1)}, bf16[2,2,256,128]{3,2,1,0:T(8,128)(2,1)S(1)}, u32[]{:S(2)}, u32[]{:S(2)}) collective-permute-start(bf16[2,2,256,128]{3,2,1,0:T(8,128)(2,1)} %bitcast.39), channel_id=1, source_target_pairs={{0,2},{1,3},{2,0},{3,1},{4,6},{5,7},{6,4},{7,5},{8,10},{9,11},{10,... | collective-permute-start | bytes 786440 | tf_op jit(solution)/shard_map/ppermute | solution.py:295
  226.8 13.4 %copy-start.22 = (bf16[2,2,256,128]{3,2,1,0:T(8,128)(2,1)}, bf16[2,2,256,128]{3,2,1,0:T(8,128)(2,1)S(1)}, u32[]{:S(2)}) copy-start(bf16[2,2,256,128]{3,2,1,0:T(8,128)(2,1)S(1)} %collective-permute-done.15.refs_3_) | copy-start | bytes 786436
  226.8 13.4 %collective-permute-start.16 = (bf16[2,2,256,128]{3,2,1,0:T(8,128)(2,1)}, bf16[2,2,256,128]{3,2,1,0:T(8,128)(2,1)S(1)}, u32[]{:S(2)}, u32[]{:S(2)}) collective-permute-start(bf16[2,2,256,128]{3,2,1,0:T(8,128)(2,1)} %bitcast.40), channel_id=1, source_target_pairs={{0,1},{1,2},{2,3},{3,0},{4,5},{5,6},{6,7},{7,4},{8,9},{9,10},{10,1... | collective-permute-start | bytes 786440 | tf_op jit(solution)/shard_map/ppermute | solution.py:295
  232.7 7.5 %copy-start.23 = (bf16[2,2,256,128]{3,2,1,0:T(8,128)(2,1)}, bf16[2,2,256,128]{3,2,1,0:T(8,128)(2,1)S(1)}, u32[]{:S(2)}) copy-start(bf16[2,2,256,128]{3,2,1,0:T(8,128)(2,1)S(1)} %collective-permute-done.14.refs_2_) | copy-start | bytes 786436
  232.7 7.5 %copy-start.24 = (bf16[2,2,256,128]{3,2,1,0:T(8,128)(2,1)}, bf16[2,2,256,128]{3,2,1,0:T(8,128)(2,1)S(1)}, u32[]{:S(2)}) copy-start(bf16[2,2,256,128]{3,2,1,0:T(8,128)(2,1)S(1)} %collective-permute-done.13.refs_1_) | copy-start | bytes 786436
  237.1 3.0 copy-start.25
  237.1 3.0 copy-start.26
  240.1 0.7 copy-start.27
  244.9 2.2 collective-permute-start.19
  249.3 50.1 %all-to-all-start.3 = ((bf16[16,32,512]{2,1,0:T(8,128)(2,1)}), bf16[16,32,512]{2,1,0:T(8,128)(2,1)S(1)}, u32[]{:S(2)}, u32[]{:S(2)}) async-start(bf16[16,32,512]{2,1,0:T(8,128)(2,1)} %bitcast.16), calls=%async_computation.3 | async-start | bytes 1048576 | tf_op jit(solution)/shard_map/all_to_all | solution.py:368
  263.1 15.1 %collective-permute-start.22 = (bf16[2,2,256,256]{3,2,1,0:T(8,128)(2,1)}, bf16[2,2,256,256]{3,2,1,0:T(8,128)(2,1)S(1)}, u32[]{:S(2)}, u32[]{:S(2)}) collective-permute-start(bf16[2,2,256,256]{3,2,1,0:T(8,128)(2,1)} %bitcast.30), channel_id=1, source_target_pairs={{0,3},{1,0},{2,1},{3,2},{4,7},{5,4},{6,5},{7,6},{8,11},{9,8},{10,9... | collective-permute-start | bytes 1572872 | tf_op jit(solution)/shard_map/ppermute | solution.py:295
  263.9 16.6 %collective-permute-start.21 = (bf16[2,2,256,256]{3,2,1,0:T(8,128)(2,1)}, bf16[2,2,256,256]{3,2,1,0:T(8,128)(2,1)S(1)}, u32[]{:S(2)}, u32[]{:S(2)}) collective-permute-start(bf16[2,2,256,256]{3,2,1,0:T(8,128)(2,1)} %bitcast.31), channel_id=1, source_target_pairs={{0,2},{1,3},{2,0},{3,1},{4,6},{5,7},{6,4},{7,5},{8,10},{9,11},{10,... | collective-permute-start | bytes 1572872 | tf_op jit(solution)/shard_map/ppermute | solution.py:295
  265.4 24.9 %collective-permute-start.20 = (bf16[2,2,256,256]{3,2,1,0:T(8,128)(2,1)}, bf16[2,2,256,256]{3,2,1,0:T(8,128)(2,1)S(1)}, u32[]{:S(2)}, u32[]{:S(2)}) collective-permute-start(bf16[2,2,256,256]{3,2,1,0:T(8,128)(2,1)} %bitcast.32), channel_id=1, source_target_pairs={{0,1},{1,2},{2,3},{3,0},{4,5},{5,6},{6,7},{7,4},{8,9},{9,10},{10,1... | collective-permute-start | bytes 1572872 | tf_op jit(solution)/shard_map/ppermute | solution.py:295
  278.2 12.1 %copy-start.19 = (bf16[2,2,256,256]{3,2,1,0:T(8,128)(2,1)}, bf16[2,2,256,256]{3,2,1,0:T(8,128)(2,1)S(1)}, u32[]{:S(2)}) copy-start(bf16[2,2,256,256]{3,2,1,0:T(8,128)(2,1)S(1)} %collective-permute-done.22.refs_3_) | copy-start | bytes 1572868
  280.5 9.8 %copy-start.20 = (bf16[2,2,256,256]{3,2,1,0:T(8,128)(2,1)}, bf16[2,2,256,256]{3,2,1,0:T(8,128)(2,1)S(1)}, u32[]{:S(2)}) copy-start(bf16[2,2,256,256]{3,2,1,0:T(8,128)(2,1)S(1)} %collective-permute-done.21.refs_2_) | copy-start | bytes 1572868
  290.3 0.8 copy-start.21
  295.1 16.4 %copy-start.29 = (bf16[224,512]{1,0:T(8,128)(2,1)S(1)}, bf16[224,512]{1,0:T(8,128)(2,1)}, u32[]{:S(2)}) copy-start(bf16[224,512]{1,0:T(8,128)(2,1)} %get-tuple-element.42) | copy-start | bytes 688132
  295.1 19.3 %copy-start.28 = (bf16[224,512]{1,0:T(8,128)(2,1)S(1)}, bf16[224,512]{1,0:T(8,128)(2,1)}, u32[]{:S(2)}) copy-start(bf16[224,512]{1,0:T(8,128)(2,1)} %get-tuple-element.43) | copy-start | bytes 688132
  295.1 2.2 collective-permute-start.23
  299.4 30.3 %copy-start.9 = (bf16[128,2048]{1,0:T(8,128)(2,1)S(1)}, bf16[128,2048]{1,0:T(8,128)(2,1)}, u32[]{:S(2)}) copy-start(bf16[128,2048]{1,0:T(8,128)(2,1)} %get-tuple-element.35) | copy-start | bytes 1572868
  299.4 30.3 %copy-start.10 = (bf16[128,2048]{1,0:T(8,128)(2,1)S(1)}, bf16[128,2048]{1,0:T(8,128)(2,1)}, u32[]{:S(2)}) copy-start(bf16[128,2048]{1,0:T(8,128)(2,1)} %get-tuple-element.38) | copy-start | bytes 1572868
  299.4 30.3 %copy-start.11 = (bf16[96,2048]{1,0:T(8,128)(2,1)S(1)}, bf16[96,2048]{1,0:T(8,128)(2,1)}, u32[]{:S(2)}) copy-start(bf16[96,2048]{1,0:T(8,128)(2,1)} %get-tuple-element.37) | copy-start | bytes 1179652
  299.4 30.3 %copy-start.12 = (bf16[96,2048]{1,0:T(8,128)(2,1)S(1)}, bf16[96,2048]{1,0:T(8,128)(2,1)}, u32[]{:S(2)}) copy-start(bf16[96,2048]{1,0:T(8,128)(2,1)} %get-tuple-element.39) | copy-start | bytes 1179652
  299.4 40.9 %all-to-all-start.4 = ((bf16[16,32,512]{2,1,0:T(8,128)(2,1)}), bf16[16,32,512]{2,1,0:T(8,128)(2,1)S(1)}, u32[]{:S(2)}, u32[]{:S(2)}) async-start(bf16[16,32,512]{2,1,0:T(8,128)(2,1)} %bitcast.18), calls=%async_computation.4 | async-start | bytes 1048576 | tf_op jit(solution)/shard_map/all_to_all | solution.py:368
  311.3 13.8 %collective-permute-start.3 = (bf16[224,512]{1,0:T(8,128)(2,1)}, bf16[224,512]{1,0:T(8,128)(2,1)S(1)}, u32[]{:S(2)}, u32[]{:S(2)}) collective-permute-start(bf16[224,512]{1,0:T(8,128)(2,1)} %get-tuple-element.41), channel_id=1, source_target_pairs={{0,1},{1,2},{2,3},{3,0},{4,5},{5,6},{6,7},{7,4},{8,9},{9,10},{10,1... | collective-permute-start | bytes 688136 | tf_op jit(solution)/shard_map/ppermute | solution.py:303
  311.4 13.7 %collective-permute-start.4 = (bf16[224,512]{1,0:T(8,128)(2,1)S(1)}, bf16[224,512]{1,0:T(8,128)(2,1)S(1)}, u32[]{:S(2)}, u32[]{:S(2)}) collective-permute-start(bf16[224,512]{1,0:T(8,128)(2,1)S(1)} %copy-done.29), channel_id=1, source_target_pairs={{0,2},{1,3},{2,0},{3,1},{4,6},{5,7},{6,4},{7,5},{8,10},{9,11},{10,... | collective-permute-start | bytes 688136 | tf_op jit(solution)/shard_map/ppermute | solution.py:303
  314.3 11.2 %collective-permute-start.5 = (bf16[224,512]{1,0:T(8,128)(2,1)S(1)}, bf16[224,512]{1,0:T(8,128)(2,1)S(1)}, u32[]{:S(2)}, u32[]{:S(2)}) collective-permute-start(bf16[224,512]{1,0:T(8,128)(2,1)S(1)} %copy-done.28), channel_id=1, source_target_pairs={{0,3},{1,0},{2,1},{3,2},{4,7},{5,4},{6,5},{7,6},{8,11},{9,8},{10,9... | collective-permute-start | bytes 688136 | tf_op jit(solution)/shard_map/ppermute | solution.py:303
  325.1 0.7 copy-start.13
  325.1 0.8 copy-start.14
  325.5 0.7 copy-start.15
Sparse Core Ops, SparseCore 0:
  65.5 85.1 all-gather.1

commit v3 on v2

--- a/solution.py
+++ b/solution.py
@@ -16,10 +16,53 @@
     return pltpu.CompilerParams(dimension_semantics=semantics, vmem_limit_bytes=VMEM)
 
 
+def rows_kernel(place_ref, tokens_ref, routes_ref, logits_ref, out_ref):
+    values = tokens_ref[...].astype(F32)
+    rows, depth = values.shape
+    mean_square = jnp.mean(values * values, axis=-1, keepdims=True)
+    out_ref[:, :depth] = (values * lax.rsqrt(mean_square + 1e-06)).astype(BF16)
+    dims = (rows, routes_ref.shape[1])
+    spot = place_ref[0] * rows + lax.broadcasted_iota(jnp.int32, dims, 0)
+    mine = lax.broadcasted_iota(jnp.int32, dims, 1) == spot
+
+    def column(row):
+        return jnp.sum(jnp.where(mine, row, 0.0), axis=1, keepdims=True)
+
+    names = lax.broadcasted_iota(jnp.int32, (rows, LANES), 1).astype(F32)
+    logits = [column(logits_ref[k : k + 1]) for k in range(2)]
+    share = 0.0
+    for k in range(2):
+        weight = 1.0 / (1.0 + jnp.exp(logits[1 - k] - logits[k]))
+        named = column(routes_ref[k : k + 1].astype(F32)) == names
+        share = share + jnp.where(named, weight, 0.0)
+    out_ref[:, depth:] = share.astype(BF16)
+
+
+def rows_of(place, tokens, routes, route_logits, some):
+    count, depth = tokens.shape
+    return pl.pallas_call(
+        rows_kernel,
+        grid_spec=pltpu.PrefetchScalarGridSpec(
+            num_scalar_prefetch=1,
+            grid=(1,),
+            in_specs=[
+                pl.BlockSpec((some, depth), lambda i, p: (p[0], 0)),
+                pl.BlockSpec((2, count), lambda i, p: (0, 0)),
+                pl.BlockSpec((2, count), lambda i, p: (0, 0)),
+            ],
+            out_specs=pl.BlockSpec((some, depth + LANES), lambda i, p: (0, 0)),
+        ),
+        out_shape=jax.ShapeDtypeStruct((some, depth + LANES), BF16),
+        compiler_params=params("arbitrary"),
+        cost_estimate=pl.CostEstimate(flops=some * depth * 1000, bytes_accessed=some * depth * 4, transcendentals=some * 4),
+        name="rows",
+    )(place, tokens, routes.T, route_logits.T)
+
+
 def pack_kernel(parts, width, place_ref, scale_ref, gate_ref, up_ref, first_ref, *late_refs):
     del place_ref
     both = jnp.concatenate([gate_ref[0], up_ref[0]], axis=0)
-    columns = (both.T * scale_ref[...]).astype(BF16)
+    columns = (both.T * jnp.concatenate([scale_ref[...]] * 2, axis=1)).astype(BF16)
     blocks = columns.shape[0] // width
     for k in range(blocks):
         low, size = parts[0]
@@ -35,7 +78,7 @@
 
 def pack(place, gain, w_gate, w_up, parts, width):
     experts, rows, columns = w_gate.shape
-    scale = jnp.concatenate([gain, gain])[None, :]
+    scale = gain[None, :]
     blocks = columns // width
     chosen = lambda s, place_ref: (lax.rem(s + place_ref[0], experts), 0, 0)
     out = pl.pallas_call(
@@ -44,7 +87,7 @@
             num_scalar_prefetch=1,
             grid=(experts,),
             in_specs=[
-                pl.BlockSpec((1, 2 * rows), lambda s, place_ref: (0, 0)),
+                pl.BlockSpec((1, rows), lambda s, place_ref: (0, 0)),
                 pl.BlockSpec((1, rows, columns), chosen),
                 pl.BlockSpec((1, rows, columns), chosen),
             ],
@@ -317,18 +360,7 @@
     n_z = n_fs // 2
 
     some = count // n_tp
-    tokens, routes, route_logits = (
-        lax.dynamic_slice_in_dim(a, expert * some, some) for a in (tokens, routes, route_logits)
-    )
-    values = tokens.astype(F32)
-    mean_square = jnp.mean(values * values, axis=-1, keepdims=True)
-    normed = (values * lax.rsqrt(mean_square + 1e-06)).astype(BF16)
-    first = jax.nn.sigmoid(route_logits[:, 0:1] - route_logits[:, 1:2])
-    second = jax.nn.sigmoid(route_logits[:, 1:2] - route_logits[:, 0:1])
-    names = lax.broadcasted_iota(jnp.int32, (some, LANES), 1)
-    share = first * (routes[:, 0:1] == names).astype(F32)
-    share = (share + second * (routes[:, 1:2] == names).astype(F32)).astype(BF16)
-    rows = jnp.concatenate([normed, share], axis=1)
+    rows = rows_of(place, tokens, routes, route_logits, some)
     rows, place = lax.optimization_barrier((rows, place))
     quarter = lax.all_gather(rows, "fs", axis=0, axis_index_groups=columns, tiled=True)
     first_part, late_parts = pack(place, gain, w_gate, w_up, parts, hidden_rows)

time: 349 us -> 346 us (level)
  other arithmetic: 10.9 us -> 6.86 us
where the time goes in v3:
time: 346 us; the launch traced here: 345 us
  waiting for transfers between devices  171 us (49%)
  starting transfers between devices  74.4 us (22%)
  Pallas kernels  53 us (15%)
  blocking collectives  20 us (6%)
  between operations  14.4 us (4%)
  other arithmetic  6.86 us (2%)
  local copies, waits for them, and re-layouts  4.9 us (1%)
    ppermute x12, waiting for transfers between devices, around(): lax.ppermute(array, axis, [(i, (i + shift) % n) for i in range(n)])  73.8 us
    all_to_all x1, waiting for transfers between devices, body(): received = lax.all_to_all(across, 'fs', 0, 0, tiled=True)  41 us
    all_to_all x1, starting transfers between devices, body(): received = lax.all_to_all(across, 'fs', 0, 0, tiled=True)  24.7 us
    all_gather x1, waiting for transfers between devices, body(): lax.all_gather(rows, 'fs', axis=0, axis_index_groups=columns, tiled=True)  23.5 us
    all_to_all x1, blocking collectives, body(): lax.all_to_all(first_part, 'tp', 0, 0, tiled=True)  20 us
    ppermute x6, waiting for transfers between devices, dealt(): lax.ppermute(pieces[shift], axis, [(i, (i + shift) % n) for i in range(n)])  19.1 us
    all_to_all x2, starting transfers between devices, body(): lax.all_to_all(summed, 'fs', 0, 0, axis_index_groups=columns, tiled=True)  18.1 us
    pallas_call x3, Pallas kernels, hidden_of(): pl.pallas_call(functools.partial(hidden_kernel, depth, n_tp, first, len(b...  17.1 us
  transfers between devices with their start and end apart: 29, of which 17 were waited for; matrix products, arithmetic and copies ran while one was open for 1% of the time, Pallas kernels for 12%

profile of v3, /device:TPU:40, one launch (start us, length us, event | category | flops | bytes accessed | tf_op | source)
XLA Modules:
  0.0 344.9 jit_solution(1300892852795405763)
XLA Ops:
  7.2 0.6 pad_add_fusion.place_ref
  7.8 2.2 rows.1
  10.1 5.4 %pack.1 = (bf16[4,8,128,128]{3,2,1,0:T(8,128)(2,1)}, bf16[8,96,128]{2,1,0:T(8,128)(2,1)}, bf16[8,96,128]{2,1,0:T(8,128)(2,1)}, bf16[8,96,128]{2,1,0:T(8,128)(2,1)}, bf16[8,96,128]{2,1,0:T(8,128)(2,1)}) custom-call(s32[2]{0:T(128)} %pad_add_fusion.place_ref, f32[1,64]{1,0:T(1,128)} %bitcast.37, f32[4,64,1792]{2,1,0:T(8,128)} %gate_ref.1, f32[4,64,1792]{2,1,0:T(8,128)} %up_ref.1), custom_call_target="tpu_custom_call" | custom-call | flops 458752000 | bytes 5505024 | tf_op jit(solution)/shard_map/pack/pallas_call | solution.py:84
  15.5 20.0 %all_to_all.25 = bf16[4,1024,128]{2,1,0:T(8,128)(2,1)} all-to-all(bf16[4,1024,128]{2,1,0:T(8,128)(2,1)} %bitcast.21), channel_id=1, replica_groups=mesh['grp'=2,'fs'=32,'tp'=4] {'tp'}, dimensions={0} | all-to-all | bytes 2097152 | tf_op jit(solution)/shard_map/all_to_all | solution.py:368
  35.5 24.7 %all-to-all-start.1 = ((bf16[32,128,128]{2,1,0:T(8,128)(2,1)}), bf16[32,128,128]{2,1,0:T(8,128)(2,1)S(1)}, u32[]{:S(2)}, u32[]{:S(2)}) async-start(bf16[32,128,128]{2,1,0:T(8,128)(2,1)} %bitcast.6), calls=%async_computation.1 | async-start | bytes 2097152 | tf_op jit(solution)/shard_map/all_to_all | solution.py:369
  60.3 0.7 all-gather.2.cloned.1.call-update
  61.1 0.9 collective-permute-start
  62.0 1.9 collective-permute-start.1
  63.8 1.0 collective-permute-start.2
  64.8 8.4 %collective-permute-done.refs_1_ = bf16[8,96,128]{2,1,0:T(8,128)(2,1)S(1)} collective-permute-done((bf16[8,96,128]{2,1,0:T(8,128)(2,1)S(1)}, bf16[8,96,128]{2,1,0:T(8,128)(2,1)S(1)}, u32[]{:S(2)}, u32[]{:S(2)}) %collective-permute-start) | collective-permute-done | bytes 196640 | tf_op jit(solution)/shard_map/ppermute | solution.py:346
  73.2 0.6 collective-permute-done.2.refs_3_
  74.0 0.5 copy-done.17
  74.5 3.4 join.2
  77.9 41.0 %all-to-all-done.1.recv_ref = bf16[32,128,128]{2,1,0:T(8,128)(2,1)S(1)} async-done(((bf16[32,128,128]{2,1,0:T(8,128)(2,1)}), bf16[32,128,128]{2,1,0:T(8,128)(2,1)S(1)}, u32[]{:S(2)}, u32[]{:S(2)}) %all-to-all-start.1) | async-done | bytes 1048608 | tf_op jit(solution)/shard_map/all_to_all | solution.py:369
  118.9 5.8 %all-to-all-start.2 = ((bf16[32,96,128]{2,1,0:T(8,128)(2,1)}), bf16[32,96,128]{2,1,0:T(8,128)(2,1)}, u32[]{:S(2)}, u32[]{:S(2)}) async-start(bf16[32,96,128]{2,1,0:T(8,128)(2,1)} %join.2), calls=%async_computation.2 | async-start | bytes 1572864 | tf_op jit(solution)/shard_map/all_to_all | solution.py:372
  124.7 23.5 %all-gather.2.cloned.1.call-done.in_ref = bf16[256,2176]{1,0:T(8,128)(2,1)} async-done(((bf16[16,2176]{1,0:T(8,128)(2,1)}), bf16[256,2176]{1,0:T(8,128)(2,1)}) %all-gather.2.cloned.1.call-update) | async-done | bytes 1114128 | tf_op jit(solution)/shard_map/all_gather | solution.py:365
  148.2 2.4 held.1.refs_1_.refs_2_
  150.6 4.7 %collective-permute-start.11 = (bf16[256,2176]{1,0:T(8,128)(2,1)}, bf16[256,2176]{1,0:T(8,128)(2,1)S(1)}, u32[]{:S(2)}, u32[]{:S(2)}) collective-permute-start(bf16[256,2176]{1,0:T(8,128)(2,1)} %held.1.refs_1_.refs_2_), channel_id=1, source_target_pairs={{0,3},{1,0},{2,1},{3,2},{4,7},{5,4},{6,5},{7,6},{8,11},{9,8},{10,9... | collective-permute-start | bytes 3342344 | tf_op jit(solution)/shard_map/ppermute | solution.py:338
  155.3 1.3 collective-permute-start.7
  156.6 39.0 %collective-permute-done.11.refs_7_.refs_8_ = bf16[256,2176]{1,0:T(8,128)(2,1)S(1)} collective-permute-done((bf16[256,2176]{1,0:T(8,128)(2,1)}, bf16[256,2176]{1,0:T(8,128)(2,1)S(1)}, u32[]{:S(2)}, u32[]{:S(2)}) %collective-permute-start.11) | collective-permute-done | bytes 1114144 | tf_op jit(solution)/shard_map/ppermute | solution.py:338
  195.6 0.5 collective-permute-start.10
  196.1 3.0 collective-permute-done.7.refs_3_.refs_4_
  199.1 3.5 %unpack.2 = (bf16[128,2048]{1,0:T(8,128)(2,1)}, bf16[128,2048]{1,0:T(8,128)(2,1)}, bf16[256,2048]{1,0:T(8,128)(2,1)}) custom-call(bf16[32,128,128]{2,1,0:T(8,128)(2,1)} %copy-done.7), custom_call_target="tpu_custom_call" | custom-call | flops 20971520 | bytes 3145728 | tf_op jit(solution)/shard_map/unpack/pallas_call | solution.py:202
  202.8 0.9 copy-done.3
  203.7 0.4 copy-done.4
  204.1 0.3 copy-done.5
  204.4 0.3 copy-done.6
  204.7 5.2 %hidden.3 = bf16[4,256,128]{2,1,0:T(8,128)(2,1)} custom-call(s32[2]{0:T(128)} %pad_add_fusion.place_ref, bf16[256,2048]{1,0:T(8,128)(2,1)} %get-tuple-element.45.refs_0_, bf16[256,2176]{1,0:T(8,128)(2,1)} %held.1.refs_1_.refs_2_, bf16[256,2176]{1,0:T(8,128)(2,1)} %copy-done.3, bf16[256,2176]{1,0:T(8,128)(2,1)} %copy-done.2, bf16[256,2176]{1,0:T(8,128)(2,1)} %copy-done.6, ...), custom_call_target="tpu_custom_call" | custom-call | flops 1073741824 | bytes 4456448 | tf_op jit(solution)/shard_map/hidden/pallas_call | solution.py:256
  209.9 1.4 collective-permute-start.15
  211.3 1.2 collective-permute-start.13
  212.5 2.8 unpack.3
  215.3 5.2 %hidden.4 = bf16[4,256,128]{2,1,0:T(8,128)(2,1)} custom-call(s32[2]{0:T(128)} %pad_add_fusion.place_ref, bf16[256,2048]{1,0:T(8,128)(2,1)} %get-tuple-element.47.refs_0_.refs_1_, bf16[256,2176]{1,0:T(8,128)(2,1)} %held.1.refs_1_.refs_2_, bf16[256,2176]{1,0:T(8,128)(2,1)} %copy-done.3, bf16[256,2176]{1,0:T(8,128)(2,1)} %copy-done.2, ...), custom_call_target="tpu_custom_call" | custom-call | flops 1073741824 | bytes 4456448 | tf_op jit(solution)/shard_map/hidden/pallas_call | solution.py:256
  220.5 2.3 collective-permute-start.18
  222.8 2.2 collective-permute-start.17
  225.0 0.7 collective-permute-start.16
  225.7 4.6 %cast_down.1 = (bf16[4,256,512]{2,1,0:T(8,128)(2,1)}, bf16[224,512]{1,0:T(8,128)(2,1)}, bf16[224,512]{1,0:T(8,128)(2,1)}, bf16[224,512]{1,0:T(8,128)(2,1)}, bf16[224,512]{1,0:T(8,128)(2,1)}) custom-call(s32[2]{0:T(128)} %pad_add_fusion.place_ref, f32[4,224,512]{2,1,0:T(8,128)} %down_ref.1), custom_call_target="tpu_custom_call" | custom-call | flops 229376000 | bytes 3670016 | tf_op jit(solution)/shard_map/cast_down/pallas_call | solution.py:130
  230.6 3.2 collective-permute-done.17.refs_6_
  233.8 4.2 %collective-permute-done.16.refs_5_ = bf16[2,2,256,128]{3,2,1,0:T(8,128)(2,1)S(1)} collective-permute-done((bf16[2,2,256,128]{3,2,1,0:T(8,128)(2,1)}, bf16[2,2,256,128]{3,2,1,0:T(8,128)(2,1)S(1)}, u32[]{:S(2)}, u32[]{:S(2)}) %collective-permute-start.16) | collective-permute-done | bytes 262176 | tf_op jit(solution)/shard_map/ppermute | solution.py:338
  238.1 0.7 copy-done.26
  238.7 4.1 %down.2 = (bf16[16,2,16,512]{3,2,1,0:T(8,128)(2,1)}, bf16[16,2,16,512]{3,2,1,0:T(8,128)(2,1)}) custom-call(s32[2]{0:T(128)} %pad_add_fusion.place_ref, bf16[4,256,512]{2,1,0:T(8,128)(2,1)} %get-tuple-element.44.down_ref, bf16[2,2,256,128]{3,2,1,0:T(8,128)(2,1)} %bitcast.30, bf16[2,2,256,128]{3,2,1,0:T(8,128)(2,1)} %copy-done.23, ...), custom_call_target="tpu_custom_call" | custom-call | flops 1073741824 | bytes 3670016 | tf_op jit(solution)/shard_map/down/pallas_call | solution.py:299
  243.0 2.1 collective-permute-done.19
  245.1 2.1 add_convert_fusion.1
  247.1 6.2 %all-to-all-start.3 = ((bf16[16,32,512]{2,1,0:T(8,128)(2,1)}), bf16[16,32,512]{2,1,0:T(8,128)(2,1)S(1)}, u32[]{:S(2)}, u32[]{:S(2)}) async-start(bf16[16,32,512]{2,1,0:T(8,128)(2,1)} %bitcast.14), calls=%async_computation.3 | async-start | bytes 1048576 | tf_op jit(solution)/shard_map/all_to_all | solution.py:400
  253.4 6.7 %hidden.5 = bf16[4,256,256]{2,1,0:T(8,128)(2,1)} custom-call(s32[2]{0:T(128)} %pad_add_fusion.place_ref, bf16[256,2048]{1,0:T(8,128)(2,1)} %get-tuple-element.45.refs_0_, bf16[256,2048]{1,0:T(8,128)(2,1)} %get-tuple-element.47.refs_0_.refs_1_, bf16[256,2176]{1,0:T(8,128)(2,1)} %held.1.refs_1_.refs_2_, bf16[256,2176]{1,0:T(8,128)(2,1)} %copy-done.3, ...), custom_call_target="tpu_custom_call" | custom-call | flops 2147483648 | bytes 4456448 | tf_op jit(solution)/shard_map/hidden/pallas_call | solution.py:256
  260.1 0.9 collective-permute-start.22
  261.0 1.4 collective-permute-start.21
  262.4 0.8 collective-permute-start.20
  263.2 12.0 %collective-permute-done.22.refs_3_ = bf16[2,2,256,256]{3,2,1,0:T(8,128)(2,1)S(1)} collective-permute-done((bf16[2,2,256,256]{3,2,1,0:T(8,128)(2,1)}, bf16[2,2,256,256]{3,2,1,0:T(8,128)(2,1)S(1)}, u32[]{:S(2)}, u32[]{:S(2)}) %collective-permute-start.22) | collective-permute-done | bytes 524320 | tf_op jit(solution)/shard_map/ppermute | solution.py:338
  275.2 2.4 collective-permute-done.21.refs_2_
  277.6 9.8 %collective-permute-done.20.refs_1_ = bf16[2,2,256,256]{3,2,1,0:T(8,128)(2,1)S(1)} collective-permute-done((bf16[2,2,256,256]{3,2,1,0:T(8,128)(2,1)}, bf16[2,2,256,256]{3,2,1,0:T(8,128)(2,1)S(1)}, u32[]{:S(2)}, u32[]{:S(2)}) %collective-permute-start.20) | collective-permute-done | bytes 524320 | tf_op jit(solution)/shard_map/ppermute | solution.py:338
  287.4 0.8 copy-done.20
  288.2 3.9 %down.3 = (bf16[16,2,16,512]{3,2,1,0:T(8,128)(2,1)}, bf16[16,2,16,512]{3,2,1,0:T(8,128)(2,1)}) custom-call(s32[2]{0:T(128)} %pad_add_fusion.place_ref, bf16[4,256,512]{2,1,0:T(8,128)(2,1)} %get-tuple-element.44.down_ref, bf16[2,2,256,256]{3,2,1,0:T(8,128)(2,1)} %bitcast.26, bf16[2,2,256,256]{3,2,1,0:T(8,128)(2,1)} %copy-done.20, ...), custom_call_target="tpu_custom_call" | custom-call | flops 1073741824 | bytes 3670016 | tf_op jit(solution)/shard_map/down/pallas_call | solution.py:299
  292.3 2.1 collective-permute-done.23
  294.4 2.0 add_convert_fusion
  296.4 11.9 %all-to-all-start.4 = ((bf16[16,32,512]{2,1,0:T(8,128)(2,1)}), bf16[16,32,512]{2,1,0:T(8,128)(2,1)S(1)}, u32[]{:S(2)}, u32[]{:S(2)}) async-start(bf16[16,32,512]{2,1,0:T(8,128)(2,1)} %bitcast.16), calls=%async_computation.4 | async-start | bytes 1048576 | tf_op jit(solution)/shard_map/all_to_all | solution.py:400
  308.5 2.8 collective-permute-start.4
  311.3 1.2 collective-permute-start.5
  312.5 9.7 %collective-permute-done.3.refs_1_ = bf16[224,512]{1,0:T(8,128)(2,1)S(1)} collective-permute-done((bf16[224,512]{1,0:T(8,128)(2,1)}, bf16[224,512]{1,0:T(8,128)(2,1)S(1)}, u32[]{:S(2)}, u32[]{:S(2)}) %collective-permute-start.3) | collective-permute-done | bytes 229408 | tf_op jit(solution)/shard_map/ppermute | solution.py:346
  322.2 0.4 collective-permute-done.5.refs_3_
  322.9 0.3 copy-done.14
  323.3 3.5 %join.3 = bf16[224,2048]{1,0:T(8,128)(2,1)} custom-call(s32[2]{0:T(128)} %pad_add_fusion.place_ref, bf16[224,512]{1,0:T(8,128)(2,1)} %get-tuple-element.40.refs_0_, bf16[224,512]{1,0:T(8,128)(2,1)} %copy-done.12, bf16[224,512]{1,0:T(8,128)(2,1)} %copy-done.13, bf16[224,512]{1,0:T(8,128)(2,1)} %copy-done.14), custom_call_target="tpu_custom_call" | custom-call | flops 229376000 | bytes 1835008 | tf_op jit(solution)/shard_map/join/pallas_call | solution.py:166
  326.8 1.3 maximum_bitcast_fusion
  328.2 9.2 %all-to-all-done.4 = bf16[16,32,512]{2,1,0:T(8,128)(2,1)S(1)} async-done(((bf16[16,32,512]{2,1,0:T(8,128)(2,1)}), bf16[16,32,512]{2,1,0:T(8,128)(2,1)S(1)}, u32[]{:S(2)}, u32[]{:S(2)}) %all-to-all-start.4) | async-done | bytes 524320 | tf_op jit(solution)/shard_map/all_to_all | solution.py:400
  337.4 0.6 pad_maximum_fusion
  (80 shorter events, 1.5 us)
Async XLA Ops:
  15.5 45.6 %copy-start.31 = (bf16[8,96,128]{2,1,0:T(8,128)(2,1)S(1)}, bf16[8,96,128]{2,1,0:T(8,128)(2,1)}, u32[]{:S(2)}) copy-start(bf16[8,96,128]{2,1,0:T(8,128)(2,1)} %get-tuple-element.30) | copy-start | bytes 589828
  15.5 46.4 %copy-start.30 = (bf16[8,96,128]{2,1,0:T(8,128)(2,1)S(1)}, bf16[8,96,128]{2,1,0:T(8,128)(2,1)}, u32[]{:S(2)}) copy-start(bf16[8,96,128]{2,1,0:T(8,128)(2,1)} %get-tuple-element.31) | copy-start | bytes 589828
  15.5 48.3 %copy-start.29 = (bf16[8,96,128]{2,1,0:T(8,128)(2,1)S(1)}, bf16[8,96,128]{2,1,0:T(8,128)(2,1)}, u32[]{:S(2)}) copy-start(bf16[8,96,128]{2,1,0:T(8,128)(2,1)} %get-tuple-element.32) | copy-start | bytes 589828
  35.5 83.4 %all-to-all-start.1 = ((bf16[32,128,128]{2,1,0:T(8,128)(2,1)}), bf16[32,128,128]{2,1,0:T(8,128)(2,1)S(1)}, u32[]{:S(2)}, u32[]{:S(2)}) async-start(bf16[32,128,128]{2,1,0:T(8,128)(2,1)} %bitcast.6), calls=%async_computation.1 | async-start | bytes 2097152 | tf_op jit(solution)/shard_map/all_to_all | solution.py:369
  60.3 87.9 %all-gather.2.cloned.1.call-start = ((), (), s32[]{:S(2)}) async-start(), calls=%async_computation.5 | async-start | bytes 1183744 | tf_op jit(solution)/shard_map/all_gather | solution.py:365
  61.1 12.2 %collective-permute-start = (bf16[8,96,128]{2,1,0:T(8,128)(2,1)S(1)}, bf16[8,96,128]{2,1,0:T(8,128)(2,1)S(1)}, u32[]{:S(2)}, u32[]{:S(2)}) collective-permute-start(bf16[8,96,128]{2,1,0:T(8,128)(2,1)S(1)} %copy-done.31), channel_id=1, source_target_pairs={{0,1},{1,2},{2,3},{3,0},{4,5},{5,6},{6,7},{7,4},{8,9},{9,10},{10,1... | collective-permute-start | bytes 589832 | tf_op jit(solution)/shard_map/ppermute | solution.py:346
  62.0 11.3 %collective-permute-start.1 = (bf16[8,96,128]{2,1,0:T(8,128)(2,1)S(1)}, bf16[8,96,128]{2,1,0:T(8,128)(2,1)S(1)}, u32[]{:S(2)}, u32[]{:S(2)}) collective-permute-start(bf16[8,96,128]{2,1,0:T(8,128)(2,1)S(1)} %copy-done.30), channel_id=1, source_target_pairs={{0,2},{1,3},{2,0},{3,1},{4,6},{5,7},{6,4},{7,5},{8,10},{9,11},{10,... | collective-permute-start | bytes 589832 | tf_op jit(solution)/shard_map/ppermute | solution.py:346
  63.8 10.0 %collective-permute-start.2 = (bf16[8,96,128]{2,1,0:T(8,128)(2,1)S(1)}, bf16[8,96,128]{2,1,0:T(8,128)(2,1)S(1)}, u32[]{:S(2)}, u32[]{:S(2)}) collective-permute-start(bf16[8,96,128]{2,1,0:T(8,128)(2,1)S(1)} %copy-done.29), channel_id=1, source_target_pairs={{0,3},{1,0},{2,1},{3,2},{4,7},{5,4},{6,5},{7,6},{8,11},{9,8},{10,9... | collective-permute-start | bytes 589832 | tf_op jit(solution)/shard_map/ppermute | solution.py:346
  73.2 0.7 copy-start.15
  73.2 0.7 copy-start.16
  73.8 0.7 copy-start.17
  118.9 29.3 %copy-start.7 = (bf16[32,128,128]{2,1,0:T(8,128)(2,1)}, bf16[32,128,128]{2,1,0:T(8,128)(2,1)S(1)}, u32[]{:S(2)}) copy-start(bf16[32,128,128]{2,1,0:T(8,128)(2,1)S(1)} %all-to-all-done.1.recv_ref) | copy-start | bytes 3145732
  118.9 93.6 %all-to-all-start.2 = ((bf16[32,96,128]{2,1,0:T(8,128)(2,1)}), bf16[32,96,128]{2,1,0:T(8,128)(2,1)}, u32[]{:S(2)}, u32[]{:S(2)}) async-start(bf16[32,96,128]{2,1,0:T(8,128)(2,1)} %join.2), calls=%async_computation.2 | async-start | bytes 1572864 | tf_op jit(solution)/shard_map/all_to_all | solution.py:372
  150.6 45.0 %collective-permute-start.11 = (bf16[256,2176]{1,0:T(8,128)(2,1)}, bf16[256,2176]{1,0:T(8,128)(2,1)S(1)}, u32[]{:S(2)}, u32[]{:S(2)}) collective-permute-start(bf16[256,2176]{1,0:T(8,128)(2,1)} %held.1.refs_1_.refs_2_), channel_id=1, source_target_pairs={{0,3},{1,0},{2,1},{3,2},{4,7},{5,4},{6,5},{7,6},{8,11},{9,8},{10,9... | collective-permute-start | bytes 3342344 | tf_op jit(solution)/shard_map/ppermute | solution.py:338
  155.3 40.3 %collective-permute-start.9 = (bf16[256,2176]{1,0:T(8,128)(2,1)}, bf16[256,2176]{1,0:T(8,128)(2,1)S(1)}, u32[]{:S(2)}, u32[]{:S(2)}) collective-permute-start(bf16[256,2176]{1,0:T(8,128)(2,1)} %held.1.refs_1_.refs_2_), channel_id=1, source_target_pairs={{0,2},{1,3},{2,0},{3,1},{4,6},{5,7},{6,4},{7,5},{8,10},{9,11},{10,... | collective-permute-start | bytes 3342344 | tf_op jit(solution)/shard_map/ppermute | solution.py:338
  155.3 43.8 %collective-permute-start.7 = (bf16[256,2176]{1,0:T(8,128)(2,1)}, bf16[256,2176]{1,0:T(8,128)(2,1)S(1)}, u32[]{:S(2)}, u32[]{:S(2)}) collective-permute-start(bf16[256,2176]{1,0:T(8,128)(2,1)} %held.1.refs_1_.refs_2_), channel_id=1, source_target_pairs={{0,1},{1,2},{2,3},{3,0},{4,5},{5,6},{6,7},{7,4},{8,9},{9,10},{10,1... | collective-permute-start | bytes 3342344 | tf_op jit(solution)/shard_map/ppermute | solution.py:338
  156.6 46.1 %collective-permute-start.6 = (bf16[256,2176]{1,0:T(8,128)(2,1)}, bf16[256,2176]{1,0:T(8,128)(2,1)S(1)}, u32[]{:S(2)}, u32[]{:S(2)}) collective-permute-start(bf16[256,2176]{1,0:T(8,128)(2,1)} %held.1.refs_1_.refs_2_), channel_id=1, source_target_pairs={{0,4},{4,0},{8,12},{12,8},{16,20},{20,16},{24,28},{28,24},{32,36},... | collective-permute-start | bytes 3342344 | tf_op jit(solution)/shard_map/ppermute | solution.py:378
  195.5 7.2 %copy-start = (bf16[256,2176]{1,0:T(8,128)(2,1)}, bf16[256,2176]{1,0:T(8,128)(2,1)S(1)}, u32[]{:S(2)}) copy-start(bf16[256,2176]{1,0:T(8,128)(2,1)S(1)} %collective-permute-done.11.refs_7_.refs_8_) | copy-start | bytes 3342340
  195.5 7.1 %collective-permute-start.12 = (bf16[256,2176]{1,0:T(8,128)(2,1)S(1)}, bf16[256,2176]{1,0:T(8,128)(2,1)S(1)}, u32[]{:S(2)}, u32[]{:S(2)}) collective-permute-start(bf16[256,2176]{1,0:T(8,128)(2,1)S(1)} %collective-permute-done.11.refs_7_.refs_8_), channel_id=1, source_target_pairs={{0,4},{4,0},{8,12},{12,8},{16,20},{20,16},{24,28},{28,24},{32,36},... | collective-permute-start | bytes 3342344 | tf_op jit(solution)/shard_map/ppermute | solution.py:378
  195.6 7.2 %copy-start.1 = (bf16[256,2176]{1,0:T(8,128)(2,1)}, bf16[256,2176]{1,0:T(8,128)(2,1)S(1)}, u32[]{:S(2)}) copy-start(bf16[256,2176]{1,0:T(8,128)(2,1)S(1)} %collective-permute-done.9.refs_5_.refs_6_) | copy-start | bytes 3342340
  195.6 7.1 %collective-permute-start.10 = (bf16[256,2176]{1,0:T(8,128)(2,1)S(1)}, bf16[256,2176]{1,0:T(8,128)(2,1)S(1)}, u32[]{:S(2)}, u32[]{:S(2)}) collective-permute-start(bf16[256,2176]{1,0:T(8,128)(2,1)S(1)} %collective-permute-done.9.refs_5_.refs_6_), channel_id=1, source_target_pairs={{0,4},{4,0},{8,12},{12,8},{16,20},{20,16},{24,28},{28,24},{32,36},... | collective-permute-start | bytes 3342344 | tf_op jit(solution)/shard_map/ppermute | solution.py:378
  199.1 3.6 %copy-start.2 = (bf16[256,2176]{1,0:T(8,128)(2,1)}, bf16[256,2176]{1,0:T(8,128)(2,1)S(1)}, u32[]{:S(2)}) copy-start(bf16[256,2176]{1,0:T(8,128)(2,1)S(1)} %collective-permute-done.7.refs_3_.refs_4_) | copy-start | bytes 3342340
  199.1 3.6 %collective-permute-start.8 = (bf16[256,2176]{1,0:T(8,128)(2,1)S(1)}, bf16[256,2176]{1,0:T(8,128)(2,1)S(1)}, u32[]{:S(2)}, u32[]{:S(2)}) collective-permute-start(bf16[256,2176]{1,0:T(8,128)(2,1)S(1)} %collective-permute-done.7.refs_3_.refs_4_), channel_id=1, source_target_pairs={{0,4},{4,0},{8,12},{12,8},{16,20},{20,16},{24,28},{28,24},{32,36},... | collective-permute-start | bytes 3342344 | tf_op jit(solution)/shard_map/ppermute | solution.py:378
  202.7 1.0 copy-start.3
  202.7 1.4 copy-start.4
  202.7 1.7 copy-start.5
  202.7 2.0 copy-start.6
  209.9 15.1 %collective-permute-start.15 = (bf16[2,2,256,128]{3,2,1,0:T(8,128)(2,1)}, bf16[2,2,256,128]{3,2,1,0:T(8,128)(2,1)S(1)}, u32[]{:S(2)}, u32[]{:S(2)}) collective-permute-start(bf16[2,2,256,128]{3,2,1,0:T(8,128)(2,1)} %bitcast.27), channel_id=1, source_target_pairs={{0,3},{1,0},{2,1},{3,2},{4,7},{5,4},{6,5},{7,6},{8,11},{9,8},{10,9... | collective-permute-start | bytes 786440 | tf_op jit(solution)/shard_map/ppermute | solution.py:338
  211.3 19.0 %collective-permute-start.14 = (bf16[2,2,256,128]{3,2,1,0:T(8,128)(2,1)}, bf16[2,2,256,128]{3,2,1,0:T(8,128)(2,1)S(1)}, u32[]{:S(2)}, u32[]{:S(2)}) collective-permute-start(bf16[2,2,256,128]{3,2,1,0:T(8,128)(2,1)} %bitcast.28), channel_id=1, source_target_pairs={{0,2},{1,3},{2,0},{3,1},{4,6},{5,7},{6,4},{7,5},{8,10},{9,11},{10,... | collective-permute-start | bytes 786440 | tf_op jit(solution)/shard_map/ppermute | solution.py:338
  211.3 19.0 %collective-permute-start.13 = (bf16[2,2,256,128]{3,2,1,0:T(8,128)(2,1)}, bf16[2,2,256,128]{3,2,1,0:T(8,128)(2,1)S(1)}, u32[]{:S(2)}, u32[]{:S(2)}) collective-permute-start(bf16[2,2,256,128]{3,2,1,0:T(8,128)(2,1)} %bitcast.29), channel_id=1, source_target_pairs={{0,1},{1,2},{2,3},{3,0},{4,5},{5,6},{6,7},{7,4},{8,9},{9,10},{10,1... | collective-permute-start | bytes 786440 | tf_op jit(solution)/shard_map/ppermute | solution.py:338
  220.5 10.0 %collective-permute-start.18 = (bf16[2,2,256,128]{3,2,1,0:T(8,128)(2,1)}, bf16[2,2,256,128]{3,2,1,0:T(8,128)(2,1)S(1)}, u32[]{:S(2)}, u32[]{:S(2)}) collective-permute-start(bf16[2,2,256,128]{3,2,1,0:T(8,128)(2,1)} %bitcast.31), channel_id=1, source_target_pairs={{0,3},{1,0},{2,1},{3,2},{4,7},{5,4},{6,5},{7,6},{8,11},{9,8},{10,9... | collective-permute-start | bytes 786440 | tf_op jit(solution)/shard_map/ppermute | solution.py:338
  222.8 10.9 %collective-permute-start.17 = (bf16[2,2,256,128]{3,2,1,0:T(8,128)(2,1)}, bf16[2,2,256,128]{3,2,1,0:T(8,128)(2,1)S(1)}, u32[]{:S(2)}, u32[]{:S(2)}) collective-permute-start(bf16[2,2,256,128]{3,2,1,0:T(8,128)(2,1)} %bitcast.32), channel_id=1, source_target_pairs={{0,2},{1,3},{2,0},{3,1},{4,6},{5,7},{6,4},{7,5},{8,10},{9,11},{10,... | collective-permute-start | bytes 786440 | tf_op jit(solution)/shard_map/ppermute | solution.py:338
  225.0 13.0 %copy-start.21 = (bf16[2,2,256,128]{3,2,1,0:T(8,128)(2,1)}, bf16[2,2,256,128]{3,2,1,0:T(8,128)(2,1)S(1)}, u32[]{:S(2)}) copy-start(bf16[2,2,256,128]{3,2,1,0:T(8,128)(2,1)S(1)} %collective-permute-done.15.refs_3_) | copy-start | bytes 786436
  225.0 13.0 %collective-permute-start.16 = (bf16[2,2,256,128]{3,2,1,0:T(8,128)(2,1)}, bf16[2,2,256,128]{3,2,1,0:T(8,128)(2,1)S(1)}, u32[]{:S(2)}, u32[]{:S(2)}) collective-permute-start(bf16[2,2,256,128]{3,2,1,0:T(8,128)(2,1)} %bitcast.33), channel_id=1, source_target_pairs={{0,1},{1,2},{2,3},{3,0},{4,5},{5,6},{6,7},{7,4},{8,9},{9,10},{10,1... | collective-permute-start | bytes 786440 | tf_op jit(solution)/shard_map/ppermute | solution.py:338
  230.3 7.7 %copy-start.22 = (bf16[2,2,256,128]{3,2,1,0:T(8,128)(2,1)}, bf16[2,2,256,128]{3,2,1,0:T(8,128)(2,1)S(1)}, u32[]{:S(2)}) copy-start(bf16[2,2,256,128]{3,2,1,0:T(8,128)(2,1)S(1)} %collective-permute-done.14.refs_2_) | copy-start | bytes 786436
  230.4 7.7 %copy-start.23 = (bf16[2,2,256,128]{3,2,1,0:T(8,128)(2,1)}, bf16[2,2,256,128]{3,2,1,0:T(8,128)(2,1)S(1)}, u32[]{:S(2)}) copy-start(bf16[2,2,256,128]{3,2,1,0:T(8,128)(2,1)S(1)} %collective-permute-done.13.refs_1_) | copy-start | bytes 786436
  230.6 7.5 %copy-start.24 = (bf16[2,2,256,128]{3,2,1,0:T(8,128)(2,1)}, bf16[2,2,256,128]{3,2,1,0:T(8,128)(2,1)S(1)}, u32[]{:S(2)}) copy-start(bf16[2,2,256,128]{3,2,1,0:T(8,128)(2,1)S(1)} %collective-permute-done.18.refs_7_) | copy-start | bytes 786436
  233.8 4.3 %copy-start.25 = (bf16[2,2,256,128]{3,2,1,0:T(8,128)(2,1)}, bf16[2,2,256,128]{3,2,1,0:T(8,128)(2,1)S(1)}, u32[]{:S(2)}) copy-start(bf16[2,2,256,128]{3,2,1,0:T(8,128)(2,1)S(1)} %collective-permute-done.17.refs_6_) | copy-start | bytes 786436
  238.0 0.7 copy-start.26
  242.8 2.2 collective-permute-start.19
  247.1 49.3 %all-to-all-start.3 = ((bf16[16,32,512]{2,1,0:T(8,128)(2,1)}), bf16[16,32,512]{2,1,0:T(8,128)(2,1)S(1)}, u32[]{:S(2)}, u32[]{:S(2)}) async-start(bf16[16,32,512]{2,1,0:T(8,128)(2,1)} %bitcast.14), calls=%async_computation.3 | async-start | bytes 1048576 | tf_op jit(solution)/shard_map/all_to_all | solution.py:400
  260.1 15.1 %collective-permute-start.22 = (bf16[2,2,256,256]{3,2,1,0:T(8,128)(2,1)}, bf16[2,2,256,256]{3,2,1,0:T(8,128)(2,1)S(1)}, u32[]{:S(2)}, u32[]{:S(2)}) collective-permute-start(bf16[2,2,256,256]{3,2,1,0:T(8,128)(2,1)} %bitcast.23), channel_id=1, source_target_pairs={{0,3},{1,0},{2,1},{3,2},{4,7},{5,4},{6,5},{7,6},{8,11},{9,8},{10,9... | collective-permute-start | bytes 1572872 | tf_op jit(solution)/shard_map/ppermute | solution.py:338
  261.0 16.6 %collective-permute-start.21 = (bf16[2,2,256,256]{3,2,1,0:T(8,128)(2,1)}, bf16[2,2,256,256]{3,2,1,0:T(8,128)(2,1)S(1)}, u32[]{:S(2)}, u32[]{:S(2)}) collective-permute-start(bf16[2,2,256,256]{3,2,1,0:T(8,128)(2,1)} %bitcast.24), channel_id=1, source_target_pairs={{0,2},{1,3},{2,0},{3,1},{4,6},{5,7},{6,4},{7,5},{8,10},{9,11},{10,... | collective-permute-start | bytes 1572872 | tf_op jit(solution)/shard_map/ppermute | solution.py:338
  262.4 25.0 %collective-permute-start.20 = (bf16[2,2,256,256]{3,2,1,0:T(8,128)(2,1)}, bf16[2,2,256,256]{3,2,1,0:T(8,128)(2,1)S(1)}, u32[]{:S(2)}, u32[]{:S(2)}) collective-permute-start(bf16[2,2,256,256]{3,2,1,0:T(8,128)(2,1)} %bitcast.25), channel_id=1, source_target_pairs={{0,1},{1,2},{2,3},{3,0},{4,5},{5,6},{6,7},{7,4},{8,9},{9,10},{10,1... | collective-permute-start | bytes 1572872 | tf_op jit(solution)/shard_map/ppermute | solution.py:338
  275.2 12.2 %copy-start.18 = (bf16[2,2,256,256]{3,2,1,0:T(8,128)(2,1)}, bf16[2,2,256,256]{3,2,1,0:T(8,128)(2,1)S(1)}, u32[]{:S(2)}) copy-start(bf16[2,2,256,256]{3,2,1,0:T(8,128)(2,1)S(1)} %collective-permute-done.22.refs_3_) | copy-start | bytes 1572868
  277.6 9.8 %copy-start.19 = (bf16[2,2,256,256]{3,2,1,0:T(8,128)(2,1)}, bf16[2,2,256,256]{3,2,1,0:T(8,128)(2,1)S(1)}, u32[]{:S(2)}) copy-start(bf16[2,2,256,256]{3,2,1,0:T(8,128)(2,1)S(1)} %collective-permute-done.21.refs_2_) | copy-start | bytes 1572868
  287.4 0.8 copy-start.20
  292.1 16.4 %copy-start.28 = (bf16[224,512]{1,0:T(8,128)(2,1)S(1)}, bf16[224,512]{1,0:T(8,128)(2,1)}, u32[]{:S(2)}) copy-start(bf16[224,512]{1,0:T(8,128)(2,1)} %get-tuple-element.42) | copy-start | bytes 688132
  292.1 19.2 %copy-start.27 = (bf16[224,512]{1,0:T(8,128)(2,1)S(1)}, bf16[224,512]{1,0:T(8,128)(2,1)}, u32[]{:S(2)}) copy-start(bf16[224,512]{1,0:T(8,128)(2,1)} %get-tuple-element.43) | copy-start | bytes 688132
  292.1 2.2 collective-permute-start.23
  296.4 30.3 %copy-start.8 = (bf16[128,2048]{1,0:T(8,128)(2,1)S(1)}, bf16[128,2048]{1,0:T(8,128)(2,1)}, u32[]{:S(2)}) copy-start(bf16[128,2048]{1,0:T(8,128)(2,1)} %get-tuple-element.35) | copy-start | bytes 1572868
  296.4 30.3 %copy-start.9 = (bf16[128,2048]{1,0:T(8,128)(2,1)S(1)}, bf16[128,2048]{1,0:T(8,128)(2,1)}, u32[]{:S(2)}) copy-start(bf16[128,2048]{1,0:T(8,128)(2,1)} %get-tuple-element.38) | copy-start | bytes 1572868
  296.4 30.3 %copy-start.10 = (bf16[96,2048]{1,0:T(8,128)(2,1)S(1)}, bf16[96,2048]{1,0:T(8,128)(2,1)}, u32[]{:S(2)}) copy-start(bf16[96,2048]{1,0:T(8,128)(2,1)} %get-tuple-element.37) | copy-start | bytes 1179652
  296.4 30.4 %copy-start.11 = (bf16[96,2048]{1,0:T(8,128)(2,1)S(1)}, bf16[96,2048]{1,0:T(8,128)(2,1)}, u32[]{:S(2)}) copy-start(bf16[96,2048]{1,0:T(8,128)(2,1)} %get-tuple-element.39) | copy-start | bytes 1179652
  296.4 40.9 %all-to-all-start.4 = ((bf16[16,32,512]{2,1,0:T(8,128)(2,1)}), bf16[16,32,512]{2,1,0:T(8,128)(2,1)S(1)}, u32[]{:S(2)}, u32[]{:S(2)}) async-start(bf16[16,32,512]{2,1,0:T(8,128)(2,1)} %bitcast.16), calls=%async_computation.4 | async-start | bytes 1048576 | tf_op jit(solution)/shard_map/all_to_all | solution.py:400
  308.3 13.8 %collective-permute-start.3 = (bf16[224,512]{1,0:T(8,128)(2,1)}, bf16[224,512]{1,0:T(8,128)(2,1)S(1)}, u32[]{:S(2)}, u32[]{:S(2)}) collective-permute-start(bf16[224,512]{1,0:T(8,128)(2,1)} %get-tuple-element.41), channel_id=1, source_target_pairs={{0,1},{1,2},{2,3},{3,0},{4,5},{5,6},{6,7},{7,4},{8,9},{9,10},{10,1... | collective-permute-start | bytes 688136 | tf_op jit(solution)/shard_map/ppermute | solution.py:346
  308.5 13.7 %collective-permute-start.4 = (bf16[224,512]{1,0:T(8,128)(2,1)S(1)}, bf16[224,512]{1,0:T(8,128)(2,1)S(1)}, u32[]{:S(2)}, u32[]{:S(2)}) collective-permute-start(bf16[224,512]{1,0:T(8,128)(2,1)S(1)} %copy-done.28), channel_id=1, source_target_pairs={{0,2},{1,3},{2,0},{3,1},{4,6},{5,7},{6,4},{7,5},{8,10},{9,11},{10,... | collective-permute-start | bytes 688136 | tf_op jit(solution)/shard_map/ppermute | solution.py:346
  311.3 11.2 %collective-permute-start.5 = (bf16[224,512]{1,0:T(8,128)(2,1)S(1)}, bf16[224,512]{1,0:T(8,128)(2,1)S(1)}, u32[]{:S(2)}, u32[]{:S(2)}) collective-permute-start(bf16[224,512]{1,0:T(8,128)(2,1)S(1)} %copy-done.27), channel_id=1, source_target_pairs={{0,3},{1,0},{2,1},{3,2},{4,7},{5,4},{6,5},{7,6},{8,11},{9,8},{10,9... | collective-permute-start | bytes 688136 | tf_op jit(solution)/shard_map/ppermute | solution.py:346
  322.1 0.7 copy-start.12
  322.2 0.8 copy-start.13
  322.6 0.7 copy-start.14
Sparse Core Ops, SparseCore 0:
  62.9 85.2 all-gather.1
